TPU v7x, 32 devices: a whole 2x2x4 slice. The times are simulated.
32 devices in a mesh: grp: 2 (over x), ep: 4 (over y, core), tp: 4 (over z).
Axes of the slice: x: 2, y: 2, z: 4, core: 2. Of those that a mesh axis runs over, the one named last changes fastest.
Arguments:
- tokens: bfloat16 [3072, 4096], P(('grp', 'ep'), 'tp'), parts along dimension 0
- pre_gain: float32 [4096], replicated, may hold values from 0.1 to 1.9
- out_gain: float32 [4096], P('tp'), may hold values from 0.1 to 1.9
- chosen: int32 [8, 4, 48], P(('grp', 'ep')), parts along dimension 0, may hold values from 0 to 383, as said below
- route_weight: float32 [8, 4, 48], P(('grp', 'ep')), parts along dimension 0, may hold values from 0.3 to 3
- expert_gate: bfloat16 [4, 4096, 3072], P('ep', None, 'tp'), may hold values from -0.09375 to 0.09375
- expert_up: bfloat16 [4, 4096, 3072], P('ep', None, 'tp'), may hold values from -0.09375 to 0.09375
- expert_down: bfloat16 [4, 3072, 4096], P('ep', 'tp'), may hold values from -0.109375 to 0.109375
Outputs:
- output: bfloat16 [3072, 4096], P(('grp', 'ep'), 'tp'), parts along dimension 0
There are 2 independent parts, one for each index of `grp`. A program takes and returns all parts, laid end to end along the dimension named above; an argument that names none is the same for every part. Nothing has to cross between parts.
Inputs may be any that keep to these rules, and one draw needn't show every extreme that they name: chosen[b, e, k] is the position, within block b of 384 tokens, of the k-th token that expert e takes from that block; the 48 positions of one block and one expert are all different.
All inputs are finite; a program needn't handle non-finite values.
Results may differ from a plain program's by a relative error of at most 0.0075.
Values may be sent and summed in bfloat16 or wider, within the bound.
No kernel may reach another device: no remote copies, remote signals or barrier semaphores. Data moves between devices by JAX's collectives and lax.ppermute only.
A program may use at most 64 MiB of HBM per device.

v0:
```python
import jax
import jax.numpy as jnp
from jax import lax
from jax.sharding import PartitionSpec as P

NORM_EPS = 1e-06


def shards(tokens, pre_gain, out_gain, chosen, route_weight, expert_gate, expert_up, expert_down):
    model_width = pre_gain.shape[0]
    shard_width = tokens.shape[1]
    tok_count = tokens.shape[0]
    chosen_here = chosen[0]
    experts_all = chosen_here.shape[0]
    slot_count = chosen_here.shape[1]
    resident = tokens.astype(jnp.float32)
    square_sum = lax.psum(jnp.sum(resident * resident, axis=1), "tp")
    row_scale = lax.rsqrt(square_sum / model_width + NORM_EPS)[:, None]
    gain_slice = lax.dynamic_slice_in_dim(
        pre_gain, lax.axis_index("tp") * shard_width, shard_width, 0
    )
    normed = (resident * row_scale * gain_slice).astype(jnp.bfloat16)
    outgoing = jnp.take(normed, chosen_here, axis=0)
    incoming = lax.all_to_all(outgoing, "ep", split_axis=0, concat_axis=0, tiled=True)
    picked_rows = lax.all_gather(incoming.reshape(-1, shard_width), "tp", axis=1, tiled=True)
    gate_act = jnp.dot(picked_rows, expert_gate[0], preferred_element_type=jnp.float32)
    up_act = jnp.dot(picked_rows, expert_up[0], preferred_element_type=jnp.float32)
    hidden = (jax.nn.silu(gate_act) * up_act).astype(jnp.bfloat16)
    down_shard = expert_down[0]
    summed = lax.psum_scatter(
        lax.dot_general(
            down_shard, hidden, (((0,), (1,)), ((), ())), preferred_element_type=jnp.float32
        ).astype(jnp.bfloat16),
        "tp",
        scatter_dimension=0,
        tiled=True,
    )
    expert_out = summed.reshape(shard_width, experts_all, slot_count)
    returned = lax.all_to_all(expert_out, "ep", split_axis=1, concat_axis=1, tiled=True)
    weighted = returned.astype(jnp.float32) * route_weight[0][None]
    flat_weighted = weighted.reshape(shard_width, experts_all * slot_count)
    update_cols = (
        jnp.zeros((shard_width, tok_count), jnp.float32)
        .at[:, chosen_here.reshape(-1)]
        .add(flat_weighted)
    )
    mixed_rows = resident + update_cols.T
    out_sum = lax.psum(jnp.sum(mixed_rows * mixed_rows, axis=1), "tp")
    out_scale = lax.rsqrt(out_sum / model_width + NORM_EPS)[:, None]
    return (mixed_rows * out_scale * out_gain).astype(jnp.bfloat16)


def solution(mesh):
    return jax.shard_map(
        shards,
        mesh=mesh,
        in_specs=(
            P(("grp", "ep"), "tp"),
            P(),
            P("tp"),
            P(("grp", "ep"), None, None),
            P(("grp", "ep"), None, None),
            P("ep", None, "tp"),
            P("ep", None, "tp"),
            P("ep", "tp", None),
        ),
        out_specs=P(("grp", "ep"), "tp"),
        check_vma=False,
    )
```

profile of v0, /device:TPU:0, one launch (start us, length us, event | category | flops | bytes accessed | tf_op | source)
XLA Modules:
  0.0 150.9 jit_solution(1247583569600255627)
XLA Ops:
  6.5 0.0 all-gather.2.cloned.1.call-start
  6.5 0.7 compare_select_fusion.1
  7.2 0.7 compare_and_fusion
  7.9 1.4 fusion.12
  9.3 13.5 %psum.14 = f32[384]{0:T(512)S(1)} all-reduce(f32[384]{0:T(512)S(1)} %fusion.12), channel_id=1, replica_groups=mesh['grp'=2,'ep'=4,'tp'=4] {'tp'}, use_global_device_ids=true, to_apply=%region_1.0 | all-reduce | flops 384 | bytes 3072 | tf_op jit(solution)/shard_map/psum | solution.py:17
  22.8 0.1 reshape.80
  22.9 0.7 dynamic_slice.3
  23.6 1.4 fusion.14
  24.9 1.0 gather_fusion
  26.0 0.1 broadcast_select_fusion
  26.1 10.5 %all_to_all.10 = bf16[4,48,1024]{2,1,0:T(8,128)(2,1)} all-to-all(bf16[4,48,1024]{2,1,0:T(8,128)(2,1)S(1)} %broadcast_select_fusion), channel_id=1, replica_groups=mesh['grp'=2,'ep'=4,'tp'=4] {'ep'}, dimensions={0} | all-to-all | bytes 786432 | tf_op jit(solution)/shard_map/all_to_all | solution.py:24
  36.5 0.0 all-gather.2.cloned.1.call-update
  36.6 0.0 reduce-scatter.2.cloned.1.call-start
  36.6 34.4 %all-gather.2.cloned.1.call-done = bf16[192,4096]{1,0:T(8,128)(2,1)} async-done(((bf16[192,1024]{1,0:T(8,128)(2,1)}), bf16[192,4096]{1,0:T(8,128)(2,1)}) %all-gather.2.cloned.1.call-update) | async-done | bytes 1572880 | tf_op jit(solution)/shard_map/all_gather | solution.py:25
  71.0 0.0 copy-start.4
  71.0 4.8 %fusion.4 = f32[192,768]{1,0:T(8,128)S(1)} fusion(bf16[192,4096]{1,0:T(8,128)(2,1)} %all-gather.2.cloned.1.call-done, bf16[1,4096,768]{2,1,0:T(8,128)(2,1)} %param.13), kind=kOutput, calls=%fused_computation.6 | convolution fusion | flops 1207959552 | bytes 8454144 | tf_op jit(solution)/shard_map/dot_general | solution.py:26
  75.8 0.0 copy-done.4
  75.8 9.3 %fusion.9 = bf16[4096,192]{0,1:T(8,128)(2,1)} fusion(bf16[1,768,4096]{2,1,0:T(8,128)(2,1)} %param.15, bf16[192,4096]{1,0:T(8,128)(2,1)S(1)} %copy-done.4, bf16[1,4096,768]{2,1,0:T(8,128)(2,1)} %param.14, f32[192,768]{1,0:T(8,128)S(1)} %fusion.4), kind=kOutput, calls=%fused_computation.9 | convolution fusion | flops 2417590272 | bytes 16318464 | tf_op jit(solution)/shard_map/dot_general | solution.py:31
  85.0 0.0 copy-start.1
  85.0 0.0 copy-start.3
  85.0 0.0 reduce-scatter.2.cloned.1.call-update
  85.1 34.4 %reduce-scatter.2.cloned.1.call-done = bf16[1024,192]{0,1:T(8,128)(2,1)} async-done(((bf16[4096,192]{0,1:T(8,128)(2,1)}), bf16[1024,192]{0,1:T(8,128)(2,1)}) %reduce-scatter.2.cloned.1.call-update) | async-done | bytes 393232 | tf_op jit(solution)/shard_map/reduce_scatter | solution.py:30
  119.5 3.5 %all-to-all-start.1 = ((bf16[1024,4,48]{0,2,1:T(8,128)(2,1)}), bf16[1024,4,48]{0,2,1:T(8,128)(2,1)S(1)}, u32[]{:S(2)}, u32[]{:S(2)}) async-start(bf16[1024,4,48]{0,2,1:T(8,128)(2,1)} %bitcast.48), calls=%async_computation.2 | async-start | bytes 786432 | tf_op jit(solution)/shard_map/all_to_all | solution.py:39
  123.0 0.0 copy-done.1
  123.0 0.0 copy-start
  123.0 0.1 reshape_squeeze.3
  123.1 7.3 %all-to-all-done.1 = bf16[1024,4,48]{0,2,1:T(8,128)(2,1)S(1)} async-done(((bf16[1024,4,48]{0,2,1:T(8,128)(2,1)}), bf16[1024,4,48]{0,2,1:T(8,128)(2,1)S(1)}, u32[]{:S(2)}, u32[]{:S(2)}) %all-to-all-start.1) | async-done | bytes 393248 | tf_op jit(solution)/shard_map/all_to_all | solution.py:39
  130.3 0.0 copy-done.3
  130.3 0.1 convert_multiply_fusion.2
  130.5 2.5 %scatter_custom_fusion = f32[1024,384]{0,1:T(8,128)S(1)} fusion(s32[192]{0:T(256)S(1)} %bitcast.50, f32[192,1024]{1,0:T(8,128)S(1)} %bitcast.47, f32[]{:T(128)} %constant.11.clone.1), kind=kCustom, calls=%fused_computation.21 | custom fusion | flops 196608 | bytes 1572868 | tf_op jit(solution)/shard_map/scatter-add | solution.py:45
  133.0 0.0 copy-done
  133.0 0.0 copy-start.2
  133.0 0.3 multiply_reduce_fusion
  133.3 9.6 %psum.15 = f32[384]{0:T(512)S(1)} all-reduce(f32[384]{0:T(512)S(1)} %multiply_reduce_fusion), channel_id=1, replica_groups=mesh['grp'=2,'ep'=4,'tp'=4] {'tp'}, use_global_device_ids=true, to_apply=%region_5.6 | all-reduce | flops 384 | bytes 3072 | tf_op jit(solution)/shard_map/psum | solution.py:48
  142.9 0.0 copy-done.2
  142.9 1.1 multiply_convert_fusion
  (4 shorter events, 0.0 us)
Async XLA Ops:
  6.5 64.5 %all-gather.2.cloned.1.call-start = ((), (), s32[]{:S(2)}) async-start(), calls=%async_computation.3 | async-start | bytes 1966080 | tf_op jit(solution)/shard_map/all_gather | solution.py:25
  36.6 82.9 %reduce-scatter.2.cloned.1.call-start = ((), (), s32[]{:S(2)}) async-start(), calls=%async_computation.4 | async-start | bytes 1966080 | tf_op jit(solution)/shard_map/reduce_scatter | solution.py:30
  71.0 4.8 %copy-start.4 = (bf16[192,4096]{1,0:T(8,128)(2,1)S(1)}, bf16[192,4096]{1,0:T(8,128)(2,1)}, u32[]{:S(2)}) copy-start(bf16[192,4096]{1,0:T(8,128)(2,1)} %all-gather.2.cloned.1.call-done) | copy-start | bytes 4718596
  85.0 37.9 %copy-start.1 = (s32[1,4,48]{2,1,0:T(4,128)S(1)}, s32[1,4,48]{2,1,0:T(4,128)}, u32[]{:S(2)}) copy-start(s32[1,4,48]{2,1,0:T(4,128)} %param.11) | copy-start | bytes 2308
  85.0 45.3 %copy-start.3 = (f32[1,4,48]{2,1,0:T(4,128)S(1)}, f32[1,4,48]{2,1,0:T(4,128)}, u32[]{:S(2)}) copy-start(f32[1,4,48]{2,1,0:T(4,128)} %param.12) | copy-start | bytes 2308
  119.5 10.8 %all-to-all-start.1 = ((bf16[1024,4,48]{0,2,1:T(8,128)(2,1)}), bf16[1024,4,48]{0,2,1:T(8,128)(2,1)S(1)}, u32[]{:S(2)}, u32[]{:S(2)}) async-start(bf16[1024,4,48]{0,2,1:T(8,128)(2,1)} %bitcast.48), calls=%async_computation.2 | async-start | bytes 786432 | tf_op jit(solution)/shard_map/all_to_all | solution.py:39
  123.0 10.0 %copy-start = (bf16[384,1024]{1,0:T(8,128)(2,1)S(1)}, bf16[384,1024]{1,0:T(8,128)(2,1)}, u32[]{:S(2)}) copy-start(bf16[384,1024]{1,0:T(8,128)(2,1)} %param.8) | copy-start | bytes 2359300
  133.0 9.9 %copy-start.2 = (f32[1024]{0:T(1024)S(1)}, f32[1024]{0:T(1024)}, u32[]{:S(2)}) copy-start(f32[1024]{0:T(1024)} %param.10) | copy-start | bytes 12292
Sparse Core Ops, SparseCore 0:
  36.7 34.2 all-gather.1
  85.2 34.2 reduce-scatter.1
where the time goes:
time: 151 us
  waiting for transfers between devices  76.1 us (50%)
  blocking collectives  33.6 us (22%)
  matrix products  14 us (9%)
  between operations  13.5 us (9%)
  other arithmetic  8.29 us (5%)
  starting transfers between devices  3.5 us (2%)
  local copies, waits for them, and re-layouts  1.9 us (1%)
    reduce_scatter x1, waiting for transfers between devices, shards(): lax.psum_scatter(lax.dot_general(down_shard, hidden, (((0,), (1,)), ((),...  34.4 us
    all_gather x1, waiting for transfers between devices, shards(): lax.all_gather(incoming.reshape(-1, shard_width), 'tp', axis=1, tiled=True)  34.4 us
    psum x1, blocking collectives, shards(): square_sum = lax.psum(jnp.sum(resident * resident, axis=1), 'tp')  13.5 us
    all_to_all x1, blocking collectives, shards(): lax.all_to_all(outgoing, 'ep', split_axis=0, concat_axis=0, tiled=True)  10.5 us
    psum x1, blocking collectives, shards(): out_sum = lax.psum(jnp.sum(mixed_rows * mixed_rows, axis=1), 'tp')  9.64 us
    dot_general x1, matrix products, shards(): lax.dot_general(down_shard, hidden, (((0,), (1,)), ((), ())), preferred_e...  9.25 us
    all_to_all x1, waiting for transfers between devices, shards(): lax.all_to_all(expert_out, 'ep', split_axis=1, concat_axis=1, tiled=True)  7.26 us
    dot_general x1, matrix products, shards(): jnp.dot(picked_rows, expert_gate[0], preferred_element_type=jnp.float32)  4.76 us
  transfers between devices with their start and end apart: 3, of which 3 were waited for; matrix products, arithmetic and copies ran while one was open for 0% of the time, Pallas kernels for 0%

commit v1 on v0

v1 whole, which is shorter than its diff:
```python
import jax
import jax.numpy as jnp
from jax import lax
from jax.sharding import PartitionSpec as P

NORM_EPS = 1e-06
PRESCALE = 2.0 ** -20


def shift(value, axis, n, step):
    return lax.ppermute(value, axis, [(i, (i + step) % n) for i in range(n)])


def ring_gather(own, axis, n):
    half = own.shape[0] // 2
    forward, backward = own, own
    for d in range(1, n // 2 + 1):
        if 2 * d == n:
            forward = shift(forward[:half], axis, n, 1)
            backward = shift(backward[half:], axis, n, -1)
            yield d, jnp.concatenate([forward, backward], axis=0)
        else:
            forward = shift(forward, axis, n, 1)
            backward = shift(backward, axis, n, -1)
            yield -d, forward
            yield d, backward


def ring_scatter(part, axis, n, rows):
    half = rows // 2

    def add(full, extra, low):
        if extra is None:
            return full
        extra = extra.astype(jnp.float32)
        if extra.shape[0] == rows:
            return full + extra
        if low:
            return jnp.concatenate([full[:half] + extra, full[half:]], axis=0)
        return jnp.concatenate([full[:half], full[half:] + extra], axis=0)

    forward, backward = None, None
    for d in range(n // 2, 0, -1):
        if 2 * d == n:
            whole = part(d).astype(jnp.bfloat16)
            forward = shift(whole[:half], axis, n, 1)
            backward = shift(whole[half:], axis, n, -1)
        else:
            ahead = add(part(d), forward, True).astype(jnp.bfloat16)
            behind = add(part(-d), backward, False).astype(jnp.bfloat16)
            forward = shift(ahead, axis, n, 1)
            backward = shift(behind, axis, n, -1)
    return add(add(part(0), forward, True), backward, False)


def shards(tokens, pre_gain, out_gain, chosen, route_weight, expert_gate, expert_up, expert_down, n_ep, n_tp):
    model_width = pre_gain.shape[0]
    tok_count, shard_width = tokens.shape
    slot_count = chosen.shape[2]
    here_ep = lax.axis_index("ep")
    here_tp = lax.axis_index("tp")
    bf16, f32 = jnp.bfloat16, jnp.float32

    def relative(table):
        return lax.dynamic_slice_in_dim(jnp.concatenate([table, table], axis=0), here_ep, n_ep, 0)

    slots = relative(chosen[0]).reshape(-1)
    weights = relative(route_weight[0]).reshape(-1)
    token_ids = lax.broadcasted_iota(jnp.int32, (tok_count, slots.shape[0]), 0)
    hit = token_ids == slots[None, :]
    select = hit.astype(bf16)

    picked = lax.dot_general(
        select, tokens, (((0,), (0,)), ((), ())), preferred_element_type=f32
    ).astype(bf16)
    received = [picked[:slot_count]]
    for s in range(1, n_ep):
        received.append(shift(picked[s * slot_count:(s + 1) * slot_count], "ep", n_ep, s))
    rows = jnp.concatenate(received, axis=0)

    gate_matrix, up_matrix, down_matrix = expert_gate[0], expert_up[0], expert_down[0]

    def start_of(offset):
        return ((here_tp + offset) % n_tp) * shard_width

    def chunk(offset, block):
        start = start_of(offset)
        gain = lax.dynamic_slice_in_dim(pre_gain, start, shard_width, 0) * PRESCALE
        wide = block.astype(f32)
        squares = jnp.sum(wide * wide, axis=1)
        scaled = (wide * gain).astype(bf16)
        gate_rows = lax.dynamic_slice_in_dim(gate_matrix, start, shard_width, 0)
        up_rows = lax.dynamic_slice_in_dim(up_matrix, start, shard_width, 0)
        return (
            squares,
            jnp.dot(scaled, gate_rows, preferred_element_type=f32),
            jnp.dot(scaled, up_rows, preferred_element_type=f32),
        )

    square_sum, gate_act, up_act = chunk(0, rows)
    for offset, block in ring_gather(rows, "tp", n_tp):
        more = chunk(offset, block)
        square_sum, gate_act, up_act = square_sum + more[0], gate_act + more[1], up_act + more[2]
    row_scale = (lax.rsqrt(square_sum / model_width + NORM_EPS) / PRESCALE)[:, None]
    hidden = (jax.nn.silu(gate_act * row_scale) * (up_act * row_scale)).astype(bf16)

    def part(offset):
        columns = lax.dynamic_slice_in_dim(down_matrix, start_of(offset), shard_width, 1)
        return jnp.dot(hidden, columns, preferred_element_type=f32)

    expert_out = ring_scatter(part, "tp", n_tp, rows.shape[0]).astype(bf16)

    returned = [expert_out[:slot_count]]
    for s in range(1, n_ep):
        returned.append(shift(expert_out[s * slot_count:(s + 1) * slot_count], "ep", n_ep, -s))
    back = jnp.concatenate(returned, axis=0)

    spread = jnp.where(hit, weights[None, :], 0.0)
    coarse = spread.astype(bf16)
    fine = (spread - coarse.astype(f32)).astype(bf16)
    mixed = (
        tokens.astype(f32)
        + jnp.dot(coarse, back, preferred_element_type=f32)
        + jnp.dot(fine, back, preferred_element_type=f32)
    )
    own_sum = jnp.sum(mixed * mixed, axis=1)
    out_sum = own_sum
    for s in range(1, n_tp):
        out_sum = out_sum + shift(own_sum, "tp", n_tp, s)
    out_scale = lax.rsqrt(out_sum / model_width + NORM_EPS)[:, None]
    return (mixed * out_scale * out_gain).astype(bf16)


def solution(mesh):
    def body(*args):
        return shards(*args, n_ep=mesh.shape["ep"], n_tp=mesh.shape["tp"])

    return jax.shard_map(
        body,
        mesh=mesh,
        in_specs=(
            P(("grp", "ep"), "tp"),
            P(),
            P("tp"),
            P(("grp", "ep"), None, None),
            P(("grp", "ep"), None, None),
            P("ep", None, "tp"),
            P("ep", None, "tp"),
            P("ep", "tp", None),
        ),
        out_specs=P(("grp", "ep"), "tp"),
        check_vma=False,
    )
```

time: 151 us -> 91.1 us (0.60)
  blocking collectives: 33.6 us -> 0 us
  waiting for transfers between devices: 76.1 us -> 47.8 us
  starting transfers between devices: 3.5 us -> 25 us
  between operations: 13.5 us -> 0.31 us
  other arithmetic: 8.29 us -> 2.95 us
    ppermute x0 -> x17, waiting for transfers between devices: none -> 47.8 us  [shift(): return lax.ppermute(value, axis, [(i, (i + step) % n) for i in range(n)])]
    reduce_scatter x1 -> x0, waiting for transfers between devices: 34.4 us -> none  [shards(): lax.psum_scatter(lax.dot_general(down_shard, hidden, (((0,), (1,)), ((),...]
    all_gather x1 -> x0, waiting for transfers between devices: 34.4 us -> none  [shards(): lax.all_gather(incoming.reshape(-1, shard_width), 'tp', axis=1, tiled=True)]
    ppermute x0 -> x17, starting transfers between devices: none -> 25 us  [shift(): return lax.ppermute(value, axis, [(i, (i + step) % n) for i in range(n)])]
    psum x2 -> x0, blocking collectives: 23.1 us -> none  [the longest x1 13.5 us: shards(): square_sum = lax.psum(jnp.sum(resident * resident, axis=1), 'tp')]
    all_to_all x1 -> x0, blocking collectives: 10.5 us -> none  [shards(): lax.all_to_all(outgoing, 'ep', split_axis=0, concat_axis=0, tiled=True)]
    all_to_all x1 -> x0, waiting for transfers between devices: 7.26 us -> none  [shards(): lax.all_to_all(expert_out, 'ep', split_axis=1, concat_axis=1, tiled=True)]
    all_to_all x1 -> x0, starting transfers between devices: 3.46 us -> none  [shards(): lax.all_to_all(expert_out, 'ep', split_axis=1, concat_axis=1, tiled=True)]
  transfers between devices with their start and end apart: 3 -> 17, of which waited for: 3 -> 15; matrix products, arithmetic and copies ran while one was open for 0% -> 9% of each run, Pallas kernels for 0% -> 0%
where the time goes in v1:
time: 91.1 us; the launch traced here: 90.9 us
  waiting for transfers between devices  47.8 us (52%)
  starting transfers between devices  25 us (27%)
  matrix products  13.1 us (14%)
  other arithmetic  2.95 us (3%)
  local copies, waits for them, and re-layouts  1.73 us (2%)
    ppermute x17, waiting for transfers between devices, shift(): return lax.ppermute(value, axis, [(i, (i + step) % n) for i in range(n)])  47.8 us
    ppermute x17, starting transfers between devices, shift(): return lax.ppermute(value, axis, [(i, (i + step) % n) for i in range(n)])  25 us
    dot_general x4, matrix products, chunk(): jnp.dot(scaled, up_rows, preferred_element_type=f32)  5.12 us
    dot_general x4, matrix products, chunk(): jnp.dot(scaled, gate_rows, preferred_element_type=f32)  3.51 us
    dot_general x4, matrix products, part(): return jnp.dot(hidden, columns, preferred_element_type=f32)  1.92 us
  transfers between devices with their start and end apart: 17, of which 15 were waited for; matrix products, arithmetic and copies ran while one was open for 9% of the time, Pallas kernels for 0%

profile of v1, /device:TPU:0, one launch (start us, length us, event | category | flops | bytes accessed | tf_op | source)
XLA Modules:
  0.0 90.9 jit_solution(13254459956955016609)
XLA Ops:
  0.0 0.8 pad_add_fusion
  0.9 1.7 %convolution_convert_fusion = bf16[192,1024]{1,0:T(8,128)(2,1)S(1)} fusion(bf16[384,1024]{1,0:T(8,128)(2,1)} %param.8, s32[192]{0:T(256)S(1)} %eq.19), kind=kOutput, calls=%fused_computation.49 | convolution fusion | flops 151265280 | bytes 1180416 | tf_op jit(solution)/shard_map/dot_general | solution.py:73
  2.6 0.5 collective-permute-start
  3.2 2.6 %collective-permute-start.1 = (bf16[48,1024]{1,0:T(8,128)(2,1)S(1)}, bf16[48,1024]{1,0:T(8,128)(2,1)S(1)}, u32[]{:S(2)}, u32[]{:S(2)}) collective-permute-start(bf16[48,1024]{1,0:T(8,128)(2,1)S(1)} %get-tuple-element.15), channel_id=1, source_target_pairs={{0,8},{4,12},{8,0},{12,4},{1,9},{5,13},{9,1},{13,5},{2,10},{6,14},... | collective-permute-start | bytes 294920 | tf_op jit(solution)/shard_map/ppermute | solution.py:11
  5.7 1.4 %collective-permute-start.2 = (bf16[48,1024]{1,0:T(8,128)(2,1)S(1)}, bf16[48,1024]{1,0:T(8,128)(2,1)S(1)}, u32[]{:S(2)}, u32[]{:S(2)}) collective-permute-start(bf16[48,1024]{1,0:T(8,128)(2,1)S(1)} %get-tuple-element.14), channel_id=1, source_target_pairs={{0,12},{4,0},{8,4},{12,8},{1,13},{5,1},{9,5},{13,9},{2,14},{6,2},{... | collective-permute-start | bytes 294920 | tf_op jit(solution)/shard_map/ppermute | solution.py:11
  7.1 0.4 collective-permute-done
  7.5 1.4 %collective-permute-done.1 = bf16[48,1024]{1,0:T(8,128)(2,1)S(1)} collective-permute-done((bf16[48,1024]{1,0:T(8,128)(2,1)S(1)}, bf16[48,1024]{1,0:T(8,128)(2,1)S(1)}, u32[]{:S(2)}, u32[]{:S(2)}) %collective-permute-start.1) | collective-permute-done | bytes 98336 | tf_op jit(solution)/shard_map/ppermute | solution.py:11
  8.9 1.5 %collective-permute-done.2 = bf16[48,1024]{1,0:T(8,128)(2,1)S(1)} collective-permute-done((bf16[48,1024]{1,0:T(8,128)(2,1)S(1)}, bf16[48,1024]{1,0:T(8,128)(2,1)S(1)}, u32[]{:S(2)}, u32[]{:S(2)}) %collective-permute-start.2) | collective-permute-done | bytes 98336 | tf_op jit(solution)/shard_map/ppermute | solution.py:11
  10.5 1.6 %collective-permute-start.3 = (bf16[192,1024]{1,0:T(8,128)(2,1)S(1)}, bf16[192,1024]{1,0:T(8,128)(2,1)S(1)}, u32[]{:S(2)}, u32[]{:S(2)}) collective-permute-start(bf16[192,1024]{1,0:T(8,128)(2,1)S(1)} %get-tuple-element.6), channel_id=1, source_target_pairs={{0,1},{1,2},{2,3},{3,0},{4,5},{5,6},{6,7},{7,4},{8,9},{9,10},{10,1... | collective-permute-start | bytes 1179656 | tf_op jit(solution)/shard_map/ppermute | solution.py:11
  12.2 2.2 %collective-permute-start.4 = (bf16[192,1024]{1,0:T(8,128)(2,1)S(1)}, bf16[192,1024]{1,0:T(8,128)(2,1)S(1)}, u32[]{:S(2)}, u32[]{:S(2)}) collective-permute-start(bf16[192,1024]{1,0:T(8,128)(2,1)S(1)} %get-tuple-element.6), channel_id=1, source_target_pairs={{0,3},{1,0},{2,1},{3,2},{4,7},{5,4},{6,5},{7,6},{8,11},{9,8},{10,9... | collective-permute-start | bytes 1179656 | tf_op jit(solution)/shard_map/ppermute | solution.py:11
  14.4 2.0 %fusion.22 = f32[192,768]{1,0:T(8,128)S(1)} fusion(bf16[1,4096,768]{2,1,0:T(8,128)(2,1)} %param.13, s32[]{:T(128)S(6)} %select_n.62, bf16[192,1024]{1,0:T(8,128)(2,1)S(1)} %get-tuple-element.6, f32[1024]{0:T(1024)S(1)} %get-tuple-element.18), kind=kOutput, calls=%fused_computation.22 | convolution fusion | flops 302579712 | bytes 2560004 | tf_op jit(solution)/shard_map/dot_general | solution.py:96
  16.4 2.1 %fusion.14 = f32[192,768]{1,0:T(8,128)S(1)} fusion(bf16[1,4096,768]{2,1,0:T(8,128)(2,1)} %param.14, s32[]{:T(128)S(6)} %select_n.62, bf16[192,1024]{1,0:T(8,128)(2,1)S(1)} %get-tuple-element.6, f32[1024]{0:T(1024)S(1)} %get-tuple-element.18), kind=kOutput, calls=%fused_computation.14 | convolution fusion | flops 302579712 | bytes 2560004 | tf_op jit(solution)/shard_map/dot_general | solution.py:97
  18.6 5.8 %collective-permute-done.3 = bf16[192,1024]{1,0:T(8,128)(2,1)S(1)} collective-permute-done((bf16[192,1024]{1,0:T(8,128)(2,1)S(1)}, bf16[192,1024]{1,0:T(8,128)(2,1)S(1)}, u32[]{:S(2)}, u32[]{:S(2)}) %collective-permute-start.3) | collective-permute-done | bytes 393248 | tf_op jit(solution)/shard_map/ppermute | solution.py:11
  24.5 7.6 %collective-permute-done.4 = bf16[192,1024]{1,0:T(8,128)(2,1)S(1)} collective-permute-done((bf16[192,1024]{1,0:T(8,128)(2,1)S(1)}, bf16[192,1024]{1,0:T(8,128)(2,1)S(1)}, u32[]{:S(2)}, u32[]{:S(2)}) %collective-permute-start.4) | collective-permute-done | bytes 393248 | tf_op jit(solution)/shard_map/ppermute | solution.py:11
  32.1 2.6 %collective-permute-start.6 = (bf16[96,1024]{1,0:T(8,128)(2,1)S(1)}, bf16[96,1024]{1,0:T(8,128)(2,1)S(1)}, u32[]{:S(2)}, u32[]{:S(2)}) collective-permute-start(bf16[96,1024]{1,0:T(8,128)(2,1)S(1)} %slice.71), channel_id=1, source_target_pairs={{0,3},{1,0},{2,1},{3,2},{4,7},{5,4},{6,5},{7,6},{8,11},{9,8},{10,9... | collective-permute-start | bytes 589832 | tf_op jit(solution)/shard_map/ppermute | solution.py:11
  35.0 0.5 fusion.18
  35.5 1.9 %fusion.10 = f32[192,768]{1,0:T(8,128)S(1)} fusion(bf16[1,4096,768]{2,1,0:T(8,128)(2,1)} %param.14, s32[]{:T(128)S(6)} %select_n.66, bf16[192,1024]{1,0:T(8,128)(2,1)S(1)} %collective-permute-done.4, f32[1024]{0:T(1024)S(1)} %get-tuple-element.20), kind=kOutput, calls=%fused_computation.10 | convolution fusion | flops 302579712 | bytes 2560004 | tf_op jit(solution)/shard_map/dot_general | solution.py:97
  37.4 2.3 %collective-permute-done.5 = bf16[96,1024]{1,0:T(8,128)(2,1)S(1)} collective-permute-done((bf16[96,1024]{1,0:T(8,128)(2,1)S(1)}, bf16[96,1024]{1,0:T(8,128)(2,1)S(1)}, u32[]{:S(2)}, u32[]{:S(2)}) %collective-permute-start.5) | collective-permute-done | bytes 196640 | tf_op jit(solution)/shard_map/ppermute | solution.py:11
  39.7 1.4 %collective-permute-done.6 = bf16[96,1024]{1,0:T(8,128)(2,1)S(1)} collective-permute-done((bf16[96,1024]{1,0:T(8,128)(2,1)S(1)}, bf16[96,1024]{1,0:T(8,128)(2,1)S(1)}, u32[]{:S(2)}, u32[]{:S(2)}) %collective-permute-start.6) | collective-permute-done | bytes 196640 | tf_op jit(solution)/shard_map/ppermute | solution.py:11
  41.3 0.5 fusion.16
  41.9 0.5 fusion.8
  42.4 0.5 fusion.60
  42.9 0.6 fusion.66
  43.5 0.5 slice-done
  44.0 0.8 slice-done.1
  44.8 0.5 fusion.63
  45.3 0.5 fusion.4
  45.9 1.3 %collective-permute-start.7 = (bf16[96,1024]{1,0:T(8,128)(2,1)S(1)}, bf16[96,1024]{1,0:T(8,128)(2,1)S(1)}, u32[]{:S(2)}, u32[]{:S(2)}) collective-permute-start(bf16[96,1024]{1,0:T(8,128)(2,1)S(1)} %get-tuple-element.11), channel_id=1, source_target_pairs={{0,1},{1,2},{2,3},{3,0},{4,5},{5,6},{6,7},{7,4},{8,9},{9,10},{10,1... | collective-permute-start | bytes 589832 | tf_op jit(solution)/shard_map/ppermute | solution.py:11
  47.1 2.7 %collective-permute-start.9 = (bf16[96,1024]{1,0:T(8,128)(2,1)S(1)}, bf16[96,1024]{1,0:T(8,128)(2,1)S(1)}, u32[]{:S(2)}, u32[]{:S(2)}) collective-permute-start(bf16[96,1024]{1,0:T(8,128)(2,1)S(1)} %get-tuple-element.12), channel_id=1, source_target_pairs={{0,3},{1,0},{2,1},{3,2},{4,7},{5,4},{6,5},{7,6},{8,11},{9,8},{10,9... | collective-permute-start | bytes 589832 | tf_op jit(solution)/shard_map/ppermute | solution.py:11
  49.8 0.5 fusion
  50.3 5.1 %collective-permute-done.7 = bf16[96,1024]{1,0:T(8,128)(2,1)S(1)} collective-permute-done((bf16[96,1024]{1,0:T(8,128)(2,1)S(1)}, bf16[96,1024]{1,0:T(8,128)(2,1)S(1)}, u32[]{:S(2)}, u32[]{:S(2)}) %collective-permute-start.7) | collective-permute-done | bytes 196640 | tf_op jit(solution)/shard_map/ppermute | solution.py:11
  55.6 1.6 %collective-permute-done.9 = bf16[96,1024]{1,0:T(8,128)(2,1)S(1)} collective-permute-done((bf16[96,1024]{1,0:T(8,128)(2,1)S(1)}, bf16[96,1024]{1,0:T(8,128)(2,1)S(1)}, u32[]{:S(2)}, u32[]{:S(2)}) %collective-permute-start.9) | collective-permute-done | bytes 196640 | tf_op jit(solution)/shard_map/ppermute | solution.py:11
  57.3 3.4 %collective-permute-start.10 = (bf16[192,1024]{1,0:T(8,128)(2,1)S(1)}, bf16[192,1024]{1,0:T(8,128)(2,1)S(1)}, u32[]{:S(2)}, u32[]{:S(2)}) collective-permute-start(bf16[192,1024]{1,0:T(8,128)(2,1)S(1)} %pad_maximum_fusion.3), channel_id=1, source_target_pairs={{0,3},{1,0},{2,1},{3,2},{4,7},{5,4},{6,5},{7,6},{8,11},{9,8},{10,9... | collective-permute-start | bytes 1179656 | tf_op jit(solution)/shard_map/ppermute | solution.py:11
  60.7 0.5 fusion.6
  61.2 9.0 %collective-permute-done.8 = bf16[192,1024]{1,0:T(8,128)(2,1)S(1)} collective-permute-done((bf16[192,1024]{1,0:T(8,128)(2,1)S(1)}, bf16[192,1024]{1,0:T(8,128)(2,1)S(1)}, u32[]{:S(2)}, u32[]{:S(2)}) %collective-permute-start.8) | collective-permute-done | bytes 393248 | tf_op jit(solution)/shard_map/ppermute | solution.py:11
  70.2 4.3 %collective-permute-done.10 = bf16[192,1024]{1,0:T(8,128)(2,1)S(1)} collective-permute-done((bf16[192,1024]{1,0:T(8,128)(2,1)S(1)}, bf16[192,1024]{1,0:T(8,128)(2,1)S(1)}, u32[]{:S(2)}, u32[]{:S(2)}) %collective-permute-start.10) | collective-permute-done | bytes 393248 | tf_op jit(solution)/shard_map/ppermute | solution.py:11
  74.7 2.0 %collective-permute-start.11 = (bf16[48,1024]{1,0:T(8,128)(2,1)S(1)}, bf16[48,1024]{1,0:T(8,128)(2,1)S(1)}, u32[]{:S(2)}, u32[]{:S(2)}) collective-permute-start(bf16[48,1024]{1,0:T(8,128)(2,1)S(1)} %get-tuple-element.10), channel_id=1, source_target_pairs={{0,12},{4,0},{8,4},{12,8},{1,13},{5,1},{9,5},{13,9},{2,14},{6,2},{... | collective-permute-start | bytes 294920 | tf_op jit(solution)/shard_map/ppermute | solution.py:11
  76.7 0.5 collective-permute-start.12
  77.5 2.4 %collective-permute-done.11 = bf16[48,1024]{1,0:T(8,128)(2,1)S(1)} collective-permute-done((bf16[48,1024]{1,0:T(8,128)(2,1)S(1)}, bf16[48,1024]{1,0:T(8,128)(2,1)S(1)}, u32[]{:S(2)}, u32[]{:S(2)}) %collective-permute-start.11) | collective-permute-done | bytes 98336 | tf_op jit(solution)/shard_map/ppermute | solution.py:11
  79.9 2.8 %collective-permute-done.12 = bf16[48,1024]{1,0:T(8,128)(2,1)S(1)} collective-permute-done((bf16[48,1024]{1,0:T(8,128)(2,1)S(1)}, bf16[48,1024]{1,0:T(8,128)(2,1)S(1)}, u32[]{:S(2)}, u32[]{:S(2)}) %collective-permute-start.12) | collective-permute-done | bytes 98336 | tf_op jit(solution)/shard_map/ppermute | solution.py:11
  82.8 0.4 fusion.88
  83.2 0.5 multiply_reduce_fusion
  83.7 0.7 collective-permute-start.14
  84.4 1.1 %collective-permute-start.15 = (f32[384]{0:T(512)S(1)}, f32[384]{0:T(512)S(1)}, u32[]{:S(2)}, u32[]{:S(2)}) collective-permute-start(f32[384]{0:T(512)S(1)} %get-tuple-element.21), channel_id=1, source_target_pairs={{0,2},{1,3},{2,0},{3,1},{4,6},{5,7},{6,4},{7,5},{8,10},{9,11},{10,... | collective-permute-start | bytes 4616 | tf_op jit(solution)/shard_map/ppermute | solution.py:11
  85.5 2.1 %collective-permute-start.16 = (f32[384]{0:T(512)S(1)}, f32[384]{0:T(512)S(1)}, u32[]{:S(2)}, u32[]{:S(2)}) collective-permute-start(f32[384]{0:T(512)S(1)} %get-tuple-element.21), channel_id=1, source_target_pairs={{0,3},{1,0},{2,1},{3,2},{4,7},{5,4},{6,5},{7,6},{8,11},{9,8},{10,9... | collective-permute-start | bytes 4616 | tf_op jit(solution)/shard_map/ppermute | solution.py:11
  87.5 1.6 %collective-permute-done.14 = f32[384]{0:T(512)S(1)} collective-permute-done((f32[384]{0:T(512)S(1)}, f32[384]{0:T(512)S(1)}, u32[]{:S(2)}, u32[]{:S(2)}) %collective-permute-start.14) | collective-permute-done | bytes 1568 | tf_op jit(solution)/shard_map/ppermute | solution.py:11
  89.1 0.6 collective-permute-done.16
  89.7 1.2 %multiply_convert_fusion = bf16[384,1024]{1,0:T(8,128)(2,1)} fusion(f32[1024]{0:T(1024)S(1)} %copy-done.3, f32[384]{0:T(512)S(1)} %add_rsqrt_fusion, f32[384,1024]{1,0:T(8,128)S(1)} %get-tuple-element.22, f32[384,1024]{1,0:T(8,128)S(1)} %fusion.88, bf16[384,1024]{1,0:T(8,128)(2,1)S(1)} %copy-done), kind=kLoop, calls=%fused_computation.24 | loop fusion | flops 2359296 | bytes 4724224 | tf_op jit(solution)/shard_map/convert_element_type | solution.py:131
  (47 shorter events, 1.6 us)
Async XLA Ops:
  0.0 7.1 %copy-start.2 = (f32[4096]{0:T(1024)S(1)}, f32[4096]{0:T(1024)}, u32[]{:S(2)}) copy-start(f32[4096]{0:T(1024)} %param.9) | copy-start | bytes 49156
  0.9 41.0 %slice-start.2 = ((s8[6291456]{0:T(1024)(128)(4,1)}), s8[2097152]{0:T(1024)(128)(4,1)S(1)}, s32[]{:S(2)}) async-start(s8[6291456]{0:T(1024)(128)(4,1)} %bitcast.67), calls=%async_computation.2 | async-start | bytes 4194304
  2.6 4.9 %collective-permute-start = (bf16[48,1024]{1,0:T(8,128)(2,1)S(1)}, bf16[48,1024]{1,0:T(8,128)(2,1)S(1)}, u32[]{:S(2)}, u32[]{:S(2)}) collective-permute-start(bf16[48,1024]{1,0:T(8,128)(2,1)S(1)} %get-tuple-element.16), channel_id=1, source_target_pairs={{0,4},{4,8},{8,12},{12,0},{1,5},{5,9},{9,13},{13,1},{2,6},{6,10},{... | collective-permute-start | bytes 294920 | tf_op jit(solution)/shard_map/ppermute | solution.py:11
  3.2 5.8 %collective-permute-start.1 = (bf16[48,1024]{1,0:T(8,128)(2,1)S(1)}, bf16[48,1024]{1,0:T(8,128)(2,1)S(1)}, u32[]{:S(2)}, u32[]{:S(2)}) collective-permute-start(bf16[48,1024]{1,0:T(8,128)(2,1)S(1)} %get-tuple-element.15), channel_id=1, source_target_pairs={{0,8},{4,12},{8,0},{12,4},{1,9},{5,13},{9,1},{13,5},{2,10},{6,14},... | collective-permute-start | bytes 294920 | tf_op jit(solution)/shard_map/ppermute | solution.py:11
  5.7 4.6 %collective-permute-start.2 = (bf16[48,1024]{1,0:T(8,128)(2,1)S(1)}, bf16[48,1024]{1,0:T(8,128)(2,1)S(1)}, u32[]{:S(2)}, u32[]{:S(2)}) collective-permute-start(bf16[48,1024]{1,0:T(8,128)(2,1)S(1)} %get-tuple-element.14), channel_id=1, source_target_pairs={{0,12},{4,0},{8,4},{12,8},{1,13},{5,1},{9,5},{13,9},{2,14},{6,2},{... | collective-permute-start | bytes 294920 | tf_op jit(solution)/shard_map/ppermute | solution.py:11
  10.5 13.9 %collective-permute-start.3 = (bf16[192,1024]{1,0:T(8,128)(2,1)S(1)}, bf16[192,1024]{1,0:T(8,128)(2,1)S(1)}, u32[]{:S(2)}, u32[]{:S(2)}) collective-permute-start(bf16[192,1024]{1,0:T(8,128)(2,1)S(1)} %get-tuple-element.6), channel_id=1, source_target_pairs={{0,1},{1,2},{2,3},{3,0},{4,5},{5,6},{6,7},{7,4},{8,9},{9,10},{10,1... | collective-permute-start | bytes 1179656 | tf_op jit(solution)/shard_map/ppermute | solution.py:11
  12.2 19.9 %collective-permute-start.4 = (bf16[192,1024]{1,0:T(8,128)(2,1)S(1)}, bf16[192,1024]{1,0:T(8,128)(2,1)S(1)}, u32[]{:S(2)}, u32[]{:S(2)}) collective-permute-start(bf16[192,1024]{1,0:T(8,128)(2,1)S(1)} %get-tuple-element.6), channel_id=1, source_target_pairs={{0,3},{1,0},{2,1},{3,2},{4,7},{5,4},{6,5},{7,6},{8,11},{9,8},{10,9... | collective-permute-start | bytes 1179656 | tf_op jit(solution)/shard_map/ppermute | solution.py:11
  14.4 20.6 %copy-start.1 = (bf16[1,4096,768]{2,1,0:T(8,128)(2,1)S(1)}, bf16[1,4096,768]{2,1,0:T(8,128)(2,1)}, u32[]{:S(2)}) copy-start(bf16[1,4096,768]{2,1,0:T(8,128)(2,1)} %param.13) | copy-start | bytes 18874372
  24.4 15.3 %collective-permute-start.5 = (bf16[96,1024]{1,0:T(8,128)(2,1)S(1)}, bf16[96,1024]{1,0:T(8,128)(2,1)S(1)}, u32[]{:S(2)}, u32[]{:S(2)}) collective-permute-start(bf16[96,1024]{1,0:T(8,128)(2,1)S(1)} %slice.70), channel_id=1, source_target_pairs={{0,1},{1,2},{2,3},{3,0},{4,5},{5,6},{6,7},{7,4},{8,9},{9,10},{10,1... | collective-permute-start | bytes 589832 | tf_op jit(solution)/shard_map/ppermute | solution.py:11
  32.1 9.7 %slice-start.3 = ((s8[6291456]{0:T(1024)(128)(4,1)}), s8[4194304]{0:T(1024)(128)(4,1)S(1)}, s32[]{:S(2)}) async-start(s8[6291456]{0:T(1024)(128)(4,1)} %bitcast.67), calls=%async_computation.3 | async-start | bytes 8388608
  32.1 9.0 %collective-permute-start.6 = (bf16[96,1024]{1,0:T(8,128)(2,1)S(1)}, bf16[96,1024]{1,0:T(8,128)(2,1)S(1)}, u32[]{:S(2)}, u32[]{:S(2)}) collective-permute-start(bf16[96,1024]{1,0:T(8,128)(2,1)S(1)} %slice.71), channel_id=1, source_target_pairs={{0,3},{1,0},{2,1},{3,2},{4,7},{5,4},{6,5},{7,6},{8,11},{9,8},{10,9... | collective-permute-start | bytes 589832 | tf_op jit(solution)/shard_map/ppermute | solution.py:11
  41.8 2.2 %slice-start = ((s8[6291456]{0:T(1024)(128)(4,1)}), s8[4194304]{0:T(1024)(128)(4,1)S(1)}, s32[]{:S(2)}) async-start(s8[6291456]{0:T(1024)(128)(4,1)} %bitcast.65), calls=%async_computation | async-start | bytes 8388608
  42.4 2.5 %slice-start.1 = ((s8[6291456]{0:T(1024)(128)(4,1)}), s8[2097152]{0:T(1024)(128)(4,1)S(1)}, s32[]{:S(2)}) async-start(s8[6291456]{0:T(1024)(128)(4,1)} %bitcast.65), calls=%async_computation.1 | async-start | bytes 4194304
  45.9 9.6 %collective-permute-start.7 = (bf16[96,1024]{1,0:T(8,128)(2,1)S(1)}, bf16[96,1024]{1,0:T(8,128)(2,1)S(1)}, u32[]{:S(2)}, u32[]{:S(2)}) collective-permute-start(bf16[96,1024]{1,0:T(8,128)(2,1)S(1)} %get-tuple-element.11), channel_id=1, source_target_pairs={{0,1},{1,2},{2,3},{3,0},{4,5},{5,6},{6,7},{7,4},{8,9},{9,10},{10,1... | collective-permute-start | bytes 589832 | tf_op jit(solution)/shard_map/ppermute | solution.py:11
  47.1 10.1 %collective-permute-start.9 = (bf16[96,1024]{1,0:T(8,128)(2,1)S(1)}, bf16[96,1024]{1,0:T(8,128)(2,1)S(1)}, u32[]{:S(2)}, u32[]{:S(2)}) collective-permute-start(bf16[96,1024]{1,0:T(8,128)(2,1)S(1)} %get-tuple-element.12), channel_id=1, source_target_pairs={{0,3},{1,0},{2,1},{3,2},{4,7},{5,4},{6,5},{7,6},{8,11},{9,8},{10,9... | collective-permute-start | bytes 589832 | tf_op jit(solution)/shard_map/ppermute | solution.py:11
  50.3 10.4 %copy-start.4 = (f32[1,4,48]{2,1,0:T(4,128)S(1)}, f32[1,4,48]{2,1,0:T(4,128)}, u32[]{:S(2)}) copy-start(f32[1,4,48]{2,1,0:T(4,128)} %param.12) | copy-start | bytes 2308
  55.6 14.6 %collective-permute-start.8 = (bf16[192,1024]{1,0:T(8,128)(2,1)S(1)}, bf16[192,1024]{1,0:T(8,128)(2,1)S(1)}, u32[]{:S(2)}, u32[]{:S(2)}) collective-permute-start(bf16[192,1024]{1,0:T(8,128)(2,1)S(1)} %pad_maximum_fusion.2), channel_id=1, source_target_pairs={{0,1},{1,2},{2,3},{3,0},{4,5},{5,6},{6,7},{7,4},{8,9},{9,10},{10,1... | collective-permute-start | bytes 1179656 | tf_op jit(solution)/shard_map/ppermute | solution.py:11
  57.3 17.2 %collective-permute-start.10 = (bf16[192,1024]{1,0:T(8,128)(2,1)S(1)}, bf16[192,1024]{1,0:T(8,128)(2,1)S(1)}, u32[]{:S(2)}, u32[]{:S(2)}) collective-permute-start(bf16[192,1024]{1,0:T(8,128)(2,1)S(1)} %pad_maximum_fusion.3), channel_id=1, source_target_pairs={{0,3},{1,0},{2,1},{3,2},{4,7},{5,4},{6,5},{7,6},{8,11},{9,8},{10,9... | collective-permute-start | bytes 1179656 | tf_op jit(solution)/shard_map/ppermute | solution.py:11
  74.7 8.5 %copy-start = (bf16[384,1024]{1,0:T(8,128)(2,1)S(1)}, bf16[384,1024]{1,0:T(8,128)(2,1)}, u32[]{:S(2)}) copy-start(bf16[384,1024]{1,0:T(8,128)(2,1)} %param.8) | copy-start | bytes 2359300
  74.7 5.2 %collective-permute-start.11 = (bf16[48,1024]{1,0:T(8,128)(2,1)S(1)}, bf16[48,1024]{1,0:T(8,128)(2,1)S(1)}, u32[]{:S(2)}, u32[]{:S(2)}) collective-permute-start(bf16[48,1024]{1,0:T(8,128)(2,1)S(1)} %get-tuple-element.10), channel_id=1, source_target_pairs={{0,12},{4,0},{8,4},{12,8},{1,13},{5,1},{9,5},{13,9},{2,14},{6,2},{... | collective-permute-start | bytes 294920 | tf_op jit(solution)/shard_map/ppermute | solution.py:11
  76.7 6.0 %collective-permute-start.12 = (bf16[48,1024]{1,0:T(8,128)(2,1)S(1)}, bf16[48,1024]{1,0:T(8,128)(2,1)S(1)}, u32[]{:S(2)}, u32[]{:S(2)}) collective-permute-start(bf16[48,1024]{1,0:T(8,128)(2,1)S(1)} %get-tuple-element.9), channel_id=1, source_target_pairs={{0,8},{4,12},{8,0},{12,4},{1,9},{5,13},{9,1},{13,5},{2,10},{6,14},... | collective-permute-start | bytes 294920 | tf_op jit(solution)/shard_map/ppermute | solution.py:11
  77.3 5.5 %collective-permute-start.13 = (bf16[48,1024]{1,0:T(8,128)(2,1)S(1)}, bf16[48,1024]{1,0:T(8,128)(2,1)S(1)}, u32[]{:S(2)}, u32[]{:S(2)}) collective-permute-start(bf16[48,1024]{1,0:T(8,128)(2,1)S(1)} %get-tuple-element.8), channel_id=1, source_target_pairs={{0,4},{4,8},{8,12},{12,0},{1,5},{5,9},{9,13},{13,1},{2,6},{6,10},{... | collective-permute-start | bytes 294920 | tf_op jit(solution)/shard_map/ppermute | solution.py:11
  83.2 6.5 %copy-start.3 = (f32[1024]{0:T(1024)S(1)}, f32[1024]{0:T(1024)}, u32[]{:S(2)}) copy-start(f32[1024]{0:T(1024)} %param.10) | copy-start | bytes 12292
  83.7 5.4 %collective-permute-start.14 = (f32[384]{0:T(512)S(1)}, f32[384]{0:T(512)S(1)}, u32[]{:S(2)}, u32[]{:S(2)}) collective-permute-start(f32[384]{0:T(512)S(1)} %get-tuple-element.21), channel_id=1, source_target_pairs={{0,1},{1,2},{2,3},{3,0},{4,5},{5,6},{6,7},{7,4},{8,9},{9,10},{10,1... | collective-permute-start | bytes 4616 | tf_op jit(solution)/shard_map/ppermute | solution.py:11
  84.4 4.7 %collective-permute-start.15 = (f32[384]{0:T(512)S(1)}, f32[384]{0:T(512)S(1)}, u32[]{:S(2)}, u32[]{:S(2)}) collective-permute-start(f32[384]{0:T(512)S(1)} %get-tuple-element.21), channel_id=1, source_target_pairs={{0,2},{1,3},{2,0},{3,1},{4,6},{5,7},{6,4},{7,5},{8,10},{9,11},{10,... | collective-permute-start | bytes 4616 | tf_op jit(solution)/shard_map/ppermute | solution.py:11
  85.5 4.2 %collective-permute-start.16 = (f32[384]{0:T(512)S(1)}, f32[384]{0:T(512)S(1)}, u32[]{:S(2)}, u32[]{:S(2)}) collective-permute-start(f32[384]{0:T(512)S(1)} %get-tuple-element.21), channel_id=1, source_target_pairs={{0,3},{1,0},{2,1},{3,2},{4,7},{5,4},{6,5},{7,6},{8,11},{9,8},{10,9... | collective-permute-start | bytes 4616 | tf_op jit(solution)/shard_map/ppermute | solution.py:11

commit v2 on v1

v2 whole, which is shorter than its diff:
```python
import jax
import jax.numpy as jnp
from jax import lax
from jax.sharding import PartitionSpec as P

NORM_EPS = 1e-06
PRESCALE = 2.0 ** -20


def shift(value, axis, n, step):
    return lax.ppermute(value, axis, [(i, (i + step) % n) for i in range(n)])


def move(value, axis, pairs):
    return lax.ppermute(value, axis, pairs)


def line_gather(own, axis, n, here):
    right, left = own, own
    for k in range(1, n):
        going_right = [(i, i + 1) for i in range(k - 1, n - 1)]
        going_left = [(i, i - 1) for i in range(1, n - k + 1)]
        if k == n - 1 and n > 2:
            joined = jnp.where(here >= n // 2, right, left)
            arrived = move(joined, axis, going_right + going_left)
            yield [(jnp.where(here >= k, here - k, (here + k) % n), arrived)]
            continue
        right = move(right, axis, going_right)
        left = move(left, axis, going_left)
        if 2 * k >= n:
            yield [(jnp.where(here >= k, here - k, (here + k) % n), right + left)]
        else:
            yield [((here - k) % n, right), ((here + k) % n, left)]


def line_scatter(part, axis, n, here):
    bf16, f32 = jnp.bfloat16, jnp.float32
    right, left = None, None
    for d in range(n - 1, 0, -1):
        going_right = [(i, i + 1) for i in range(0, n - d)]
        going_left = [(i, i - 1) for i in range(d, n)]
        if 2 * d >= n:
            ahead = part(jnp.where(here < n - d, here + d, (here - d) % n))
            if right is not None:
                ahead = ahead + right.astype(f32) + left.astype(f32)
            ahead = ahead.astype(bf16)
            behind = ahead
        else:
            ahead, behind = part((here + d) % n), part((here - d) % n)
            if right is not None:
                ahead, behind = ahead + right.astype(f32), behind + left.astype(f32)
            ahead, behind = ahead.astype(bf16), behind.astype(bf16)
        if d == n - 1 and n > 2:
            both = move(ahead, axis, going_right + going_left)
            zero = jnp.zeros_like(both)
            right = jnp.where(here < n // 2, both, zero)
            left = jnp.where(here < n // 2, zero, both)
        else:
            right = move(ahead, axis, going_right)
            left = move(behind, axis, going_left)
    total = part(here)
    if right is None:
        return total
    return total + right.astype(f32) + left.astype(f32)


def shards(tokens, pre_gain, out_gain, chosen, route_weight, expert_gate, expert_up, expert_down, n_ep, n_tp):
    model_width = pre_gain.shape[0]
    tok_count, shard_width = tokens.shape
    slot_count = chosen.shape[2]
    here_ep = lax.axis_index("ep")
    here_tp = lax.axis_index("tp")
    bf16, f32 = jnp.bfloat16, jnp.float32

    def relative(table):
        return lax.dynamic_slice_in_dim(jnp.concatenate([table, table], axis=0), here_ep, n_ep, 0)

    slots = relative(chosen[0]).reshape(-1)
    weights = relative(route_weight[0]).reshape(-1)
    token_ids = lax.broadcasted_iota(jnp.int32, (tok_count, slots.shape[0]), 0)
    hit = token_ids == slots[None, :]
    select = hit.astype(bf16)

    picked = lax.dot_general(
        select, tokens, (((0,), (0,)), ((), ())), preferred_element_type=f32
    ).astype(bf16)
    received = [picked[:slot_count]]
    for s in range(1, n_ep):
        received.append(shift(picked[s * slot_count:(s + 1) * slot_count], "ep", n_ep, s))

    gate_matrix, up_matrix, down_matrix = expert_gate[0], expert_up[0], expert_down[0]

    def chunk(owner, block):
        start = owner * shard_width
        gain = lax.dynamic_slice_in_dim(pre_gain, start, shard_width, 0) * PRESCALE
        wide = block.astype(f32)
        squares = jnp.sum(wide * wide, axis=1)
        scaled = (wide * gain).astype(bf16)
        gate_rows = lax.dynamic_slice_in_dim(gate_matrix, start, shard_width, 0)
        up_rows = lax.dynamic_slice_in_dim(up_matrix, start, shard_width, 0)
        return (
            squares,
            jnp.dot(scaled, gate_rows, preferred_element_type=f32),
            jnp.dot(scaled, up_rows, preferred_element_type=f32),
        )

    def gathered(rows):
        total = chunk(here_tp, rows)
        marks = [rows]
        for arrivals in line_gather(rows, "tp", n_tp, here_tp):
            for owner, block in arrivals:
                total = tuple(x + y for x, y in zip(total, chunk(owner, block)))
            marks.append(arrivals[-1][1])
        square_sum, gate_act, up_act = total
        row_scale = (lax.rsqrt(square_sum / model_width + NORM_EPS) / PRESCALE)[:, None]
        hidden = (jax.nn.silu(gate_act * row_scale) * (up_act * row_scale)).astype(bf16)
        return hidden, marks[-2] if len(marks) > 1 else rows

    def part_of(hidden):
        def part(owner):
            columns = lax.dynamic_slice_in_dim(down_matrix, owner * shard_width, shard_width, 1)
            return jnp.dot(hidden, columns, preferred_element_type=f32)

        return part

    cut = (n_ep + 1) // 2
    returned = []
    mark = None
    for group in (range(0, cut), range(cut, n_ep)):
        if len(group) == 0:
            continue
        rows = jnp.concatenate([received[s] for s in group], axis=0)
        if mark is not None:
            rows, _ = lax.optimization_barrier((rows, mark))
        hidden, mark = gathered(rows)
        expert_out = line_scatter(part_of(hidden), "tp", n_tp, here_tp).astype(bf16)
        for at, s in enumerate(group):
            piece = expert_out[at * slot_count:(at + 1) * slot_count]
            returned.append(shift(piece, "ep", n_ep, -s) if s else piece)
    back = jnp.concatenate(returned, axis=0)

    spread = jnp.where(hit, weights[None, :], 0.0)
    coarse = spread.astype(bf16)
    fine = (spread - coarse.astype(f32)).astype(bf16)
    mixed = (
        tokens.astype(f32)
        + jnp.dot(coarse, back, preferred_element_type=f32)
        + jnp.dot(fine, back, preferred_element_type=f32)
    )
    own_sum = jnp.sum(mixed * mixed, axis=1)
    out_sum = own_sum
    for s in range(1, n_tp):
        out_sum = out_sum + shift(own_sum, "tp", n_tp, s)
    out_scale = lax.rsqrt(out_sum / model_width + NORM_EPS)[:, None]
    return (mixed * out_scale * out_gain).astype(bf16)


def solution(mesh):
    def body(*args):
        return shards(*args, n_ep=mesh.shape["ep"], n_tp=mesh.shape["tp"])

    return jax.shard_map(
        body,
        mesh=mesh,
        in_specs=(
            P(("grp", "ep"), "tp"),
            P(),
            P("tp"),
            P(("grp", "ep"), None, None),
            P(("grp", "ep"), None, None),
            P("ep", None, "tp"),
            P("ep", None, "tp"),
            P("ep", "tp", None),
        ),
        out_specs=P(("grp", "ep"), "tp"),
        check_vma=False,
    )
```

time: 91.1 us -> 117 us (1.28)
  starting transfers between devices: 25 us -> 58 us
  waiting for transfers between devices: 47.8 us -> 32.2 us
  matrix products: 13.1 us -> 20.9 us
    ppermute x0 -> x20, starting transfers between devices: none -> 47.1 us  [move(): return lax.ppermute(value, axis, pairs)]
    ppermute x17 -> x9, waiting for transfers between devices: 47.8 us -> 13 us  [shift(): return lax.ppermute(value, axis, [(i, (i + step) % n) for i in range(n)])]
    ppermute x0 -> x20, waiting for transfers between devices: none -> 19.2 us  [move(): return lax.ppermute(value, axis, pairs)]
    ppermute x17 -> x9, starting transfers between devices: 25 us -> 10.9 us  [shift(): return lax.ppermute(value, axis, [(i, (i + step) % n) for i in range(n)])]
    dot_general x4 -> x10, matrix products: 5.12 us -> 8.92 us  [chunk(): jnp.dot(scaled, up_rows, preferred_element_type=f32)]
    dot_general x4 -> x10, matrix products: 1.92 us -> 3.98 us  [part(): return jnp.dot(hidden, columns, preferred_element_type=f32)]
    dot_general x4 -> x10, matrix products: 3.51 us -> 5.56 us  [chunk(): jnp.dot(scaled, gate_rows, preferred_element_type=f32)]
  transfers between devices with their start and end apart: 17 -> 29, of which waited for: 15 -> 12; matrix products, arithmetic and copies ran while one was open for 9% -> 17% of each run, Pallas kernels for 0% -> 0%
where the time goes in v2:
time: 117 us; the launch traced here: 116 us
  starting transfers between devices  58 us (50%)
  waiting for transfers between devices  32.2 us (28%)
  matrix products  20.9 us (18%)
  other arithmetic  3.78 us (3%)
    ppermute x20, starting transfers between devices, move(): return lax.ppermute(value, axis, pairs)  47.1 us
    ppermute x20, waiting for transfers between devices, move(): return lax.ppermute(value, axis, pairs)  19.2 us
    ppermute x9, waiting for transfers between devices, shift(): return lax.ppermute(value, axis, [(i, (i + step) % n) for i in range(n)])  13 us
    ppermute x9, starting transfers between devices, shift(): return lax.ppermute(value, axis, [(i, (i + step) % n) for i in range(n)])  10.9 us
    dot_general x10, matrix products, chunk(): jnp.dot(scaled, up_rows, preferred_element_type=f32)  8.92 us
    dot_general x10, matrix products, chunk(): jnp.dot(scaled, gate_rows, preferred_element_type=f32)  5.56 us
    dot_general x10, matrix products, part(): return jnp.dot(hidden, columns, preferred_element_type=f32)  3.98 us
  transfers between devices with their start and end apart: 29, of which 12 were waited for; matrix products, arithmetic and copies ran while one was open for 17% of the time, Pallas kernels for 0%

profile of v2, /device:TPU:0, one launch (start us, length us, event | category | flops | bytes accessed | tf_op | source)
XLA Modules:
  0.0 116.0 jit_solution(18205669394729433923)
XLA Ops:
  0.0 0.8 pad_add_fusion
  0.9 1.5 %convolution_convert_fusion = bf16[192,1024]{1,0:T(8,128)(2,1)S(1)} fusion(bf16[384,1024]{1,0:T(8,128)(2,1)} %param.8, s32[192]{0:T(256)S(1)} %eq.27), kind=kOutput, calls=%fused_computation.93 | convolution fusion | flops 151265280 | bytes 1180416 | tf_op jit(solution)/shard_map/dot_general | solution.py:84
  2.5 2.5 %collective-permute-start.13 = (bf16[48,1024]{1,0:T(8,128)(2,1)S(1)}, bf16[48,1024]{1,0:T(8,128)(2,1)S(1)}, u32[]{:S(2)}, u32[]{:S(2)}) collective-permute-start(bf16[48,1024]{1,0:T(8,128)(2,1)S(1)} %get-tuple-element.10), channel_id=1, source_target_pairs={{0,12},{4,0},{8,4},{12,8},{1,13},{5,1},{9,5},{13,9},{2,14},{6,2},{... | collective-permute-start | bytes 294920 | tf_op jit(solution)/shard_map/ppermute | solution.py:11
  4.9 0.6 collective-permute-start.12
  5.8 5.1 %collective-permute-done = bf16[48,1024]{1,0:T(8,128)(2,1)S(1)} collective-permute-done((bf16[48,1024]{1,0:T(8,128)(2,1)S(1)}, bf16[48,1024]{1,0:T(8,128)(2,1)S(1)}, u32[]{:S(2)}, u32[]{:S(2)}) %collective-permute-start) | collective-permute-done | bytes 98336 | tf_op jit(solution)/shard_map/ppermute | solution.py:11
  10.9 3.9 %collective-permute-start.1 = (bf16[96,1024]{1,0:T(8,128)(2,1)S(1)}, bf16[96,1024]{1,0:T(8,128)(2,1)S(1)}, u32[]{:S(2)}, u32[]{:S(2)}) collective-permute-start(bf16[96,1024]{1,0:T(8,128)(2,1)S(1)} %pad_maximum_fusion.1), channel_id=1, source_target_pairs={{0,1},{1,2},{2,3},{4,5},{5,6},{6,7},{8,9},{9,10},{10,11},{12,13},{... | collective-permute-start | bytes 589832 | tf_op jit(solution)/shard_map/ppermute | solution.py:15
  14.8 1.3 %collective-permute-start.2 = (bf16[96,1024]{1,0:T(8,128)(2,1)S(1)}, bf16[96,1024]{1,0:T(8,128)(2,1)S(1)}, u32[]{:S(2)}, u32[]{:S(2)}) collective-permute-start(bf16[96,1024]{1,0:T(8,128)(2,1)S(1)} %pad_maximum_fusion.1), channel_id=1, source_target_pairs={{1,0},{2,1},{3,2},{5,4},{6,5},{7,6},{9,8},{10,9},{11,10},{13,12},{... | collective-permute-start | bytes 589832 | tf_op jit(solution)/shard_map/ppermute | solution.py:15
  16.1 2.0 %fusion.58 = f32[96,768]{1,0:T(8,128)S(1)} fusion(bf16[1,4096,768]{2,1,0:T(8,128)(2,1)} %param.13, s32[]{:T(128)S(6)} %select_n.157, f32[1024]{0:T(1024)S(1)} %get-tuple-element.20, bf16[48,1024]{1,0:T(8,128)(2,1)S(1)} %collective-permute-done, bf16[48,1024]{1,0:T(8,128)(2,1)S(1)} %get-tuple-element.9), kind=kOutput, calls=%fused_computation.58 | convolution fusion | flops 151584768 | bytes 2068484 | tf_op jit(solution)/shard_map/dot_general | solution.py:103
  18.1 2.1 %fusion.38 = f32[96,768]{1,0:T(8,128)S(1)} fusion(bf16[1,4096,768]{2,1,0:T(8,128)(2,1)} %param.14, s32[]{:T(128)S(6)} %select_n.157, f32[1024]{0:T(1024)S(1)} %get-tuple-element.20, bf16[48,1024]{1,0:T(8,128)(2,1)S(1)} %collective-permute-done, bf16[48,1024]{1,0:T(8,128)(2,1)S(1)} %get-tuple-element.9), kind=kOutput, calls=%fused_computation.38 | convolution fusion | flops 151584768 | bytes 2068484 | tf_op jit(solution)/shard_map/dot_general | solution.py:104
  20.4 0.7 collective-permute-start.3
  21.2 1.2 %collective-permute-done.2 = bf16[96,1024]{1,0:T(8,128)(2,1)S(1)} collective-permute-done((bf16[96,1024]{1,0:T(8,128)(2,1)S(1)}, bf16[96,1024]{1,0:T(8,128)(2,1)S(1)}, u32[]{:S(2)}, u32[]{:S(2)}) %collective-permute-start.2) | collective-permute-done | bytes 196640 | tf_op jit(solution)/shard_map/ppermute | solution.py:15
  22.5 1.3 %collective-permute-start.4 = (bf16[96,1024]{1,0:T(8,128)(2,1)S(1)}, bf16[96,1024]{1,0:T(8,128)(2,1)S(1)}, u32[]{:S(2)}, u32[]{:S(2)}) collective-permute-start(bf16[96,1024]{1,0:T(8,128)(2,1)S(1)} %collective-permute-done.2), channel_id=1, source_target_pairs={{1,0},{2,1},{5,4},{6,5},{9,8},{10,9},{13,12},{14,13},{17,16},{18,1... | collective-permute-start | bytes 589832 | tf_op jit(solution)/shard_map/ppermute | solution.py:15
  23.8 1.8 %fusion.30 = f32[96,768]{1,0:T(8,128)S(1)} fusion(bf16[1,4096,768]{2,1,0:T(8,128)(2,1)} %param.14, s32[]{:T(128)S(6)} %select_n.161, bf16[96,1024]{1,0:T(8,128)(2,1)S(1)} %collective-permute-done.2, f32[1024]{0:T(1024)S(1)} %get-tuple-element.18), kind=kOutput, calls=%fused_computation.30 | convolution fusion | flops 151289856 | bytes 2068484 | tf_op jit(solution)/shard_map/dot_general | solution.py:104
  26.0 0.4 fusion.93
  26.5 2.2 %fusion.123 = f32[96,768]{1,0:T(8,128)S(1)} fusion(f32[96,768]{1,0:T(8,128)S(1)} %fusion.30, f32[96,768]{1,0:T(8,128)S(1)} %fusion.38, bf16[1,4096,768]{2,1,0:T(8,128)(2,1)} %param.14, s32[]{:T(128)S(6)} %select_n.159, bf16[96,1024]{1,0:T(8,128)(2,1)S(1)} %collective-permute-done.1, f32[1024]{0:T(1024)S(1)} %get-tuple-element.19), kind=kOutput, calls=%fused_computation.105 | convolution fusion | flops 151437312 | bytes 2658308 | tf_op jit(solution)/shard_map/dot_general | solution.py:104
  28.6 3.7 %collective-permute-done.4 = bf16[96,1024]{1,0:T(8,128)(2,1)S(1)} collective-permute-done((bf16[96,1024]{1,0:T(8,128)(2,1)S(1)}, bf16[96,1024]{1,0:T(8,128)(2,1)S(1)}, u32[]{:S(2)}, u32[]{:S(2)}) %collective-permute-start.4) | collective-permute-done | bytes 196640 | tf_op jit(solution)/shard_map/ppermute | solution.py:15
  32.6 1.3 %collective-permute-start.15 = (bf16[96,1024]{1,0:T(8,128)(2,1)S(1)}, bf16[96,1024]{1,0:T(8,128)(2,1)S(1)}, u32[]{:S(2)}, u32[]{:S(2)}) collective-permute-start(bf16[96,1024]{1,0:T(8,128)(2,1)S(1)} %pad_maximum_fusion.2), channel_id=1, source_target_pairs={{1,0},{2,1},{3,2},{5,4},{6,5},{7,6},{9,8},{10,9},{11,10},{13,12},{... | collective-permute-start | bytes 589832 | tf_op jit(solution)/shard_map/ppermute | solution.py:15
  33.9 4.6 %collective-permute-start.14 = (bf16[96,1024]{1,0:T(8,128)(2,1)S(1)}, bf16[96,1024]{1,0:T(8,128)(2,1)S(1)}, u32[]{:S(2)}, u32[]{:S(2)}) collective-permute-start(bf16[96,1024]{1,0:T(8,128)(2,1)S(1)} %pad_maximum_fusion.2), channel_id=1, source_target_pairs={{0,1},{1,2},{2,3},{4,5},{5,6},{6,7},{8,9},{9,10},{10,11},{12,13},{... | collective-permute-start | bytes 589832 | tf_op jit(solution)/shard_map/ppermute | solution.py:15
  38.9 1.3 %collective-permute-start.5 = (bf16[96,1024]{1,0:T(8,128)(2,1)S(1)}, bf16[96,1024]{1,0:T(8,128)(2,1)S(1)}, u32[]{:S(2)}, u32[]{:S(2)}) collective-permute-start(bf16[96,1024]{1,0:T(8,128)(2,1)S(1)} %broadcast_select_fusion.1), channel_id=1, source_target_pairs={{2,3},{1,0},{6,7},{5,4},{10,11},{9,8},{14,15},{13,12},{18,19},{17,... | collective-permute-start | bytes 589832 | tf_op jit(solution)/shard_map/ppermute | solution.py:15
  40.6 5.9 %collective-permute-done.5 = bf16[96,1024]{1,0:T(8,128)(2,1)S(1)} collective-permute-done((bf16[96,1024]{1,0:T(8,128)(2,1)S(1)}, bf16[96,1024]{1,0:T(8,128)(2,1)S(1)}, u32[]{:S(2)}, u32[]{:S(2)}) %collective-permute-start.5) | collective-permute-done | bytes 196640 | tf_op jit(solution)/shard_map/ppermute | solution.py:15
  47.8 0.4 fusion.162
  49.0 1.5 %collective-permute-start.6 = (bf16[96,1024]{1,0:T(8,128)(2,1)S(1)}, bf16[96,1024]{1,0:T(8,128)(2,1)S(1)}, u32[]{:S(2)}, u32[]{:S(2)}) collective-permute-start(bf16[96,1024]{1,0:T(8,128)(2,1)S(1)} %fusion.150), channel_id=1, source_target_pairs={{0,1},{3,2},{4,5},{7,6},{8,9},{11,10},{12,13},{15,14},{16,17},{19,... | collective-permute-start | bytes 589832 | tf_op jit(solution)/shard_map/ppermute | solution.py:15
  51.0 1.3 %collective-permute-start.17 = (bf16[96,1024]{1,0:T(8,128)(2,1)S(1)}, bf16[96,1024]{1,0:T(8,128)(2,1)S(1)}, u32[]{:S(2)}, u32[]{:S(2)}) collective-permute-start(bf16[96,1024]{1,0:T(8,128)(2,1)S(1)} %collective-permute-done.15), channel_id=1, source_target_pairs={{1,0},{2,1},{5,4},{6,5},{9,8},{10,9},{13,12},{14,13},{17,16},{18,1... | collective-permute-start | bytes 589832 | tf_op jit(solution)/shard_map/ppermute | solution.py:15
  52.8 0.7 collective-permute-start.16
  55.5 3.5 %collective-permute-done.17 = bf16[96,1024]{1,0:T(8,128)(2,1)S(1)} collective-permute-done((bf16[96,1024]{1,0:T(8,128)(2,1)S(1)}, bf16[96,1024]{1,0:T(8,128)(2,1)S(1)}, u32[]{:S(2)}, u32[]{:S(2)}) %collective-permute-start.17) | collective-permute-done | bytes 196640 | tf_op jit(solution)/shard_map/ppermute | solution.py:15
  59.1 1.3 %collective-permute-start.18 = (bf16[96,1024]{1,0:T(8,128)(2,1)S(1)}, bf16[96,1024]{1,0:T(8,128)(2,1)S(1)}, u32[]{:S(2)}, u32[]{:S(2)}) collective-permute-start(bf16[96,1024]{1,0:T(8,128)(2,1)S(1)} %broadcast_select_fusion), channel_id=1, source_target_pairs={{2,3},{1,0},{6,7},{5,4},{10,11},{9,8},{14,15},{13,12},{18,19},{17,... | collective-permute-start | bytes 589832 | tf_op jit(solution)/shard_map/ppermute | solution.py:15
  60.8 0.7 collective-permute-start.9
  61.5 5.2 %collective-permute-start.7 = (bf16[96,1024]{1,0:T(8,128)(2,1)S(1)}, bf16[96,1024]{1,0:T(8,128)(2,1)S(1)}, u32[]{:S(2)}, u32[]{:S(2)}) collective-permute-start(bf16[96,1024]{1,0:T(8,128)(2,1)S(1)} %add_convert_fusion.7), channel_id=1, source_target_pairs={{0,1},{1,2},{4,5},{5,6},{8,9},{9,10},{12,13},{13,14},{16,17},{17,1... | collective-permute-start | bytes 589832 | tf_op jit(solution)/shard_map/ppermute | solution.py:15
  68.2 0.4 fusion.165
  69.0 5.2 %collective-permute-start.19 = (bf16[96,1024]{1,0:T(8,128)(2,1)S(1)}, bf16[96,1024]{1,0:T(8,128)(2,1)S(1)}, u32[]{:S(2)}, u32[]{:S(2)}) collective-permute-start(bf16[96,1024]{1,0:T(8,128)(2,1)S(1)} %fusion.153), channel_id=1, source_target_pairs={{0,1},{3,2},{4,5},{7,6},{8,9},{11,10},{12,13},{15,14},{16,17},{19,... | collective-permute-start | bytes 589832 | tf_op jit(solution)/shard_map/ppermute | solution.py:15
  74.7 1.3 %collective-permute-start.10 = (bf16[96,1024]{1,0:T(8,128)(2,1)S(1)}, bf16[96,1024]{1,0:T(8,128)(2,1)S(1)}, u32[]{:S(2)}, u32[]{:S(2)}) collective-permute-start(bf16[96,1024]{1,0:T(8,128)(2,1)S(1)} %add_convert_fusion.5), channel_id=1, source_target_pairs={{1,0},{2,1},{3,2},{5,4},{6,5},{7,6},{9,8},{10,9},{11,10},{13,12},{... | collective-permute-start | bytes 589832 | tf_op jit(solution)/shard_map/ppermute | solution.py:15
  76.4 4.6 %collective-permute-start.8 = (bf16[96,1024]{1,0:T(8,128)(2,1)S(1)}, bf16[96,1024]{1,0:T(8,128)(2,1)S(1)}, u32[]{:S(2)}, u32[]{:S(2)}) collective-permute-start(bf16[96,1024]{1,0:T(8,128)(2,1)S(1)} %add_convert_fusion.6), channel_id=1, source_target_pairs={{0,1},{1,2},{2,3},{4,5},{5,6},{6,7},{8,9},{9,10},{10,11},{12,13},{... | collective-permute-start | bytes 589832 | tf_op jit(solution)/shard_map/ppermute | solution.py:15
  81.8 0.7 collective-permute-start.22
  82.5 2.8 %collective-permute-start.20 = (bf16[96,1024]{1,0:T(8,128)(2,1)S(1)}, bf16[96,1024]{1,0:T(8,128)(2,1)S(1)}, u32[]{:S(2)}, u32[]{:S(2)}) collective-permute-start(bf16[96,1024]{1,0:T(8,128)(2,1)S(1)} %add_convert_fusion.3), channel_id=1, source_target_pairs={{0,1},{1,2},{4,5},{5,6},{8,9},{9,10},{12,13},{13,14},{16,17},{17,1... | collective-permute-start | bytes 589832 | tf_op jit(solution)/shard_map/ppermute | solution.py:15
  85.4 1.3 %collective-permute-start.23 = (bf16[96,1024]{1,0:T(8,128)(2,1)S(1)}, bf16[96,1024]{1,0:T(8,128)(2,1)S(1)}, u32[]{:S(2)}, u32[]{:S(2)}) collective-permute-start(bf16[96,1024]{1,0:T(8,128)(2,1)S(1)} %add_convert_fusion.1), channel_id=1, source_target_pairs={{1,0},{2,1},{3,2},{5,4},{6,5},{7,6},{9,8},{10,9},{11,10},{13,12},{... | collective-permute-start | bytes 589832 | tf_op jit(solution)/shard_map/ppermute | solution.py:15
  86.7 1.9 %collective-permute-done.20 = bf16[96,1024]{1,0:T(8,128)(2,1)S(1)} collective-permute-done((bf16[96,1024]{1,0:T(8,128)(2,1)S(1)}, bf16[96,1024]{1,0:T(8,128)(2,1)S(1)}, u32[]{:S(2)}, u32[]{:S(2)}) %collective-permute-start.20) | collective-permute-done | bytes 196640 | tf_op jit(solution)/shard_map/ppermute | solution.py:15
  88.6 6.5 %collective-permute-start.21 = (bf16[96,1024]{1,0:T(8,128)(2,1)S(1)}, bf16[96,1024]{1,0:T(8,128)(2,1)S(1)}, u32[]{:S(2)}, u32[]{:S(2)}) collective-permute-start(bf16[96,1024]{1,0:T(8,128)(2,1)S(1)} %add_convert_fusion.2), channel_id=1, source_target_pairs={{0,1},{1,2},{2,3},{4,5},{5,6},{6,7},{8,9},{9,10},{10,11},{12,13},{... | collective-permute-start | bytes 589832 | tf_op jit(solution)/shard_map/ppermute | solution.py:15
  95.2 1.5 %collective-permute-done.23 = bf16[96,1024]{1,0:T(8,128)(2,1)S(1)} collective-permute-done((bf16[96,1024]{1,0:T(8,128)(2,1)S(1)}, bf16[96,1024]{1,0:T(8,128)(2,1)S(1)}, u32[]{:S(2)}, u32[]{:S(2)}) %collective-permute-start.23) | collective-permute-done | bytes 196640 | tf_op jit(solution)/shard_map/ppermute | solution.py:15
  96.8 1.5 %collective-permute-done.21 = bf16[96,1024]{1,0:T(8,128)(2,1)S(1)} collective-permute-done((bf16[96,1024]{1,0:T(8,128)(2,1)S(1)}, bf16[96,1024]{1,0:T(8,128)(2,1)S(1)}, u32[]{:S(2)}, u32[]{:S(2)}) %collective-permute-start.21) | collective-permute-done | bytes 196640 | tf_op jit(solution)/shard_map/ppermute | solution.py:15
  98.4 1.5 %collective-permute-start.24 = (bf16[48,1024]{1,0:T(8,128)(2,1)S(1)}, bf16[48,1024]{1,0:T(8,128)(2,1)S(1)}, u32[]{:S(2)}, u32[]{:S(2)}) collective-permute-start(bf16[48,1024]{1,0:T(8,128)(2,1)S(1)} %get-tuple-element.15), channel_id=1, source_target_pairs={{0,8},{4,12},{8,0},{12,4},{1,9},{5,13},{9,1},{13,5},{2,10},{6,14},... | collective-permute-start | bytes 294920 | tf_op jit(solution)/shard_map/ppermute | solution.py:11
  100.0 3.2 %collective-permute-done.24 = bf16[48,1024]{1,0:T(8,128)(2,1)S(1)} collective-permute-done((bf16[48,1024]{1,0:T(8,128)(2,1)S(1)}, bf16[48,1024]{1,0:T(8,128)(2,1)S(1)}, u32[]{:S(2)}, u32[]{:S(2)}) %collective-permute-start.24) | collective-permute-done | bytes 98336 | tf_op jit(solution)/shard_map/ppermute | solution.py:11
  103.2 0.9 collective-permute-done.25
  104.5 0.5 multiply_reduce_fusion
  105.0 4.4 %collective-permute-start.28 = (f32[384]{0:T(512)S(1)}, f32[384]{0:T(512)S(1)}, u32[]{:S(2)}, u32[]{:S(2)}) collective-permute-start(f32[384]{0:T(512)S(1)} %get-tuple-element.22), channel_id=1, source_target_pairs={{0,3},{1,0},{2,1},{3,2},{4,7},{5,4},{6,5},{7,6},{8,11},{9,8},{10,9... | collective-permute-start | bytes 4616 | tf_op jit(solution)/shard_map/ppermute | solution.py:11
  109.4 1.6 %collective-permute-start.26 = (f32[384]{0:T(512)S(1)}, f32[384]{0:T(512)S(1)}, u32[]{:S(2)}, u32[]{:S(2)}) collective-permute-start(f32[384]{0:T(512)S(1)} %get-tuple-element.22), channel_id=1, source_target_pairs={{0,1},{1,2},{2,3},{3,0},{4,5},{5,6},{6,7},{7,4},{8,9},{9,10},{10,1... | collective-permute-start | bytes 4616 | tf_op jit(solution)/shard_map/ppermute | solution.py:11
  111.0 2.9 %collective-permute-done.27 = f32[384]{0:T(512)S(1)} collective-permute-done((f32[384]{0:T(512)S(1)}, f32[384]{0:T(512)S(1)}, u32[]{:S(2)}, u32[]{:S(2)}) %collective-permute-start.27) | collective-permute-done | bytes 1568 | tf_op jit(solution)/shard_map/ppermute | solution.py:11
  113.9 0.9 collective-permute-done.26
  114.8 1.2 %multiply_convert_fusion = bf16[384,1024]{1,0:T(8,128)(2,1)} fusion(f32[1024]{0:T(1024)S(1)} %copy-done.4, f32[384]{0:T(512)S(1)} %add_rsqrt_fusion, f32[384,1024]{1,0:T(8,128)S(1)} %get-tuple-element.23, f32[384,1024]{1,0:T(8,128)S(1)} %fusion.189, bf16[384,1024]{1,0:T(8,128)(2,1)S(1)} %copy-done.2), kind=kLoop, calls=%fused_computation.60 | loop fusion | flops 2359296 | bytes 4724224 | tf_op jit(solution)/shard_map/convert_element_type | solution.py:155
  (94 shorter events, 12.2 us)
Async XLA Ops:
  0.0 5.7 %copy-start.3 = (f32[4096]{0:T(1024)S(1)}, f32[4096]{0:T(1024)}, u32[]{:S(2)}) copy-start(f32[4096]{0:T(1024)} %param.9) | copy-start | bytes 49156
  0.0 5.7 %copy-start.5 = (f32[1,4,48]{2,1,0:T(4,128)S(1)}, f32[1,4,48]{2,1,0:T(4,128)}, u32[]{:S(2)}) copy-start(f32[1,4,48]{2,1,0:T(4,128)} %param.12) | copy-start | bytes 2308
  2.5 17.8 %collective-permute-start.13 = (bf16[48,1024]{1,0:T(8,128)(2,1)S(1)}, bf16[48,1024]{1,0:T(8,128)(2,1)S(1)}, u32[]{:S(2)}, u32[]{:S(2)}) collective-permute-start(bf16[48,1024]{1,0:T(8,128)(2,1)S(1)} %get-tuple-element.10), channel_id=1, source_target_pairs={{0,12},{4,0},{8,4},{12,8},{1,13},{5,1},{9,5},{13,9},{2,14},{6,2},{... | collective-permute-start | bytes 294920 | tf_op jit(solution)/shard_map/ppermute | solution.py:11
  4.9 15.4 %collective-permute-start.12 = (bf16[48,1024]{1,0:T(8,128)(2,1)S(1)}, bf16[48,1024]{1,0:T(8,128)(2,1)S(1)}, u32[]{:S(2)}, u32[]{:S(2)}) collective-permute-start(bf16[48,1024]{1,0:T(8,128)(2,1)S(1)} %get-tuple-element.11), channel_id=1, source_target_pairs={{0,8},{4,12},{8,0},{12,4},{1,9},{5,13},{9,1},{13,5},{2,10},{6,14},... | collective-permute-start | bytes 294920 | tf_op jit(solution)/shard_map/ppermute | solution.py:11
  5.6 5.3 %collective-permute-start = (bf16[48,1024]{1,0:T(8,128)(2,1)S(1)}, bf16[48,1024]{1,0:T(8,128)(2,1)S(1)}, u32[]{:S(2)}, u32[]{:S(2)}) collective-permute-start(bf16[48,1024]{1,0:T(8,128)(2,1)S(1)} %get-tuple-element.12), channel_id=1, source_target_pairs={{0,4},{4,8},{8,12},{12,0},{1,5},{5,9},{9,13},{13,1},{2,6},{6,10},{... | collective-permute-start | bytes 294920 | tf_op jit(solution)/shard_map/ppermute | solution.py:11
  10.9 9.4 %collective-permute-start.1 = (bf16[96,1024]{1,0:T(8,128)(2,1)S(1)}, bf16[96,1024]{1,0:T(8,128)(2,1)S(1)}, u32[]{:S(2)}, u32[]{:S(2)}) collective-permute-start(bf16[96,1024]{1,0:T(8,128)(2,1)S(1)} %pad_maximum_fusion.1), channel_id=1, source_target_pairs={{0,1},{1,2},{2,3},{4,5},{5,6},{6,7},{8,9},{9,10},{10,11},{12,13},{... | collective-permute-start | bytes 589832 | tf_op jit(solution)/shard_map/ppermute | solution.py:15
  14.8 7.6 %collective-permute-start.2 = (bf16[96,1024]{1,0:T(8,128)(2,1)S(1)}, bf16[96,1024]{1,0:T(8,128)(2,1)S(1)}, u32[]{:S(2)}, u32[]{:S(2)}) collective-permute-start(bf16[96,1024]{1,0:T(8,128)(2,1)S(1)} %pad_maximum_fusion.1), channel_id=1, source_target_pairs={{1,0},{2,1},{3,2},{5,4},{6,5},{7,6},{9,8},{10,9},{11,10},{13,12},{... | collective-permute-start | bytes 589832 | tf_op jit(solution)/shard_map/ppermute | solution.py:15
  16.1 9.5 %copy-start = (bf16[1,4096,768]{2,1,0:T(8,128)(2,1)S(1)}, bf16[1,4096,768]{2,1,0:T(8,128)(2,1)}, u32[]{:S(2)}) copy-start(bf16[1,4096,768]{2,1,0:T(8,128)(2,1)} %param.13) | copy-start | bytes 18874372
  20.4 8.3 %collective-permute-start.3 = (bf16[96,1024]{1,0:T(8,128)(2,1)S(1)}, bf16[96,1024]{1,0:T(8,128)(2,1)S(1)}, u32[]{:S(2)}, u32[]{:S(2)}) collective-permute-start(bf16[96,1024]{1,0:T(8,128)(2,1)S(1)} %collective-permute-done.1), channel_id=1, source_target_pairs={{1,2},{2,3},{5,6},{6,7},{9,10},{10,11},{13,14},{14,15},{17,18},{18... | collective-permute-start | bytes 589832 | tf_op jit(solution)/shard_map/ppermute | solution.py:15
  22.5 9.8 %collective-permute-start.4 = (bf16[96,1024]{1,0:T(8,128)(2,1)S(1)}, bf16[96,1024]{1,0:T(8,128)(2,1)S(1)}, u32[]{:S(2)}, u32[]{:S(2)}) collective-permute-start(bf16[96,1024]{1,0:T(8,128)(2,1)S(1)} %collective-permute-done.2), channel_id=1, source_target_pairs={{1,0},{2,1},{5,4},{6,5},{9,8},{10,9},{13,12},{14,13},{17,16},{18,1... | collective-permute-start | bytes 589832 | tf_op jit(solution)/shard_map/ppermute | solution.py:15
  25.6 12.8 %copy-start.1 = (bf16[1,4096,768]{2,1,0:T(8,128)(2,1)S(1)}, bf16[1,4096,768]{2,1,0:T(8,128)(2,1)}, u32[]{:S(2)}) copy-start(bf16[1,4096,768]{2,1,0:T(8,128)(2,1)} %param.14) | copy-start | bytes 18874372
  32.6 18.3 %collective-permute-start.15 = (bf16[96,1024]{1,0:T(8,128)(2,1)S(1)}, bf16[96,1024]{1,0:T(8,128)(2,1)S(1)}, u32[]{:S(2)}, u32[]{:S(2)}) collective-permute-start(bf16[96,1024]{1,0:T(8,128)(2,1)S(1)} %pad_maximum_fusion.2), channel_id=1, source_target_pairs={{1,0},{2,1},{3,2},{5,4},{6,5},{7,6},{9,8},{10,9},{11,10},{13,12},{... | collective-permute-start | bytes 589832 | tf_op jit(solution)/shard_map/ppermute | solution.py:15
  33.9 18.8 %collective-permute-start.14 = (bf16[96,1024]{1,0:T(8,128)(2,1)S(1)}, bf16[96,1024]{1,0:T(8,128)(2,1)S(1)}, u32[]{:S(2)}, u32[]{:S(2)}) collective-permute-start(bf16[96,1024]{1,0:T(8,128)(2,1)S(1)} %pad_maximum_fusion.2), channel_id=1, source_target_pairs={{0,1},{1,2},{2,3},{4,5},{5,6},{6,7},{8,9},{9,10},{10,11},{12,13},{... | collective-permute-start | bytes 589832 | tf_op jit(solution)/shard_map/ppermute | solution.py:15
  38.9 7.6 %collective-permute-start.5 = (bf16[96,1024]{1,0:T(8,128)(2,1)S(1)}, bf16[96,1024]{1,0:T(8,128)(2,1)S(1)}, u32[]{:S(2)}, u32[]{:S(2)}) collective-permute-start(bf16[96,1024]{1,0:T(8,128)(2,1)S(1)} %broadcast_select_fusion.1), channel_id=1, source_target_pairs={{2,3},{1,0},{6,7},{5,4},{10,11},{9,8},{14,15},{13,12},{18,19},{17,... | collective-permute-start | bytes 589832 | tf_op jit(solution)/shard_map/ppermute | solution.py:15
  40.2 8.1 %slice-start = ((s8[6291456]{0:T(1024)(128)(4,1)}), s8[4194304]{0:T(1024)(128)(4,1)S(1)}, s32[]{:S(2)}) async-start(s8[6291456]{0:T(1024)(128)(4,1)} %bitcast.144), calls=%async_computation | async-start | bytes 8388608
  47.0 1.6 %slice-start.1 = ((s8[6291456]{0:T(1024)(128)(4,1)}), s8[2097152]{0:T(1024)(128)(4,1)S(1)}, s32[]{:S(2)}) async-start(s8[6291456]{0:T(1024)(128)(4,1)} %bitcast.144), calls=%async_computation.1 | async-start | bytes 4194304
  49.0 11.4 %collective-permute-start.6 = (bf16[96,1024]{1,0:T(8,128)(2,1)S(1)}, bf16[96,1024]{1,0:T(8,128)(2,1)S(1)}, u32[]{:S(2)}, u32[]{:S(2)}) collective-permute-start(bf16[96,1024]{1,0:T(8,128)(2,1)S(1)} %fusion.150), channel_id=1, source_target_pairs={{0,1},{3,2},{4,5},{7,6},{8,9},{11,10},{12,13},{15,14},{16,17},{19,... | collective-permute-start | bytes 589832 | tf_op jit(solution)/shard_map/ppermute | solution.py:15
  51.0 8.1 %collective-permute-start.17 = (bf16[96,1024]{1,0:T(8,128)(2,1)S(1)}, bf16[96,1024]{1,0:T(8,128)(2,1)S(1)}, u32[]{:S(2)}, u32[]{:S(2)}) collective-permute-start(bf16[96,1024]{1,0:T(8,128)(2,1)S(1)} %collective-permute-done.15), channel_id=1, source_target_pairs={{1,0},{2,1},{5,4},{6,5},{9,8},{10,9},{13,12},{14,13},{17,16},{18,1... | collective-permute-start | bytes 589832 | tf_op jit(solution)/shard_map/ppermute | solution.py:15
  52.8 6.2 %collective-permute-start.16 = (bf16[96,1024]{1,0:T(8,128)(2,1)S(1)}, bf16[96,1024]{1,0:T(8,128)(2,1)S(1)}, u32[]{:S(2)}, u32[]{:S(2)}) collective-permute-start(bf16[96,1024]{1,0:T(8,128)(2,1)S(1)} %collective-permute-done.14), channel_id=1, source_target_pairs={{1,2},{2,3},{5,6},{6,7},{9,10},{10,11},{13,14},{14,15},{17,18},{18... | collective-permute-start | bytes 589832 | tf_op jit(solution)/shard_map/ppermute | solution.py:15
  59.1 7.7 %collective-permute-start.18 = (bf16[96,1024]{1,0:T(8,128)(2,1)S(1)}, bf16[96,1024]{1,0:T(8,128)(2,1)S(1)}, u32[]{:S(2)}, u32[]{:S(2)}) collective-permute-start(bf16[96,1024]{1,0:T(8,128)(2,1)S(1)} %broadcast_select_fusion), channel_id=1, source_target_pairs={{2,3},{1,0},{6,7},{5,4},{10,11},{9,8},{14,15},{13,12},{18,19},{17,... | collective-permute-start | bytes 589832 | tf_op jit(solution)/shard_map/ppermute | solution.py:15
  60.8 13.8 %collective-permute-start.9 = (bf16[96,1024]{1,0:T(8,128)(2,1)S(1)}, bf16[96,1024]{1,0:T(8,128)(2,1)S(1)}, u32[]{:S(2)}, u32[]{:S(2)}) collective-permute-start(bf16[96,1024]{1,0:T(8,128)(2,1)S(1)} %add_convert_fusion.7), channel_id=1, source_target_pairs={{2,1},{3,2},{6,5},{7,6},{10,9},{11,10},{14,13},{15,14},{18,17},{19... | collective-permute-start | bytes 589832 | tf_op jit(solution)/shard_map/ppermute | solution.py:15
  61.5 14.9 %collective-permute-start.7 = (bf16[96,1024]{1,0:T(8,128)(2,1)S(1)}, bf16[96,1024]{1,0:T(8,128)(2,1)S(1)}, u32[]{:S(2)}, u32[]{:S(2)}) collective-permute-start(bf16[96,1024]{1,0:T(8,128)(2,1)S(1)} %add_convert_fusion.7), channel_id=1, source_target_pairs={{0,1},{1,2},{4,5},{5,6},{8,9},{9,10},{12,13},{13,14},{16,17},{17,1... | collective-permute-start | bytes 589832 | tf_op jit(solution)/shard_map/ppermute | solution.py:15
  69.0 12.4 %collective-permute-start.19 = (bf16[96,1024]{1,0:T(8,128)(2,1)S(1)}, bf16[96,1024]{1,0:T(8,128)(2,1)S(1)}, u32[]{:S(2)}, u32[]{:S(2)}) collective-permute-start(bf16[96,1024]{1,0:T(8,128)(2,1)S(1)} %fusion.153), channel_id=1, source_target_pairs={{0,1},{3,2},{4,5},{7,6},{8,9},{11,10},{12,13},{15,14},{16,17},{19,... | collective-permute-start | bytes 589832 | tf_op jit(solution)/shard_map/ppermute | solution.py:15
  74.7 10.6 %collective-permute-start.10 = (bf16[96,1024]{1,0:T(8,128)(2,1)S(1)}, bf16[96,1024]{1,0:T(8,128)(2,1)S(1)}, u32[]{:S(2)}, u32[]{:S(2)}) collective-permute-start(bf16[96,1024]{1,0:T(8,128)(2,1)S(1)} %add_convert_fusion.5), channel_id=1, source_target_pairs={{1,0},{2,1},{3,2},{5,4},{6,5},{7,6},{9,8},{10,9},{11,10},{13,12},{... | collective-permute-start | bytes 589832 | tf_op jit(solution)/shard_map/ppermute | solution.py:15
  76.4 8.9 %collective-permute-start.8 = (bf16[96,1024]{1,0:T(8,128)(2,1)S(1)}, bf16[96,1024]{1,0:T(8,128)(2,1)S(1)}, u32[]{:S(2)}, u32[]{:S(2)}) collective-permute-start(bf16[96,1024]{1,0:T(8,128)(2,1)S(1)} %add_convert_fusion.6), channel_id=1, source_target_pairs={{0,1},{1,2},{2,3},{4,5},{5,6},{6,7},{8,9},{9,10},{10,11},{12,13},{... | collective-permute-start | bytes 589832 | tf_op jit(solution)/shard_map/ppermute | solution.py:15
  81.8 3.6 %collective-permute-start.22 = (bf16[96,1024]{1,0:T(8,128)(2,1)S(1)}, bf16[96,1024]{1,0:T(8,128)(2,1)S(1)}, u32[]{:S(2)}, u32[]{:S(2)}) collective-permute-start(bf16[96,1024]{1,0:T(8,128)(2,1)S(1)} %add_convert_fusion.3), channel_id=1, source_target_pairs={{2,1},{3,2},{6,5},{7,6},{10,9},{11,10},{14,13},{15,14},{18,17},{19... | collective-permute-start | bytes 589832 | tf_op jit(solution)/shard_map/ppermute | solution.py:15
  82.5 6.1 %collective-permute-start.20 = (bf16[96,1024]{1,0:T(8,128)(2,1)S(1)}, bf16[96,1024]{1,0:T(8,128)(2,1)S(1)}, u32[]{:S(2)}, u32[]{:S(2)}) collective-permute-start(bf16[96,1024]{1,0:T(8,128)(2,1)S(1)} %add_convert_fusion.3), channel_id=1, source_target_pairs={{0,1},{1,2},{4,5},{5,6},{8,9},{9,10},{12,13},{13,14},{16,17},{17,1... | collective-permute-start | bytes 589832 | tf_op jit(solution)/shard_map/ppermute | solution.py:15
  85.4 11.3 %collective-permute-start.23 = (bf16[96,1024]{1,0:T(8,128)(2,1)S(1)}, bf16[96,1024]{1,0:T(8,128)(2,1)S(1)}, u32[]{:S(2)}, u32[]{:S(2)}) collective-permute-start(bf16[96,1024]{1,0:T(8,128)(2,1)S(1)} %add_convert_fusion.1), channel_id=1, source_target_pairs={{1,0},{2,1},{3,2},{5,4},{6,5},{7,6},{9,8},{10,9},{11,10},{13,12},{... | collective-permute-start | bytes 589832 | tf_op jit(solution)/shard_map/ppermute | solution.py:15
  88.6 9.6 %collective-permute-start.21 = (bf16[96,1024]{1,0:T(8,128)(2,1)S(1)}, bf16[96,1024]{1,0:T(8,128)(2,1)S(1)}, u32[]{:S(2)}, u32[]{:S(2)}) collective-permute-start(bf16[96,1024]{1,0:T(8,128)(2,1)S(1)} %add_convert_fusion.2), channel_id=1, source_target_pairs={{0,1},{1,2},{2,3},{4,5},{5,6},{6,7},{8,9},{9,10},{10,11},{12,13},{... | collective-permute-start | bytes 589832 | tf_op jit(solution)/shard_map/ppermute | solution.py:15
  95.1 9.3 %copy-start.2 = (bf16[384,1024]{1,0:T(8,128)(2,1)S(1)}, bf16[384,1024]{1,0:T(8,128)(2,1)}, u32[]{:S(2)}) copy-start(bf16[384,1024]{1,0:T(8,128)(2,1)} %param.8) | copy-start | bytes 2359300
  95.1 4.9 %collective-permute-start.11 = (bf16[48,1024]{1,0:T(8,128)(2,1)S(1)}, bf16[48,1024]{1,0:T(8,128)(2,1)S(1)}, u32[]{:S(2)}, u32[]{:S(2)}) collective-permute-start(bf16[48,1024]{1,0:T(8,128)(2,1)S(1)} %get-tuple-element.14), channel_id=1, source_target_pairs={{0,12},{4,0},{8,4},{12,8},{1,13},{5,1},{9,5},{13,9},{2,14},{6,2},{... | collective-permute-start | bytes 294920 | tf_op jit(solution)/shard_map/ppermute | solution.py:11
  98.4 4.8 %collective-permute-start.24 = (bf16[48,1024]{1,0:T(8,128)(2,1)S(1)}, bf16[48,1024]{1,0:T(8,128)(2,1)S(1)}, u32[]{:S(2)}, u32[]{:S(2)}) collective-permute-start(bf16[48,1024]{1,0:T(8,128)(2,1)S(1)} %get-tuple-element.15), channel_id=1, source_target_pairs={{0,8},{4,12},{8,0},{12,4},{1,9},{5,13},{9,1},{13,5},{2,10},{6,14},... | collective-permute-start | bytes 294920 | tf_op jit(solution)/shard_map/ppermute | solution.py:11
  99.9 4.2 %collective-permute-start.25 = (bf16[48,1024]{1,0:T(8,128)(2,1)S(1)}, bf16[48,1024]{1,0:T(8,128)(2,1)S(1)}, u32[]{:S(2)}, u32[]{:S(2)}) collective-permute-start(bf16[48,1024]{1,0:T(8,128)(2,1)S(1)} %get-tuple-element.16), channel_id=1, source_target_pairs={{0,4},{4,8},{8,12},{12,0},{1,5},{5,9},{9,13},{13,1},{2,6},{6,10},{... | collective-permute-start | bytes 294920 | tf_op jit(solution)/shard_map/ppermute | solution.py:11
  104.5 10.3 %copy-start.4 = (f32[1024]{0:T(1024)S(1)}, f32[1024]{0:T(1024)}, u32[]{:S(2)}) copy-start(f32[1024]{0:T(1024)} %param.10) | copy-start | bytes 12292
  105.0 6.0 %collective-permute-start.28 = (f32[384]{0:T(512)S(1)}, f32[384]{0:T(512)S(1)}, u32[]{:S(2)}, u32[]{:S(2)}) collective-permute-start(f32[384]{0:T(512)S(1)} %get-tuple-element.22), channel_id=1, source_target_pairs={{0,3},{1,0},{2,1},{3,2},{4,7},{5,4},{6,5},{7,6},{8,11},{9,8},{10,9... | collective-permute-start | bytes 4616 | tf_op jit(solution)/shard_map/ppermute | solution.py:11
  109.4 4.5 %collective-permute-start.27 = (f32[384]{0:T(512)S(1)}, f32[384]{0:T(512)S(1)}, u32[]{:S(2)}, u32[]{:S(2)}) collective-permute-start(f32[384]{0:T(512)S(1)} %get-tuple-element.22), channel_id=1, source_target_pairs={{0,2},{1,3},{2,0},{3,1},{4,6},{5,7},{6,4},{7,5},{8,10},{9,11},{10,... | collective-permute-start | bytes 4616 | tf_op jit(solution)/shard_map/ppermute | solution.py:11
  109.4 5.4 %collective-permute-start.26 = (f32[384]{0:T(512)S(1)}, f32[384]{0:T(512)S(1)}, u32[]{:S(2)}, u32[]{:S(2)}) collective-permute-start(f32[384]{0:T(512)S(1)} %get-tuple-element.22), channel_id=1, source_target_pairs={{0,1},{1,2},{2,3},{3,0},{4,5},{5,6},{6,7},{7,4},{8,9},{9,10},{10,1... | collective-permute-start | bytes 4616 | tf_op jit(solution)/shard_map/ppermute | solution.py:11

commit v3 on v1

--- a/solution.py
+++ b/solution.py
@@ -28,29 +28,30 @@
 
 def ring_scatter(part, axis, n, rows):
     half = rows // 2
+    parts = {}
 
-    def add(full, extra, low):
-        if extra is None:
-            return full
-        extra = extra.astype(jnp.float32)
-        if extra.shape[0] == rows:
-            return full + extra
-        if low:
-            return jnp.concatenate([full[:half] + extra, full[half:]], axis=0)
-        return jnp.concatenate([full[:half], full[half:] + extra], axis=0)
+    def take(offset, low):
+        if offset not in parts:
+            parts[offset] = part(offset)
+        return parts[offset][:half] if low else parts[offset][half:]
 
-    forward, backward = None, None
+    arrived = {}
     for d in range(n // 2, 0, -1):
-        if 2 * d == n:
-            whole = part(d).astype(jnp.bfloat16)
-            forward = shift(whole[:half], axis, n, 1)
-            backward = shift(whole[half:], axis, n, -1)
-        else:
-            ahead = add(part(d), forward, True).astype(jnp.bfloat16)
-            behind = add(part(-d), backward, False).astype(jnp.bfloat16)
-            forward = shift(ahead, axis, n, 1)
-            backward = shift(behind, axis, n, -1)
-    return add(add(part(0), forward, True), backward, False)
+        for low, way in ((True, 1), (False, -1), (False, 1), (True, -1)):
+            if 2 * d == n and low != (way == 1):
+                continue
+            value = take(way * d if 2 * d < n else d, low)
+            if (low, way) in arrived:
+                value = value + arrived[low, way].astype(jnp.float32)
+            arrived[low, way] = shift(value.astype(jnp.bfloat16), axis, n, way)
+    sums = []
+    for low in (True, False):
+        value = take(0, low)
+        for way in (1, -1):
+            if (low, way) in arrived:
+                value = value + arrived[low, way].astype(jnp.float32)
+        sums.append(value)
+    return jnp.concatenate(sums, axis=0)
 
 
 def shards(tokens, pre_gain, out_gain, chosen, route_weight, expert_gate, expert_up, expert_down, n_ep, n_tp):
@@ -68,14 +69,14 @@
     weights = relative(route_weight[0]).reshape(-1)
     token_ids = lax.broadcasted_iota(jnp.int32, (tok_count, slots.shape[0]), 0)
     hit = token_ids == slots[None, :]
-    select = hit.astype(bf16)
 
-    picked = lax.dot_general(
-        select, tokens, (((0,), (0,)), ((), ())), preferred_element_type=f32
-    ).astype(bf16)
-    received = [picked[:slot_count]]
-    for s in range(1, n_ep):
-        received.append(shift(picked[s * slot_count:(s + 1) * slot_count], "ep", n_ep, s))
+    def pick(s):
+        ids = slots[s * slot_count:(s + 1) * slot_count]
+        select = (ids[:, None] == lax.broadcasted_iota(jnp.int32, (slot_count, tok_count), 1)).astype(bf16)
+        return jnp.dot(select, tokens, preferred_element_type=f32).astype(bf16)
+
+    received = [shift(pick(s), "ep", n_ep, s) for s in range(n_ep - 1, 0, -1)][::-1]
+    received = [pick(0)] + received
     rows = jnp.concatenate(received, axis=0)
 
     gate_matrix, up_matrix, down_matrix = expert_gate[0], expert_up[0], expert_down[0]
@@ -99,6 +100,7 @@
 
     square_sum, gate_act, up_act = chunk(0, rows)
     for offset, block in ring_gather(rows, "tp", n_tp):
+        block, square_sum, gate_act, up_act = lax.optimization_barrier((block, square_sum, gate_act, up_act))
         more = chunk(offset, block)
         square_sum, gate_act, up_act = square_sum + more[0], gate_act + more[1], up_act + more[2]
     row_scale = (lax.rsqrt(square_sum / model_width + NORM_EPS) / PRESCALE)[:, None]
@@ -125,8 +127,14 @@
     )
     own_sum = jnp.sum(mixed * mixed, axis=1)
     out_sum = own_sum
-    for s in range(1, n_tp):
-        out_sum = out_sum + shift(own_sum, "tp", n_tp, s)
+    if n_tp & (n_tp - 1) == 0:
+        bit = 1
+        while bit < n_tp:
+            out_sum = out_sum + lax.ppermute(out_sum, "tp", [(i, i ^ bit) for i in range(n_tp)])
+            bit *= 2
+    else:
+        for s in range(1, n_tp):
+            out_sum = out_sum + shift(own_sum, "tp", n_tp, s)
     out_scale = lax.rsqrt(out_sum / model_width + NORM_EPS)[:, None]
     return (mixed * out_scale * out_gain).astype(bf16)
 

time: 91.1 us -> 96.5 us (1.059)
  waiting for transfers between devices: 47.8 us -> 52.3 us
  matrix products: 13.1 us -> 14.3 us
  starting transfers between devices: 25 us -> 23.8 us
    ppermute x0 -> x2, waiting for transfers between devices: none -> 6.38 us  [shards(): lax.ppermute(out_sum, 'tp', [(i, i ^ bit) for i in range(n_tp)])]
    ppermute x17 -> x16, starting transfers between devices: 25 us -> 22 us  [shift(): return lax.ppermute(value, axis, [(i, (i + step) % n) for i in range(n)])]
    ppermute x17 -> x16, waiting for transfers between devices: 47.8 us -> 45.9 us  [shift(): return lax.ppermute(value, axis, [(i, (i + step) % n) for i in range(n)])]
    dot_general x4, matrix products: 5.12 us -> 3.34 us  [chunk(): jnp.dot(scaled, up_rows, preferred_element_type=f32)]
    ppermute x0 -> x2, starting transfers between devices: none -> 1.75 us  [shards(): lax.ppermute(out_sum, 'tp', [(i, i ^ bit) for i in range(n_tp)])]
    dot_general x1 -> x4, matrix products: 1.7 us -> 3.43 us  [pick(): return jnp.dot(select, tokens, preferred_element_type=f32).astype(bf16)]
    dot_general x4, matrix products: 3.51 us -> 4.73 us  [chunk(): jnp.dot(scaled, gate_rows, preferred_element_type=f32)]
  transfers between devices with their start and end apart: 17 -> 18, of which waited for: 15 -> 15; matrix products, arithmetic and copies ran while one was open for 9% -> 11% of each run, Pallas kernels for 0% -> 0%
where the time goes in v3:
time: 96.5 us; the launch traced here: 96.2 us
  waiting for transfers between devices  52.3 us (54%)
  starting transfers between devices  23.8 us (25%)
  matrix products  14.3 us (15%)
  other arithmetic  3.51 us (4%)
  local copies, waits for them, and re-layouts  1.95 us (2%)
    ppermute x16, waiting for transfers between devices, shift(): return lax.ppermute(value, axis, [(i, (i + step) % n) for i in range(n)])  45.9 us
    ppermute x16, starting transfers between devices, shift(): return lax.ppermute(value, axis, [(i, (i + step) % n) for i in range(n)])  22 us
    ppermute x2, waiting for transfers between devices, shards(): lax.ppermute(out_sum, 'tp', [(i, i ^ bit) for i in range(n_tp)])  6.38 us
    dot_general x4, matrix products, chunk(): jnp.dot(scaled, gate_rows, preferred_element_type=f32)  4.73 us
    dot_general x4, matrix products, pick(): return jnp.dot(select, tokens, preferred_element_type=f32).astype(bf16)  3.43 us
    dot_general x4, matrix products, chunk(): jnp.dot(scaled, up_rows, preferred_element_type=f32)  3.34 us
  transfers between devices with their start and end apart: 18, of which 15 were waited for; matrix products, arithmetic and copies ran while one was open for 11% of the time, Pallas kernels for 0%

profile of v3, /device:TPU:0, one launch (start us, length us, event | category | flops | bytes accessed | tf_op | source)
XLA Modules:
  0.0 96.2 jit_solution(360381740011671146)
XLA Ops:
  0.0 0.8 pad_add_fusion
  0.8 1.4 %convolution_convert_fusion.2 = bf16[48,1024]{1,0:T(8,128)(2,1)S(1)} fusion(bf16[384,1024]{1,0:T(8,128)(2,1)} %param.8, s32[48]{0:T(128)S(1)} %get-tuple-element.46), kind=kOutput, calls=%fused_computation.42 | convolution fusion | flops 37816320 | bytes 884928 | tf_op jit(solution)/shard_map/dot_general | solution.py:76
  2.3 0.5 collective-permute-start
  2.8 1.4 %convolution_convert_fusion.1 = bf16[48,1024]{1,0:T(8,128)(2,1)S(1)} fusion(bf16[384,1024]{1,0:T(8,128)(2,1)} %param.8, s32[48]{0:T(128)S(1)} %get-tuple-element.45), kind=kOutput, calls=%fused_computation.41 | convolution fusion | flops 37816320 | bytes 884928 | tf_op jit(solution)/shard_map/dot_general | solution.py:76
  4.2 2.6 %collective-permute-start.1 = (bf16[48,1024]{1,0:T(8,128)(2,1)S(1)}, bf16[48,1024]{1,0:T(8,128)(2,1)S(1)}, u32[]{:S(2)}, u32[]{:S(2)}) collective-permute-start(bf16[48,1024]{1,0:T(8,128)(2,1)S(1)} %convolution_convert_fusion.1), channel_id=1, source_target_pairs={{0,8},{4,12},{8,0},{12,4},{1,9},{5,13},{9,1},{13,5},{2,10},{6,14},... | collective-permute-start | bytes 294920 | tf_op jit(solution)/shard_map/ppermute | solution.py:11
  6.8 0.3 convolution_convert_fusion
  7.1 1.5 %collective-permute-start.2 = (bf16[48,1024]{1,0:T(8,128)(2,1)S(1)}, bf16[48,1024]{1,0:T(8,128)(2,1)S(1)}, u32[]{:S(2)}, u32[]{:S(2)}) collective-permute-start(bf16[48,1024]{1,0:T(8,128)(2,1)S(1)} %convolution_convert_fusion), channel_id=1, source_target_pairs={{0,12},{4,0},{8,4},{12,8},{1,13},{5,1},{9,5},{13,9},{2,14},{6,2},{... | collective-permute-start | bytes 294920 | tf_op jit(solution)/shard_map/ppermute | solution.py:11
  9.1 0.3 collective-permute-done.1
  9.4 1.4 %collective-permute-done.2 = bf16[48,1024]{1,0:T(8,128)(2,1)S(1)} collective-permute-done((bf16[48,1024]{1,0:T(8,128)(2,1)S(1)}, bf16[48,1024]{1,0:T(8,128)(2,1)S(1)}, u32[]{:S(2)}, u32[]{:S(2)}) %collective-permute-start.2) | collective-permute-done | bytes 98336 | tf_op jit(solution)/shard_map/ppermute | solution.py:11
  11.0 3.6 %collective-permute-start.5 = (bf16[192,1024]{1,0:T(8,128)(2,1)S(1)}, bf16[192,1024]{1,0:T(8,128)(2,1)S(1)}, u32[]{:S(2)}, u32[]{:S(2)}) collective-permute-start(bf16[192,1024]{1,0:T(8,128)(2,1)S(1)} %get-tuple-element.30), channel_id=1, source_target_pairs={{0,3},{1,0},{2,1},{3,2},{4,7},{5,4},{6,5},{7,6},{8,11},{9,8},{10,9... | collective-permute-start | bytes 1179656 | tf_op jit(solution)/shard_map/ppermute | solution.py:11
  14.7 1.9 %fusion.22 = f32[192,768]{1,0:T(8,128)S(1)} fusion(bf16[1,4096,768]{2,1,0:T(8,128)(2,1)} %param.13, s32[]{:T(128)S(6)} %select_n.62, bf16[192,1024]{1,0:T(8,128)(2,1)S(1)} %get-tuple-element.30, f32[1024]{0:T(1024)S(1)} %get-tuple-element.41), kind=kOutput, calls=%fused_computation.22 | convolution fusion | flops 302579712 | bytes 2560004 | tf_op jit(solution)/shard_map/dot_general | solution.py:97
  16.5 1.9 %fusion.20 = f32[192,768]{1,0:T(8,128)S(1)} fusion(bf16[1,4096,768]{2,1,0:T(8,128)(2,1)} %param.14, s32[]{:T(128)S(6)} %select_n.62, bf16[192,1024]{1,0:T(8,128)(2,1)S(1)} %get-tuple-element.30, f32[1024]{0:T(1024)S(1)} %get-tuple-element.41), kind=kOutput, calls=%fused_computation.20 | convolution fusion | flops 302579712 | bytes 2560004 | tf_op jit(solution)/shard_map/dot_general | solution.py:98
  18.4 15.0 %collective-permute-done.3 = bf16[192,1024]{1,0:T(8,128)(2,1)S(1)} collective-permute-done((bf16[192,1024]{1,0:T(8,128)(2,1)S(1)}, bf16[192,1024]{1,0:T(8,128)(2,1)S(1)}, u32[]{:S(2)}, u32[]{:S(2)}) %collective-permute-start.3) | collective-permute-done | bytes 393248 | tf_op jit(solution)/shard_map/ppermute | solution.py:11
  33.5 0.5 fusion.16
  34.1 1.9 %fusion.18 = f32[192,768]{1,0:T(8,128)S(1)} fusion(bf16[1,4096,768]{2,1,0:T(8,128)(2,1)} %param.13, s32[]{:T(128)S(6)} %select_n.64, bf16[192,1024]{1,0:T(8,128)(2,1)S(1)} %collective-permute-done.3, f32[1024]{0:T(1024)S(1)} %get-tuple-element.40), kind=kOutput, calls=%fused_computation.18 | convolution fusion | flops 302579712 | bytes 2560004 | tf_op jit(solution)/shard_map/dot_general | solution.py:97
  36.0 1.9 %collective-permute-start.6 = (bf16[96,1024]{1,0:T(8,128)(2,1)S(1)}, bf16[96,1024]{1,0:T(8,128)(2,1)S(1)}, u32[]{:S(2)}, u32[]{:S(2)}) collective-permute-start(bf16[96,1024]{1,0:T(8,128)(2,1)S(1)} %slice.85), channel_id=1, source_target_pairs={{0,3},{1,0},{2,1},{3,2},{4,7},{5,4},{6,5},{7,6},{8,11},{9,8},{10,9... | collective-permute-start | bytes 589832 | tf_op jit(solution)/shard_map/ppermute | solution.py:11
  38.5 0.5 fusion.12
  39.1 1.3 %slice-done.1 = s8[4194304]{0:T(1024)(128)(4,1)S(1)} async-done(((s8[6291456]{0:T(1024)(128)(4,1)}), s8[4194304]{0:T(1024)(128)(4,1)S(1)}, s32[]{:S(2)}) %slice-start.1) | async-done | bytes 4194328
  40.4 0.5 fusion.14
  40.9 3.1 %collective-permute-done.6 = bf16[96,1024]{1,0:T(8,128)(2,1)S(1)} collective-permute-done((bf16[96,1024]{1,0:T(8,128)(2,1)S(1)}, bf16[96,1024]{1,0:T(8,128)(2,1)S(1)}, u32[]{:S(2)}, u32[]{:S(2)}) %collective-permute-start.6) | collective-permute-done | bytes 196640 | tf_op jit(solution)/shard_map/ppermute | solution.py:11
  44.0 3.3 %collective-permute-done.4 = bf16[96,1024]{1,0:T(8,128)(2,1)S(1)} collective-permute-done((bf16[96,1024]{1,0:T(8,128)(2,1)S(1)}, bf16[96,1024]{1,0:T(8,128)(2,1)S(1)}, u32[]{:S(2)}, u32[]{:S(2)}) %collective-permute-start.4) | collective-permute-done | bytes 196640 | tf_op jit(solution)/shard_map/ppermute | solution.py:11
  47.5 0.5 fusion.8
  48.0 0.5 fusion.10
  49.1 0.5 fusion.36
  49.6 0.5 fusion
  50.1 1.6 %collective-permute-start.7 = (bf16[96,1024]{1,0:T(8,128)(2,1)S(1)}, bf16[96,1024]{1,0:T(8,128)(2,1)S(1)}, u32[]{:S(2)}, u32[]{:S(2)}) collective-permute-start(bf16[96,1024]{1,0:T(8,128)(2,1)S(1)} %get-tuple-element.33), channel_id=1, source_target_pairs={{0,1},{1,2},{2,3},{3,0},{4,5},{5,6},{6,7},{7,4},{8,9},{9,10},{10,1... | collective-permute-start | bytes 589832 | tf_op jit(solution)/shard_map/ppermute | solution.py:11
  51.7 2.3 %collective-permute-start.12 = (bf16[96,1024]{1,0:T(8,128)(2,1)S(1)}, bf16[96,1024]{1,0:T(8,128)(2,1)S(1)}, u32[]{:S(2)}, u32[]{:S(2)}) collective-permute-start(bf16[96,1024]{1,0:T(8,128)(2,1)S(1)} %get-tuple-element.34), channel_id=1, source_target_pairs={{0,3},{1,0},{2,1},{3,2},{4,7},{5,4},{6,5},{7,6},{8,11},{9,8},{10,9... | collective-permute-start | bytes 589832 | tf_op jit(solution)/shard_map/ppermute | solution.py:11
  54.0 0.7 collective-permute-start.9
  54.8 0.5 fusion.4
  55.3 1.4 %collective-permute-start.11 = (bf16[96,1024]{1,0:T(8,128)(2,1)S(1)}, bf16[96,1024]{1,0:T(8,128)(2,1)S(1)}, u32[]{:S(2)}, u32[]{:S(2)}) collective-permute-start(bf16[96,1024]{1,0:T(8,128)(2,1)S(1)} %slice.120), channel_id=1, source_target_pairs={{0,1},{1,2},{2,3},{3,0},{4,5},{5,6},{6,7},{7,4},{8,9},{9,10},{10,1... | collective-permute-start | bytes 589832 | tf_op jit(solution)/shard_map/ppermute | solution.py:11
  56.7 5.4 %collective-permute-done.12 = bf16[96,1024]{1,0:T(8,128)(2,1)S(1)} collective-permute-done((bf16[96,1024]{1,0:T(8,128)(2,1)S(1)}, bf16[96,1024]{1,0:T(8,128)(2,1)S(1)}, u32[]{:S(2)}, u32[]{:S(2)}) %collective-permute-start.12) | collective-permute-done | bytes 196640 | tf_op jit(solution)/shard_map/ppermute | solution.py:11
  62.1 3.5 %collective-permute-start.13 = (bf16[96,1024]{1,0:T(8,128)(2,1)S(1)}, bf16[96,1024]{1,0:T(8,128)(2,1)S(1)}, u32[]{:S(2)}, u32[]{:S(2)}) collective-permute-start(bf16[96,1024]{1,0:T(8,128)(2,1)S(1)} %fusion.48), channel_id=1, source_target_pairs={{0,3},{1,0},{2,1},{3,2},{4,7},{5,4},{6,5},{7,6},{8,11},{9,8},{10,9... | collective-permute-start | bytes 589832 | tf_op jit(solution)/shard_map/ppermute | solution.py:11
  65.7 0.6 collective-permute-start.8
  66.3 0.5 fusion.6
  66.8 1.4 %collective-permute-done.9 = bf16[96,1024]{1,0:T(8,128)(2,1)S(1)} collective-permute-done((bf16[96,1024]{1,0:T(8,128)(2,1)S(1)}, bf16[96,1024]{1,0:T(8,128)(2,1)S(1)}, u32[]{:S(2)}, u32[]{:S(2)}) %collective-permute-start.9) | collective-permute-done | bytes 196640 | tf_op jit(solution)/shard_map/ppermute | solution.py:11
  68.3 4.1 %collective-permute-done.11 = bf16[96,1024]{1,0:T(8,128)(2,1)S(1)} collective-permute-done((bf16[96,1024]{1,0:T(8,128)(2,1)S(1)}, bf16[96,1024]{1,0:T(8,128)(2,1)S(1)}, u32[]{:S(2)}, u32[]{:S(2)}) %collective-permute-start.11) | collective-permute-done | bytes 196640 | tf_op jit(solution)/shard_map/ppermute | solution.py:11
  72.4 4.2 %collective-permute-done.13 = bf16[96,1024]{1,0:T(8,128)(2,1)S(1)} collective-permute-done((bf16[96,1024]{1,0:T(8,128)(2,1)S(1)}, bf16[96,1024]{1,0:T(8,128)(2,1)S(1)}, u32[]{:S(2)}, u32[]{:S(2)}) %collective-permute-start.13) | collective-permute-done | bytes 196640 | tf_op jit(solution)/shard_map/ppermute | solution.py:11
  76.6 2.3 %collective-permute-done.8 = bf16[96,1024]{1,0:T(8,128)(2,1)S(1)} collective-permute-done((bf16[96,1024]{1,0:T(8,128)(2,1)S(1)}, bf16[96,1024]{1,0:T(8,128)(2,1)S(1)}, u32[]{:S(2)}, u32[]{:S(2)}) %collective-permute-start.8) | collective-permute-done | bytes 196640 | tf_op jit(solution)/shard_map/ppermute | solution.py:11
  79.1 1.2 %collective-permute-start.14 = (bf16[48,1024]{1,0:T(8,128)(2,1)S(1)}, bf16[48,1024]{1,0:T(8,128)(2,1)S(1)}, u32[]{:S(2)}, u32[]{:S(2)}) collective-permute-start(bf16[48,1024]{1,0:T(8,128)(2,1)S(1)} %get-tuple-element.37), channel_id=1, source_target_pairs={{0,8},{4,12},{8,0},{12,4},{1,9},{5,13},{9,1},{13,5},{2,10},{6,14},... | collective-permute-start | bytes 294920 | tf_op jit(solution)/shard_map/ppermute | solution.py:11
  80.6 0.9 collective-permute-done.10
  81.5 3.9 %collective-permute-done.14 = bf16[48,1024]{1,0:T(8,128)(2,1)S(1)} collective-permute-done((bf16[48,1024]{1,0:T(8,128)(2,1)S(1)}, bf16[48,1024]{1,0:T(8,128)(2,1)S(1)}, u32[]{:S(2)}, u32[]{:S(2)}) %collective-permute-start.14) | collective-permute-done | bytes 98336 | tf_op jit(solution)/shard_map/ppermute | solution.py:11
  85.5 0.5 collective-permute-done.15
  86.0 0.4 fusion.62
  86.4 0.5 multiply_reduce_fusion
  87.0 3.5 %collective-permute-done.16 = f32[384]{0:T(512)S(1)} collective-permute-done((f32[384]{0:T(512)S(1)}, f32[384]{0:T(512)S(1)}, u32[]{:S(2)}, u32[]{:S(2)}) %collective-permute-start.16) | collective-permute-done | bytes 1568 | tf_op jit(solution)/shard_map/ppermute | solution.py:133
  90.5 1.6 %collective-permute-start.17 = (f32[384]{0:T(512)S(1)}, f32[384]{0:T(512)S(1)}, u32[]{:S(2)}, u32[]{:S(2)}) collective-permute-start(f32[384]{0:T(512)S(1)} %add.162), channel_id=1, source_target_pairs={{0,2},{1,3},{2,0},{3,1},{4,6},{5,7},{6,4},{7,5},{8,10},{9,11},{10,... | collective-permute-start | bytes 4616 | tf_op jit(solution)/shard_map/ppermute | solution.py:133
  92.1 2.9 %collective-permute-done.17 = f32[384]{0:T(512)S(1)} collective-permute-done((f32[384]{0:T(512)S(1)}, f32[384]{0:T(512)S(1)}, u32[]{:S(2)}, u32[]{:S(2)}) %collective-permute-start.17) | collective-permute-done | bytes 1568 | tf_op jit(solution)/shard_map/ppermute | solution.py:133
  95.0 1.2 %multiply_convert_fusion = bf16[384,1024]{1,0:T(8,128)(2,1)} fusion(f32[1024]{0:T(1024)S(1)} %copy-done.3, f32[384]{0:T(512)S(1)} %add_rsqrt_fusion, f32[384,1024]{1,0:T(8,128)S(1)} %get-tuple-element.48, f32[384,1024]{1,0:T(8,128)S(1)} %fusion.62, bf16[384,1024]{1,0:T(8,128)(2,1)S(1)} %copy-done), kind=kLoop, calls=%fused_computation.24 | loop fusion | flops 2359296 | bytes 4724224 | tf_op jit(solution)/shard_map/convert_element_type | solution.py:139
  (60 shorter events, 3.1 us)
Async XLA Ops:
  0.0 6.8 %copy-start = (bf16[384,1024]{1,0:T(8,128)(2,1)S(1)}, bf16[384,1024]{1,0:T(8,128)(2,1)}, u32[]{:S(2)}) copy-start(bf16[384,1024]{1,0:T(8,128)(2,1)} %param.8) | copy-start | bytes 2359300
  2.2 6.8 %copy-start.2 = (f32[4096]{0:T(1024)S(1)}, f32[4096]{0:T(1024)}, u32[]{:S(2)}) copy-start(f32[4096]{0:T(1024)} %param.9) | copy-start | bytes 49156
  2.2 6.8 %copy-start.4 = (f32[1,4,48]{2,1,0:T(4,128)S(1)}, f32[1,4,48]{2,1,0:T(4,128)}, u32[]{:S(2)}) copy-start(f32[1,4,48]{2,1,0:T(4,128)} %param.12) | copy-start | bytes 2308
  2.3 6.8 %collective-permute-start = (bf16[48,1024]{1,0:T(8,128)(2,1)S(1)}, bf16[48,1024]{1,0:T(8,128)(2,1)S(1)}, u32[]{:S(2)}, u32[]{:S(2)}) collective-permute-start(bf16[48,1024]{1,0:T(8,128)(2,1)S(1)} %convolution_convert_fusion.2), channel_id=1, source_target_pairs={{0,4},{4,8},{8,12},{12,0},{1,5},{5,9},{9,13},{13,1},{2,6},{6,10},{... | collective-permute-start | bytes 294920 | tf_op jit(solution)/shard_map/ppermute | solution.py:11
  4.2 5.2 %collective-permute-start.1 = (bf16[48,1024]{1,0:T(8,128)(2,1)S(1)}, bf16[48,1024]{1,0:T(8,128)(2,1)S(1)}, u32[]{:S(2)}, u32[]{:S(2)}) collective-permute-start(bf16[48,1024]{1,0:T(8,128)(2,1)S(1)} %convolution_convert_fusion.1), channel_id=1, source_target_pairs={{0,8},{4,12},{8,0},{12,4},{1,9},{5,13},{9,1},{13,5},{2,10},{6,14},... | collective-permute-start | bytes 294920 | tf_op jit(solution)/shard_map/ppermute | solution.py:11
  7.1 3.7 %collective-permute-start.2 = (bf16[48,1024]{1,0:T(8,128)(2,1)S(1)}, bf16[48,1024]{1,0:T(8,128)(2,1)S(1)}, u32[]{:S(2)}, u32[]{:S(2)}) collective-permute-start(bf16[48,1024]{1,0:T(8,128)(2,1)S(1)} %convolution_convert_fusion), channel_id=1, source_target_pairs={{0,12},{4,0},{8,4},{12,8},{1,13},{5,1},{9,5},{13,9},{2,14},{6,2},{... | collective-permute-start | bytes 294920 | tf_op jit(solution)/shard_map/ppermute | solution.py:11
  10.8 22.6 %copy-start.1 = (bf16[1,4096,768]{2,1,0:T(8,128)(2,1)S(1)}, bf16[1,4096,768]{2,1,0:T(8,128)(2,1)}, u32[]{:S(2)}) copy-start(bf16[1,4096,768]{2,1,0:T(8,128)(2,1)} %param.14) | copy-start | bytes 18874372
  11.0 25.0 %collective-permute-start.5 = (bf16[192,1024]{1,0:T(8,128)(2,1)S(1)}, bf16[192,1024]{1,0:T(8,128)(2,1)S(1)}, u32[]{:S(2)}, u32[]{:S(2)}) collective-permute-start(bf16[192,1024]{1,0:T(8,128)(2,1)S(1)} %get-tuple-element.30), channel_id=1, source_target_pairs={{0,3},{1,0},{2,1},{3,2},{4,7},{5,4},{6,5},{7,6},{8,11},{9,8},{10,9... | collective-permute-start | bytes 1179656 | tf_op jit(solution)/shard_map/ppermute | solution.py:11
  14.7 18.8 %collective-permute-start.3 = (bf16[192,1024]{1,0:T(8,128)(2,1)S(1)}, bf16[192,1024]{1,0:T(8,128)(2,1)S(1)}, u32[]{:S(2)}, u32[]{:S(2)}) collective-permute-start(bf16[192,1024]{1,0:T(8,128)(2,1)S(1)} %get-tuple-element.30), channel_id=1, source_target_pairs={{0,1},{1,2},{2,3},{3,0},{4,5},{5,6},{6,7},{7,4},{8,9},{9,10},{10,1... | collective-permute-start | bytes 1179656 | tf_op jit(solution)/shard_map/ppermute | solution.py:11
  33.4 5.6 %slice-start = ((s8[6291456]{0:T(1024)(128)(4,1)}), s8[2097152]{0:T(1024)(128)(4,1)S(1)}, s32[]{:S(2)}) async-start(s8[6291456]{0:T(1024)(128)(4,1)} %bitcast.56), calls=%async_computation | async-start | bytes 4194304
  36.0 8.0 %collective-permute-start.6 = (bf16[96,1024]{1,0:T(8,128)(2,1)S(1)}, bf16[96,1024]{1,0:T(8,128)(2,1)S(1)}, u32[]{:S(2)}, u32[]{:S(2)}) collective-permute-start(bf16[96,1024]{1,0:T(8,128)(2,1)S(1)} %slice.85), channel_id=1, source_target_pairs={{0,3},{1,0},{2,1},{3,2},{4,7},{5,4},{6,5},{7,6},{8,11},{9,8},{10,9... | collective-permute-start | bytes 589832 | tf_op jit(solution)/shard_map/ppermute | solution.py:11
  37.9 9.4 %collective-permute-start.4 = (bf16[96,1024]{1,0:T(8,128)(2,1)S(1)}, bf16[96,1024]{1,0:T(8,128)(2,1)S(1)}, u32[]{:S(2)}, u32[]{:S(2)}) collective-permute-start(bf16[96,1024]{1,0:T(8,128)(2,1)S(1)} %slice.84), channel_id=1, source_target_pairs={{0,1},{1,2},{2,3},{3,0},{4,5},{5,6},{6,7},{7,4},{8,9},{9,10},{10,1... | collective-permute-start | bytes 589832 | tf_op jit(solution)/shard_map/ppermute | solution.py:11
  38.2 2.2 %slice-start.1 = ((s8[6291456]{0:T(1024)(128)(4,1)}), s8[4194304]{0:T(1024)(128)(4,1)S(1)}, s32[]{:S(2)}) async-start(s8[6291456]{0:T(1024)(128)(4,1)} %bitcast.56), calls=%async_computation.1 | async-start | bytes 8388608
  40.9 7.9 %slice-start.2 = ((s8[6291456]{0:T(1024)(128)(4,1)}), s8[4194304]{0:T(1024)(128)(4,1)S(1)}, s32[]{:S(2)}) async-start(s8[6291456]{0:T(1024)(128)(4,1)} %bitcast.58), calls=%async_computation.2 | async-start | bytes 8388608
  47.5 1.6 %slice-start.3 = ((s8[6291456]{0:T(1024)(128)(4,1)}), s8[2097152]{0:T(1024)(128)(4,1)S(1)}, s32[]{:S(2)}) async-start(s8[6291456]{0:T(1024)(128)(4,1)} %bitcast.58), calls=%async_computation.3 | async-start | bytes 4194304
  50.1 15.6 %collective-permute-start.7 = (bf16[96,1024]{1,0:T(8,128)(2,1)S(1)}, bf16[96,1024]{1,0:T(8,128)(2,1)S(1)}, u32[]{:S(2)}, u32[]{:S(2)}) collective-permute-start(bf16[96,1024]{1,0:T(8,128)(2,1)S(1)} %get-tuple-element.33), channel_id=1, source_target_pairs={{0,1},{1,2},{2,3},{3,0},{4,5},{5,6},{6,7},{7,4},{8,9},{9,10},{10,1... | collective-permute-start | bytes 589832 | tf_op jit(solution)/shard_map/ppermute | solution.py:11
  51.7 10.4 %collective-permute-start.12 = (bf16[96,1024]{1,0:T(8,128)(2,1)S(1)}, bf16[96,1024]{1,0:T(8,128)(2,1)S(1)}, u32[]{:S(2)}, u32[]{:S(2)}) collective-permute-start(bf16[96,1024]{1,0:T(8,128)(2,1)S(1)} %get-tuple-element.34), channel_id=1, source_target_pairs={{0,3},{1,0},{2,1},{3,2},{4,7},{5,4},{6,5},{7,6},{8,11},{9,8},{10,9... | collective-permute-start | bytes 589832 | tf_op jit(solution)/shard_map/ppermute | solution.py:11
  54.0 14.3 %collective-permute-start.9 = (bf16[96,1024]{1,0:T(8,128)(2,1)S(1)}, bf16[96,1024]{1,0:T(8,128)(2,1)S(1)}, u32[]{:S(2)}, u32[]{:S(2)}) collective-permute-start(bf16[96,1024]{1,0:T(8,128)(2,1)S(1)} %slice.121), channel_id=1, source_target_pairs={{0,3},{1,0},{2,1},{3,2},{4,7},{5,4},{6,5},{7,6},{8,11},{9,8},{10,9... | collective-permute-start | bytes 589832 | tf_op jit(solution)/shard_map/ppermute | solution.py:11
  55.3 17.1 %collective-permute-start.11 = (bf16[96,1024]{1,0:T(8,128)(2,1)S(1)}, bf16[96,1024]{1,0:T(8,128)(2,1)S(1)}, u32[]{:S(2)}, u32[]{:S(2)}) collective-permute-start(bf16[96,1024]{1,0:T(8,128)(2,1)S(1)} %slice.120), channel_id=1, source_target_pairs={{0,1},{1,2},{2,3},{3,0},{4,5},{5,6},{6,7},{7,4},{8,9},{9,10},{10,1... | collective-permute-start | bytes 589832 | tf_op jit(solution)/shard_map/ppermute | solution.py:11
  62.1 14.5 %collective-permute-start.13 = (bf16[96,1024]{1,0:T(8,128)(2,1)S(1)}, bf16[96,1024]{1,0:T(8,128)(2,1)S(1)}, u32[]{:S(2)}, u32[]{:S(2)}) collective-permute-start(bf16[96,1024]{1,0:T(8,128)(2,1)S(1)} %fusion.48), channel_id=1, source_target_pairs={{0,3},{1,0},{2,1},{3,2},{4,7},{5,4},{6,5},{7,6},{8,11},{9,8},{10,9... | collective-permute-start | bytes 589832 | tf_op jit(solution)/shard_map/ppermute | solution.py:11
  65.7 13.1 %collective-permute-start.8 = (bf16[96,1024]{1,0:T(8,128)(2,1)S(1)}, bf16[96,1024]{1,0:T(8,128)(2,1)S(1)}, u32[]{:S(2)}, u32[]{:S(2)}) collective-permute-start(bf16[96,1024]{1,0:T(8,128)(2,1)S(1)} %fusion.51), channel_id=1, source_target_pairs={{0,1},{1,2},{2,3},{3,0},{4,5},{5,6},{6,7},{7,4},{8,9},{9,10},{10,1... | collective-permute-start | bytes 589832 | tf_op jit(solution)/shard_map/ppermute | solution.py:11
  79.0 2.5 %collective-permute-start.10 = (bf16[48,1024]{1,0:T(8,128)(2,1)S(1)}, bf16[48,1024]{1,0:T(8,128)(2,1)S(1)}, u32[]{:S(2)}, u32[]{:S(2)}) collective-permute-start(bf16[48,1024]{1,0:T(8,128)(2,1)S(1)} %get-tuple-element.36), channel_id=1, source_target_pairs={{0,12},{4,0},{8,4},{12,8},{1,13},{5,1},{9,5},{13,9},{2,14},{6,2},{... | collective-permute-start | bytes 294920 | tf_op jit(solution)/shard_map/ppermute | solution.py:11
  79.1 6.3 %collective-permute-start.14 = (bf16[48,1024]{1,0:T(8,128)(2,1)S(1)}, bf16[48,1024]{1,0:T(8,128)(2,1)S(1)}, u32[]{:S(2)}, u32[]{:S(2)}) collective-permute-start(bf16[48,1024]{1,0:T(8,128)(2,1)S(1)} %get-tuple-element.37), channel_id=1, source_target_pairs={{0,8},{4,12},{8,0},{12,4},{1,9},{5,13},{9,1},{13,5},{2,10},{6,14},... | collective-permute-start | bytes 294920 | tf_op jit(solution)/shard_map/ppermute | solution.py:11
  80.3 5.7 %collective-permute-start.15 = (bf16[48,1024]{1,0:T(8,128)(2,1)S(1)}, bf16[48,1024]{1,0:T(8,128)(2,1)S(1)}, u32[]{:S(2)}, u32[]{:S(2)}) collective-permute-start(bf16[48,1024]{1,0:T(8,128)(2,1)S(1)} %get-tuple-element.38), channel_id=1, source_target_pairs={{0,4},{4,8},{8,12},{12,0},{1,5},{5,9},{9,13},{13,1},{2,6},{6,10},{... | collective-permute-start | bytes 294920 | tf_op jit(solution)/shard_map/ppermute | solution.py:11
  86.4 8.7 %copy-start.3 = (f32[1024]{0:T(1024)S(1)}, f32[1024]{0:T(1024)}, u32[]{:S(2)}) copy-start(f32[1024]{0:T(1024)} %param.10) | copy-start | bytes 12292
  86.9 3.6 %collective-permute-start.16 = (f32[384]{0:T(512)S(1)}, f32[384]{0:T(512)S(1)}, u32[]{:S(2)}, u32[]{:S(2)}) collective-permute-start(f32[384]{0:T(512)S(1)} %get-tuple-element.47), channel_id=1, source_target_pairs={{0,1},{1,0},{2,3},{3,2},{4,5},{5,4},{6,7},{7,6},{8,9},{9,8},{10,11... | collective-permute-start | bytes 4616 | tf_op jit(solution)/shard_map/ppermute | solution.py:133
  90.5 4.5 %collective-permute-start.17 = (f32[384]{0:T(512)S(1)}, f32[384]{0:T(512)S(1)}, u32[]{:S(2)}, u32[]{:S(2)}) collective-permute-start(f32[384]{0:T(512)S(1)} %add.162), channel_id=1, source_target_pairs={{0,2},{1,3},{2,0},{3,1},{4,6},{5,7},{6,4},{7,5},{8,10},{9,11},{10,... | collective-permute-start | bytes 4616 | tf_op jit(solution)/shard_map/ppermute | solution.py:133

commit v4 on v1

--- a/solution.py
+++ b/solution.py
@@ -99,6 +99,8 @@
 
     square_sum, gate_act, up_act = chunk(0, rows)
     for offset, block in ring_gather(rows, "tp", n_tp):
+        if 2 * offset == n_tp:
+            block, square_sum, gate_act, up_act = lax.optimization_barrier((block, square_sum, gate_act, up_act))
         more = chunk(offset, block)
         square_sum, gate_act, up_act = square_sum + more[0], gate_act + more[1], up_act + more[2]
     row_scale = (lax.rsqrt(square_sum / model_width + NORM_EPS) / PRESCALE)[:, None]

time: 91.1 us -> 88.7 us (0.974)
  waiting for transfers between devices: 47.8 us -> 46.4 us
    dot_general x4, matrix products: 3.51 us -> 5.23 us  [chunk(): jnp.dot(scaled, gate_rows, preferred_element_type=f32)]
    dot_general x4, matrix products: 5.12 us -> 3.58 us  [chunk(): jnp.dot(scaled, up_rows, preferred_element_type=f32)]
    ppermute x17, waiting for transfers between devices: 47.8 us -> 46.4 us  [shift(): return lax.ppermute(value, axis, [(i, (i + step) % n) for i in range(n)])]
  transfers between devices with their start and end apart: 17 -> 17, of which waited for: 15 -> 12; matrix products, arithmetic and copies ran while one was open for 9% -> 11% of each run, Pallas kernels for 0% -> 0%
where the time goes in v4:
time: 88.7 us; the launch traced here: 88.4 us
  waiting for transfers between devices  46.4 us (52%)
  starting transfers between devices  24.3 us (27%)
  matrix products  13.1 us (15%)
  other arithmetic  3.27 us (4%)
    ppermute x17, waiting for transfers between devices, shift(): return lax.ppermute(value, axis, [(i, (i + step) % n) for i in range(n)])  46.4 us
    ppermute x17, starting transfers between devices, shift(): return lax.ppermute(value, axis, [(i, (i + step) % n) for i in range(n)])  24.3 us
    dot_general x4, matrix products, chunk(): jnp.dot(scaled, gate_rows, preferred_element_type=f32)  5.23 us
    dot_general x4, matrix products, chunk(): jnp.dot(scaled, up_rows, preferred_element_type=f32)  3.58 us
    dot_general x4, matrix products, part(): return jnp.dot(hidden, columns, preferred_element_type=f32)  1.93 us
  transfers between devices with their start and end apart: 17, of which 12 were waited for; matrix products, arithmetic and copies ran while one was open for 11% of the time, Pallas kernels for 0%

profile of v4, /device:TPU:0, one launch (start us, length us, event | category | flops | bytes accessed | tf_op | source)
XLA Modules:
  0.0 88.4 jit_solution(15119501842990848994)
XLA Ops:
  0.0 0.8 pad_add_fusion
  0.9 1.5 %convolution_convert_fusion = bf16[192,1024]{1,0:T(8,128)(2,1)S(1)} fusion(bf16[384,1024]{1,0:T(8,128)(2,1)} %param.8, s32[192]{0:T(256)S(1)} %eq.19), kind=kOutput, calls=%fused_computation.44 | convolution fusion | flops 151265280 | bytes 1180416 | tf_op jit(solution)/shard_map/dot_general | solution.py:73
  2.5 2.5 %collective-permute-start.2 = (bf16[48,1024]{1,0:T(8,128)(2,1)S(1)}, bf16[48,1024]{1,0:T(8,128)(2,1)S(1)}, u32[]{:S(2)}, u32[]{:S(2)}) collective-permute-start(bf16[48,1024]{1,0:T(8,128)(2,1)S(1)} %get-tuple-element.22), channel_id=1, source_target_pairs={{0,12},{4,0},{8,4},{12,8},{1,13},{5,1},{9,5},{13,9},{2,14},{6,2},{... | collective-permute-start | bytes 294920 | tf_op jit(solution)/shard_map/ppermute | solution.py:11
  4.9 0.6 collective-permute-start.1
  5.7 2.3 %collective-permute-done.2 = bf16[48,1024]{1,0:T(8,128)(2,1)S(1)} collective-permute-done((bf16[48,1024]{1,0:T(8,128)(2,1)S(1)}, bf16[48,1024]{1,0:T(8,128)(2,1)S(1)}, u32[]{:S(2)}, u32[]{:S(2)}) %collective-permute-start.2) | collective-permute-done | bytes 98336 | tf_op jit(solution)/shard_map/ppermute | solution.py:11
  8.0 3.0 %collective-permute-done.1 = bf16[48,1024]{1,0:T(8,128)(2,1)S(1)} collective-permute-done((bf16[48,1024]{1,0:T(8,128)(2,1)S(1)}, bf16[48,1024]{1,0:T(8,128)(2,1)S(1)}, u32[]{:S(2)}, u32[]{:S(2)}) %collective-permute-start.1) | collective-permute-done | bytes 98336 | tf_op jit(solution)/shard_map/ppermute | solution.py:11
  11.1 0.2 fusion.51
  11.2 3.8 %collective-permute-start.5 = (bf16[192,1024]{1,0:T(8,128)(2,1)S(1)}, bf16[192,1024]{1,0:T(8,128)(2,1)S(1)}, u32[]{:S(2)}, u32[]{:S(2)}) collective-permute-start(bf16[192,1024]{1,0:T(8,128)(2,1)S(1)} %get-tuple-element.14), channel_id=1, source_target_pairs={{0,3},{1,0},{2,1},{3,2},{4,7},{5,4},{6,5},{7,6},{8,11},{9,8},{10,9... | collective-permute-start | bytes 1179656 | tf_op jit(solution)/shard_map/ppermute | solution.py:11
  15.1 2.0 %fusion.22 = f32[192,768]{1,0:T(8,128)S(1)} fusion(bf16[1,4096,768]{2,1,0:T(8,128)(2,1)} %param.13, s32[]{:T(128)S(6)} %select_n.62, bf16[192,1024]{1,0:T(8,128)(2,1)S(1)} %get-tuple-element.14, f32[1024]{0:T(1024)S(1)} %get-tuple-element.27), kind=kOutput, calls=%fused_computation.22 | convolution fusion | flops 302579712 | bytes 2560004 | tf_op jit(solution)/shard_map/dot_general | solution.py:96
  17.1 2.1 %fusion.16 = f32[192,768]{1,0:T(8,128)S(1)} fusion(bf16[1,4096,768]{2,1,0:T(8,128)(2,1)} %param.14, s32[]{:T(128)S(6)} %select_n.62, bf16[192,1024]{1,0:T(8,128)(2,1)S(1)} %get-tuple-element.14, f32[1024]{0:T(1024)S(1)} %get-tuple-element.27), kind=kOutput, calls=%fused_computation.16 | convolution fusion | flops 302579712 | bytes 2560004 | tf_op jit(solution)/shard_map/dot_general | solution.py:97
  19.2 5.3 %collective-permute-done.5 = bf16[192,1024]{1,0:T(8,128)(2,1)S(1)} collective-permute-done((bf16[192,1024]{1,0:T(8,128)(2,1)S(1)}, bf16[192,1024]{1,0:T(8,128)(2,1)S(1)}, u32[]{:S(2)}, u32[]{:S(2)}) %collective-permute-start.5) | collective-permute-done | bytes 393248 | tf_op jit(solution)/shard_map/ppermute | solution.py:11
  24.6 4.3 %collective-permute-start.6 = (bf16[96,1024]{1,0:T(8,128)(2,1)S(1)}, bf16[96,1024]{1,0:T(8,128)(2,1)S(1)}, u32[]{:S(2)}, u32[]{:S(2)}) collective-permute-start(bf16[96,1024]{1,0:T(8,128)(2,1)S(1)} %slice.71), channel_id=1, source_target_pairs={{0,3},{1,0},{2,1},{3,2},{4,7},{5,4},{6,5},{7,6},{8,11},{9,8},{10,9... | collective-permute-start | bytes 589832 | tf_op jit(solution)/shard_map/ppermute | solution.py:11
  28.9 5.0 %collective-permute-done.3 = bf16[192,1024]{1,0:T(8,128)(2,1)S(1)} collective-permute-done((bf16[192,1024]{1,0:T(8,128)(2,1)S(1)}, bf16[192,1024]{1,0:T(8,128)(2,1)S(1)}, u32[]{:S(2)}, u32[]{:S(2)}) %collective-permute-start.3) | collective-permute-done | bytes 393248 | tf_op jit(solution)/shard_map/ppermute | solution.py:11
  34.0 1.6 %collective-permute-start.4 = (bf16[96,1024]{1,0:T(8,128)(2,1)S(1)}, bf16[96,1024]{1,0:T(8,128)(2,1)S(1)}, u32[]{:S(2)}, u32[]{:S(2)}) collective-permute-start(bf16[96,1024]{1,0:T(8,128)(2,1)S(1)} %slice.70), channel_id=1, source_target_pairs={{0,1},{1,2},{2,3},{3,0},{4,5},{5,6},{6,7},{7,4},{8,9},{9,10},{10,1... | collective-permute-start | bytes 589832 | tf_op jit(solution)/shard_map/ppermute | solution.py:11
  35.7 0.2 fusion.53
  35.9 0.5 fusion.12
  36.4 2.2 %fusion.18 = f32[192,768]{1,0:T(8,128)S(1)} fusion(bf16[1,4096,768]{2,1,0:T(8,128)(2,1)} %param.13, s32[]{:T(128)S(6)} %select_n.66, bf16[192,1024]{1,0:T(8,128)(2,1)S(1)} %collective-permute-done.5, f32[1024]{0:T(1024)S(1)} %get-tuple-element.28), kind=kOutput, calls=%fused_computation.18 | convolution fusion | flops 302579712 | bytes 2560004 | tf_op jit(solution)/shard_map/dot_general | solution.py:96
  38.6 0.2 copy-done.2
  38.8 0.5 fusion.39
  39.3 0.5 fusion.45
  39.8 1.7 %collective-permute-done.4 = bf16[96,1024]{1,0:T(8,128)(2,1)S(1)} collective-permute-done((bf16[96,1024]{1,0:T(8,128)(2,1)S(1)}, bf16[96,1024]{1,0:T(8,128)(2,1)S(1)}, u32[]{:S(2)}, u32[]{:S(2)}) %collective-permute-start.4) | collective-permute-done | bytes 196640 | tf_op jit(solution)/shard_map/ppermute | solution.py:11
  41.5 0.2 fusion.58
  41.7 0.5 fusion.8
  42.2 0.5 fusion.10
  42.7 0.3 multiply_convert_fusion.1
  43.0 0.3 slice-done.1
  43.3 0.5 fusion.48
  43.8 0.5 fusion
  44.3 0.7 collective-permute-start.7
  45.0 3.1 %collective-permute-start.9 = (bf16[96,1024]{1,0:T(8,128)(2,1)S(1)}, bf16[96,1024]{1,0:T(8,128)(2,1)S(1)}, u32[]{:S(2)}, u32[]{:S(2)}) collective-permute-start(bf16[96,1024]{1,0:T(8,128)(2,1)S(1)} %get-tuple-element.20), channel_id=1, source_target_pairs={{0,3},{1,0},{2,1},{3,2},{4,7},{5,4},{6,5},{7,6},{8,11},{9,8},{10,9... | collective-permute-start | bytes 589832 | tf_op jit(solution)/shard_map/ppermute | solution.py:11
  48.2 0.5 fusion.4
  48.7 5.3 %collective-permute-done.9 = bf16[96,1024]{1,0:T(8,128)(2,1)S(1)} collective-permute-done((bf16[96,1024]{1,0:T(8,128)(2,1)S(1)}, bf16[96,1024]{1,0:T(8,128)(2,1)S(1)}, u32[]{:S(2)}, u32[]{:S(2)}) %collective-permute-start.9) | collective-permute-done | bytes 196640 | tf_op jit(solution)/shard_map/ppermute | solution.py:11
  54.1 2.3 %collective-permute-start.10 = (bf16[192,1024]{1,0:T(8,128)(2,1)S(1)}, bf16[192,1024]{1,0:T(8,128)(2,1)S(1)}, u32[]{:S(2)}, u32[]{:S(2)}) collective-permute-start(bf16[192,1024]{1,0:T(8,128)(2,1)S(1)} %pad_maximum_fusion.3), channel_id=1, source_target_pairs={{0,3},{1,0},{2,1},{3,2},{4,7},{5,4},{6,5},{7,6},{8,11},{9,8},{10,9... | collective-permute-start | bytes 1179656 | tf_op jit(solution)/shard_map/ppermute | solution.py:11
  56.5 0.5 fusion.6
  57.0 15.7 %collective-permute-done.10 = bf16[192,1024]{1,0:T(8,128)(2,1)S(1)} collective-permute-done((bf16[192,1024]{1,0:T(8,128)(2,1)S(1)}, bf16[192,1024]{1,0:T(8,128)(2,1)S(1)}, u32[]{:S(2)}, u32[]{:S(2)}) %collective-permute-start.10) | collective-permute-done | bytes 393248 | tf_op jit(solution)/shard_map/ppermute | solution.py:11
  72.7 0.2 add_convert_fusion
  73.1 1.7 %collective-permute-start.11 = (bf16[48,1024]{1,0:T(8,128)(2,1)S(1)}, bf16[48,1024]{1,0:T(8,128)(2,1)S(1)}, u32[]{:S(2)}, u32[]{:S(2)}) collective-permute-start(bf16[48,1024]{1,0:T(8,128)(2,1)S(1)} %get-tuple-element.18), channel_id=1, source_target_pairs={{0,12},{4,0},{8,4},{12,8},{1,13},{5,1},{9,5},{13,9},{2,14},{6,2},{... | collective-permute-start | bytes 294920 | tf_op jit(solution)/shard_map/ppermute | solution.py:11
  74.9 2.6 %collective-permute-done.13 = bf16[48,1024]{1,0:T(8,128)(2,1)S(1)} collective-permute-done((bf16[48,1024]{1,0:T(8,128)(2,1)S(1)}, bf16[48,1024]{1,0:T(8,128)(2,1)S(1)}, u32[]{:S(2)}, u32[]{:S(2)}) %collective-permute-start.13) | collective-permute-done | bytes 98336 | tf_op jit(solution)/shard_map/ppermute | solution.py:11
  77.5 1.3 %collective-permute-done.12 = bf16[48,1024]{1,0:T(8,128)(2,1)S(1)} collective-permute-done((bf16[48,1024]{1,0:T(8,128)(2,1)S(1)}, bf16[48,1024]{1,0:T(8,128)(2,1)S(1)}, u32[]{:S(2)}, u32[]{:S(2)}) %collective-permute-start.12) | collective-permute-done | bytes 98336 | tf_op jit(solution)/shard_map/ppermute | solution.py:11
  78.8 0.4 fusion.70
  79.2 0.5 multiply_reduce_fusion
  79.7 1.7 %collective-permute-start.16 = (f32[384]{0:T(512)S(1)}, f32[384]{0:T(512)S(1)}, u32[]{:S(2)}, u32[]{:S(2)}) collective-permute-start(f32[384]{0:T(512)S(1)} %get-tuple-element.29), channel_id=1, source_target_pairs={{0,3},{1,0},{2,1},{3,2},{4,7},{5,4},{6,5},{7,6},{8,11},{9,8},{10,9... | collective-permute-start | bytes 4616 | tf_op jit(solution)/shard_map/ppermute | solution.py:11
  81.3 0.4 collective-permute-start.15
  81.8 1.2 %collective-permute-start.14 = (f32[384]{0:T(512)S(1)}, f32[384]{0:T(512)S(1)}, u32[]{:S(2)}, u32[]{:S(2)}) collective-permute-start(f32[384]{0:T(512)S(1)} %get-tuple-element.29), channel_id=1, source_target_pairs={{0,1},{1,2},{2,3},{3,0},{4,5},{5,6},{6,7},{7,4},{8,9},{9,10},{10,1... | collective-permute-start | bytes 4616 | tf_op jit(solution)/shard_map/ppermute | solution.py:11
  82.9 0.4 collective-permute-done.16
  83.3 2.5 %collective-permute-done.15 = f32[384]{0:T(512)S(1)} collective-permute-done((f32[384]{0:T(512)S(1)}, f32[384]{0:T(512)S(1)}, u32[]{:S(2)}, u32[]{:S(2)}) %collective-permute-start.15) | collective-permute-done | bytes 1568 | tf_op jit(solution)/shard_map/ppermute | solution.py:11
  85.8 1.3 %collective-permute-done.14 = f32[384]{0:T(512)S(1)} collective-permute-done((f32[384]{0:T(512)S(1)}, f32[384]{0:T(512)S(1)}, u32[]{:S(2)}, u32[]{:S(2)}) %collective-permute-start.14) | collective-permute-done | bytes 1568 | tf_op jit(solution)/shard_map/ppermute | solution.py:11
  87.2 1.2 %multiply_convert_fusion = bf16[384,1024]{1,0:T(8,128)(2,1)} fusion(f32[1024]{0:T(1024)S(1)} %copy-done.4, f32[384]{0:T(512)S(1)} %add_rsqrt_fusion, f32[384,1024]{1,0:T(8,128)S(1)} %get-tuple-element.30, f32[384,1024]{1,0:T(8,128)S(1)} %fusion.70, bf16[384,1024]{1,0:T(8,128)(2,1)S(1)} %copy-done), kind=kLoop, calls=%fused_computation.24 | loop fusion | flops 2359296 | bytes 4724224 | tf_op jit(solution)/shard_map/convert_element_type | solution.py:133
  (47 shorter events, 1.1 us)
Async XLA Ops:
  0.0 5.7 %copy-start.3 = (f32[4096]{0:T(1024)S(1)}, f32[4096]{0:T(1024)}, u32[]{:S(2)}) copy-start(f32[4096]{0:T(1024)} %param.9) | copy-start | bytes 49156
  2.5 5.6 %collective-permute-start.2 = (bf16[48,1024]{1,0:T(8,128)(2,1)S(1)}, bf16[48,1024]{1,0:T(8,128)(2,1)S(1)}, u32[]{:S(2)}, u32[]{:S(2)}) collective-permute-start(bf16[48,1024]{1,0:T(8,128)(2,1)S(1)} %get-tuple-element.22), channel_id=1, source_target_pairs={{0,12},{4,0},{8,4},{12,8},{1,13},{5,1},{9,5},{13,9},{2,14},{6,2},{... | collective-permute-start | bytes 294920 | tf_op jit(solution)/shard_map/ppermute | solution.py:11
  4.9 6.1 %collective-permute-start.1 = (bf16[48,1024]{1,0:T(8,128)(2,1)S(1)}, bf16[48,1024]{1,0:T(8,128)(2,1)S(1)}, u32[]{:S(2)}, u32[]{:S(2)}) collective-permute-start(bf16[48,1024]{1,0:T(8,128)(2,1)S(1)} %get-tuple-element.23), channel_id=1, source_target_pairs={{0,8},{4,12},{8,0},{12,4},{1,9},{5,13},{9,1},{13,5},{2,10},{6,14},... | collective-permute-start | bytes 294920 | tf_op jit(solution)/shard_map/ppermute | solution.py:11
  5.6 5.5 %collective-permute-start = (bf16[48,1024]{1,0:T(8,128)(2,1)S(1)}, bf16[48,1024]{1,0:T(8,128)(2,1)S(1)}, u32[]{:S(2)}, u32[]{:S(2)}) collective-permute-start(bf16[48,1024]{1,0:T(8,128)(2,1)S(1)} %get-tuple-element.24), channel_id=1, source_target_pairs={{0,4},{4,8},{8,12},{12,0},{1,5},{5,9},{9,13},{13,1},{2,6},{6,10},{... | collective-permute-start | bytes 294920 | tf_op jit(solution)/shard_map/ppermute | solution.py:11
  11.2 13.3 %collective-permute-start.5 = (bf16[192,1024]{1,0:T(8,128)(2,1)S(1)}, bf16[192,1024]{1,0:T(8,128)(2,1)S(1)}, u32[]{:S(2)}, u32[]{:S(2)}) collective-permute-start(bf16[192,1024]{1,0:T(8,128)(2,1)S(1)} %get-tuple-element.14), channel_id=1, source_target_pairs={{0,3},{1,0},{2,1},{3,2},{4,7},{5,4},{6,5},{7,6},{8,11},{9,8},{10,9... | collective-permute-start | bytes 1179656 | tf_op jit(solution)/shard_map/ppermute | solution.py:11
  15.1 18.9 %collective-permute-start.3 = (bf16[192,1024]{1,0:T(8,128)(2,1)S(1)}, bf16[192,1024]{1,0:T(8,128)(2,1)S(1)}, u32[]{:S(2)}, u32[]{:S(2)}) collective-permute-start(bf16[192,1024]{1,0:T(8,128)(2,1)S(1)} %get-tuple-element.14), channel_id=1, source_target_pairs={{0,1},{1,2},{2,3},{3,0},{4,5},{5,6},{6,7},{7,4},{8,9},{9,10},{10,1... | collective-permute-start | bytes 1179656 | tf_op jit(solution)/shard_map/ppermute | solution.py:11
  15.1 20.8 %copy-start.1 = (bf16[1,4096,768]{2,1,0:T(8,128)(2,1)S(1)}, bf16[1,4096,768]{2,1,0:T(8,128)(2,1)}, u32[]{:S(2)}) copy-start(bf16[1,4096,768]{2,1,0:T(8,128)(2,1)} %param.14) | copy-start | bytes 18874372
  24.6 15.2 %collective-permute-start.6 = (bf16[96,1024]{1,0:T(8,128)(2,1)S(1)}, bf16[96,1024]{1,0:T(8,128)(2,1)S(1)}, u32[]{:S(2)}, u32[]{:S(2)}) collective-permute-start(bf16[96,1024]{1,0:T(8,128)(2,1)S(1)} %slice.71), channel_id=1, source_target_pairs={{0,3},{1,0},{2,1},{3,2},{4,7},{5,4},{6,5},{7,6},{8,11},{9,8},{10,9... | collective-permute-start | bytes 589832 | tf_op jit(solution)/shard_map/ppermute | solution.py:11
  34.0 7.5 %collective-permute-start.4 = (bf16[96,1024]{1,0:T(8,128)(2,1)S(1)}, bf16[96,1024]{1,0:T(8,128)(2,1)S(1)}, u32[]{:S(2)}, u32[]{:S(2)}) collective-permute-start(bf16[96,1024]{1,0:T(8,128)(2,1)S(1)} %slice.70), channel_id=1, source_target_pairs={{0,1},{1,2},{2,3},{3,0},{4,5},{5,6},{6,7},{7,4},{8,9},{9,10},{10,1... | collective-permute-start | bytes 589832 | tf_op jit(solution)/shard_map/ppermute | solution.py:11
  35.6 3.3 %copy-start.2 = (bf16[1,4096,768]{2,1,0:T(8,128)(2,1)S(1)}, bf16[1,4096,768]{2,1,0:T(8,128)(2,1)}, u32[]{:S(2)}) copy-start(bf16[1,4096,768]{2,1,0:T(8,128)(2,1)} %param.13) | copy-start | bytes 18874372
  39.3 3.7 %slice-start = ((s8[6291456]{0:T(1024)(128)(4,1)}), s8[4194304]{0:T(1024)(128)(4,1)S(1)}, s32[]{:S(2)}) async-start(s8[6291456]{0:T(1024)(128)(4,1)} %bitcast.53), calls=%async_computation | async-start | bytes 8388608
  41.7 1.6 %slice-start.1 = ((s8[6291456]{0:T(1024)(128)(4,1)}), s8[2097152]{0:T(1024)(128)(4,1)S(1)}, s32[]{:S(2)}) async-start(s8[6291456]{0:T(1024)(128)(4,1)} %bitcast.53), calls=%async_computation.1 | async-start | bytes 4194304
  44.3 12.1 %collective-permute-start.7 = (bf16[96,1024]{1,0:T(8,128)(2,1)S(1)}, bf16[96,1024]{1,0:T(8,128)(2,1)S(1)}, u32[]{:S(2)}, u32[]{:S(2)}) collective-permute-start(bf16[96,1024]{1,0:T(8,128)(2,1)S(1)} %get-tuple-element.19), channel_id=1, source_target_pairs={{0,1},{1,2},{2,3},{3,0},{4,5},{5,6},{6,7},{7,4},{8,9},{9,10},{10,1... | collective-permute-start | bytes 589832 | tf_op jit(solution)/shard_map/ppermute | solution.py:11
  45.0 9.0 %collective-permute-start.9 = (bf16[96,1024]{1,0:T(8,128)(2,1)S(1)}, bf16[96,1024]{1,0:T(8,128)(2,1)S(1)}, u32[]{:S(2)}, u32[]{:S(2)}) collective-permute-start(bf16[96,1024]{1,0:T(8,128)(2,1)S(1)} %get-tuple-element.20), channel_id=1, source_target_pairs={{0,3},{1,0},{2,1},{3,2},{4,7},{5,4},{6,5},{7,6},{8,11},{9,8},{10,9... | collective-permute-start | bytes 589832 | tf_op jit(solution)/shard_map/ppermute | solution.py:11
  48.7 7.8 %copy-start.5 = (f32[1,4,48]{2,1,0:T(4,128)S(1)}, f32[1,4,48]{2,1,0:T(4,128)}, u32[]{:S(2)}) copy-start(f32[1,4,48]{2,1,0:T(4,128)} %param.12) | copy-start | bytes 2308
  54.1 18.7 %collective-permute-start.10 = (bf16[192,1024]{1,0:T(8,128)(2,1)S(1)}, bf16[192,1024]{1,0:T(8,128)(2,1)S(1)}, u32[]{:S(2)}, u32[]{:S(2)}) collective-permute-start(bf16[192,1024]{1,0:T(8,128)(2,1)S(1)} %pad_maximum_fusion.3), channel_id=1, source_target_pairs={{0,3},{1,0},{2,1},{3,2},{4,7},{5,4},{6,5},{7,6},{8,11},{9,8},{10,9... | collective-permute-start | bytes 1179656 | tf_op jit(solution)/shard_map/ppermute | solution.py:11
  56.4 16.3 %collective-permute-start.8 = (bf16[192,1024]{1,0:T(8,128)(2,1)S(1)}, bf16[192,1024]{1,0:T(8,128)(2,1)S(1)}, u32[]{:S(2)}, u32[]{:S(2)}) collective-permute-start(bf16[192,1024]{1,0:T(8,128)(2,1)S(1)} %pad_maximum_fusion.2), channel_id=1, source_target_pairs={{0,1},{1,2},{2,3},{3,0},{4,5},{5,6},{6,7},{7,4},{8,9},{9,10},{10,1... | collective-permute-start | bytes 1179656 | tf_op jit(solution)/shard_map/ppermute | solution.py:11
  72.9 6.2 %copy-start = (bf16[384,1024]{1,0:T(8,128)(2,1)S(1)}, bf16[384,1024]{1,0:T(8,128)(2,1)}, u32[]{:S(2)}) copy-start(bf16[384,1024]{1,0:T(8,128)(2,1)} %param.8) | copy-start | bytes 2359300
  73.0 4.5 %collective-permute-start.13 = (bf16[48,1024]{1,0:T(8,128)(2,1)S(1)}, bf16[48,1024]{1,0:T(8,128)(2,1)S(1)}, u32[]{:S(2)}, u32[]{:S(2)}) collective-permute-start(bf16[48,1024]{1,0:T(8,128)(2,1)S(1)} %get-tuple-element.16), channel_id=1, source_target_pairs={{0,4},{4,8},{8,12},{12,0},{1,5},{5,9},{9,13},{13,1},{2,6},{6,10},{... | collective-permute-start | bytes 294920 | tf_op jit(solution)/shard_map/ppermute | solution.py:11
  73.0 5.7 %collective-permute-start.12 = (bf16[48,1024]{1,0:T(8,128)(2,1)S(1)}, bf16[48,1024]{1,0:T(8,128)(2,1)S(1)}, u32[]{:S(2)}, u32[]{:S(2)}) collective-permute-start(bf16[48,1024]{1,0:T(8,128)(2,1)S(1)} %get-tuple-element.17), channel_id=1, source_target_pairs={{0,8},{4,12},{8,0},{12,4},{1,9},{5,13},{9,1},{13,5},{2,10},{6,14},... | collective-permute-start | bytes 294920 | tf_op jit(solution)/shard_map/ppermute | solution.py:11
  73.1 5.7 %collective-permute-start.11 = (bf16[48,1024]{1,0:T(8,128)(2,1)S(1)}, bf16[48,1024]{1,0:T(8,128)(2,1)S(1)}, u32[]{:S(2)}, u32[]{:S(2)}) collective-permute-start(bf16[48,1024]{1,0:T(8,128)(2,1)S(1)} %get-tuple-element.18), channel_id=1, source_target_pairs={{0,12},{4,0},{8,4},{12,8},{1,13},{5,1},{9,5},{13,9},{2,14},{6,2},{... | collective-permute-start | bytes 294920 | tf_op jit(solution)/shard_map/ppermute | solution.py:11
  79.1 8.0 %copy-start.4 = (f32[1024]{0:T(1024)S(1)}, f32[1024]{0:T(1024)}, u32[]{:S(2)}) copy-start(f32[1024]{0:T(1024)} %param.10) | copy-start | bytes 12292
  79.7 3.6 %collective-permute-start.16 = (f32[384]{0:T(512)S(1)}, f32[384]{0:T(512)S(1)}, u32[]{:S(2)}, u32[]{:S(2)}) collective-permute-start(f32[384]{0:T(512)S(1)} %get-tuple-element.29), channel_id=1, source_target_pairs={{0,3},{1,0},{2,1},{3,2},{4,7},{5,4},{6,5},{7,6},{8,11},{9,8},{10,9... | collective-permute-start | bytes 4616 | tf_op jit(solution)/shard_map/ppermute | solution.py:11
  81.3 4.5 %collective-permute-start.15 = (f32[384]{0:T(512)S(1)}, f32[384]{0:T(512)S(1)}, u32[]{:S(2)}, u32[]{:S(2)}) collective-permute-start(f32[384]{0:T(512)S(1)} %get-tuple-element.29), channel_id=1, source_target_pairs={{0,2},{1,3},{2,0},{3,1},{4,6},{5,7},{6,4},{7,5},{8,10},{9,11},{10,... | collective-permute-start | bytes 4616 | tf_op jit(solution)/shard_map/ppermute | solution.py:11
  81.8 5.4 %collective-permute-start.14 = (f32[384]{0:T(512)S(1)}, f32[384]{0:T(512)S(1)}, u32[]{:S(2)}, u32[]{:S(2)}) collective-permute-start(f32[384]{0:T(512)S(1)} %get-tuple-element.29), channel_id=1, source_target_pairs={{0,1},{1,2},{2,3},{3,0},{4,5},{5,6},{6,7},{7,4},{8,9},{9,10},{10,1... | collective-permute-start | bytes 4616 | tf_op jit(solution)/shard_map/ppermute | solution.py:11

commit v5 on v4

--- a/solution.py
+++ b/solution.py
@@ -62,7 +62,9 @@
     bf16, f32 = jnp.bfloat16, jnp.float32
 
     def relative(table):
-        return lax.dynamic_slice_in_dim(jnp.concatenate([table, table], axis=0), here_ep, n_ep, 0)
+        wanted = (here_ep + lax.broadcasted_iota(jnp.int32, (n_ep, n_ep, 1), 0)) % n_ep
+        own = wanted == lax.broadcasted_iota(jnp.int32, (n_ep, n_ep, 1), 1)
+        return jnp.sum(jnp.where(own, table[None], jnp.zeros_like(table)[None]), axis=1)
 
     slots = relative(chosen[0]).reshape(-1)
     weights = relative(route_weight[0]).reshape(-1)

time: 88.7 us -> 88.7 us (level)
  no operation moved by 1% of the time
where the time goes in v5:
time: 88.7 us; the launch traced here: 88.5 us
  waiting for transfers between devices  46.4 us (52%)
  starting transfers between devices  24.3 us (27%)
  matrix products  13.2 us (15%)
  other arithmetic  3.45 us (4%)
    ppermute x17, waiting for transfers between devices, shift(): return lax.ppermute(value, axis, [(i, (i + step) % n) for i in range(n)])  46.4 us
    ppermute x17, starting transfers between devices, shift(): return lax.ppermute(value, axis, [(i, (i + step) % n) for i in range(n)])  24.3 us
    dot_general x4, matrix products, chunk(): jnp.dot(scaled, gate_rows, preferred_element_type=f32)  5.24 us
    dot_general x4, matrix products, chunk(): jnp.dot(scaled, up_rows, preferred_element_type=f32)  3.58 us
    dot_general x4, matrix products, part(): return jnp.dot(hidden, columns, preferred_element_type=f32)  1.93 us
  transfers between devices with their start and end apart: 17, of which 12 were waited for; matrix products, arithmetic and copies ran while one was open for 11% of the time, Pallas kernels for 0%

profile of v5, /device:TPU:0, one launch (start us, length us, event | category | flops | bytes accessed | tf_op | source)
XLA Modules:
  0.0 88.5 jit_solution(1834973591849075829)
XLA Ops:
  0.1 0.8 select_reduce_fusion.1
  1.0 1.6 %convolution_convert_fusion = bf16[192,1024]{1,0:T(8,128)(2,1)S(1)} fusion(bf16[384,1024]{1,0:T(8,128)(2,1)} %param.8, s32[192]{0:T(256)S(1)} %eq.32), kind=kOutput, calls=%fused_computation.44 | convolution fusion | flops 151265280 | bytes 1180416 | tf_op jit(solution)/shard_map/dot_general | solution.py:75
  2.6 2.5 %collective-permute-start.2 = (bf16[48,1024]{1,0:T(8,128)(2,1)S(1)}, bf16[48,1024]{1,0:T(8,128)(2,1)S(1)}, u32[]{:S(2)}, u32[]{:S(2)}) collective-permute-start(bf16[48,1024]{1,0:T(8,128)(2,1)S(1)} %get-tuple-element.22), channel_id=1, source_target_pairs={{0,12},{4,0},{8,4},{12,8},{1,13},{5,1},{9,5},{13,9},{2,14},{6,2},{... | collective-permute-start | bytes 294920 | tf_op jit(solution)/shard_map/ppermute | solution.py:11
  5.0 0.6 collective-permute-start.1
  5.8 2.3 %collective-permute-done.2 = bf16[48,1024]{1,0:T(8,128)(2,1)S(1)} collective-permute-done((bf16[48,1024]{1,0:T(8,128)(2,1)S(1)}, bf16[48,1024]{1,0:T(8,128)(2,1)S(1)}, u32[]{:S(2)}, u32[]{:S(2)}) %collective-permute-start.2) | collective-permute-done | bytes 98336 | tf_op jit(solution)/shard_map/ppermute | solution.py:11
  8.1 3.0 %collective-permute-done.1 = bf16[48,1024]{1,0:T(8,128)(2,1)S(1)} collective-permute-done((bf16[48,1024]{1,0:T(8,128)(2,1)S(1)}, bf16[48,1024]{1,0:T(8,128)(2,1)S(1)}, u32[]{:S(2)}, u32[]{:S(2)}) %collective-permute-start.1) | collective-permute-done | bytes 98336 | tf_op jit(solution)/shard_map/ppermute | solution.py:11
  11.3 3.8 %collective-permute-start.5 = (bf16[192,1024]{1,0:T(8,128)(2,1)S(1)}, bf16[192,1024]{1,0:T(8,128)(2,1)S(1)}, u32[]{:S(2)}, u32[]{:S(2)}) collective-permute-start(bf16[192,1024]{1,0:T(8,128)(2,1)S(1)} %get-tuple-element.14), channel_id=1, source_target_pairs={{0,3},{1,0},{2,1},{3,2},{4,7},{5,4},{6,5},{7,6},{8,11},{9,8},{10,9... | collective-permute-start | bytes 1179656 | tf_op jit(solution)/shard_map/ppermute | solution.py:11
  15.2 2.0 %fusion.22 = f32[192,768]{1,0:T(8,128)S(1)} fusion(bf16[1,4096,768]{2,1,0:T(8,128)(2,1)} %param.13, s32[]{:T(128)S(6)} %select_n.81, bf16[192,1024]{1,0:T(8,128)(2,1)S(1)} %get-tuple-element.14, f32[1024]{0:T(1024)S(1)} %get-tuple-element.27), kind=kOutput, calls=%fused_computation.22 | convolution fusion | flops 302579712 | bytes 2560004 | tf_op jit(solution)/shard_map/dot_general | solution.py:98
  17.2 2.1 %fusion.16 = f32[192,768]{1,0:T(8,128)S(1)} fusion(bf16[1,4096,768]{2,1,0:T(8,128)(2,1)} %param.14, s32[]{:T(128)S(6)} %select_n.81, bf16[192,1024]{1,0:T(8,128)(2,1)S(1)} %get-tuple-element.14, f32[1024]{0:T(1024)S(1)} %get-tuple-element.27), kind=kOutput, calls=%fused_computation.16 | convolution fusion | flops 302579712 | bytes 2560004 | tf_op jit(solution)/shard_map/dot_general | solution.py:99
  19.3 5.3 %collective-permute-done.5 = bf16[192,1024]{1,0:T(8,128)(2,1)S(1)} collective-permute-done((bf16[192,1024]{1,0:T(8,128)(2,1)S(1)}, bf16[192,1024]{1,0:T(8,128)(2,1)S(1)}, u32[]{:S(2)}, u32[]{:S(2)}) %collective-permute-start.5) | collective-permute-done | bytes 393248 | tf_op jit(solution)/shard_map/ppermute | solution.py:11
  24.7 4.3 %collective-permute-start.6 = (bf16[96,1024]{1,0:T(8,128)(2,1)S(1)}, bf16[96,1024]{1,0:T(8,128)(2,1)S(1)}, u32[]{:S(2)}, u32[]{:S(2)}) collective-permute-start(bf16[96,1024]{1,0:T(8,128)(2,1)S(1)} %slice.71), channel_id=1, source_target_pairs={{0,3},{1,0},{2,1},{3,2},{4,7},{5,4},{6,5},{7,6},{8,11},{9,8},{10,9... | collective-permute-start | bytes 589832 | tf_op jit(solution)/shard_map/ppermute | solution.py:11
  29.0 5.0 %collective-permute-done.3 = bf16[192,1024]{1,0:T(8,128)(2,1)S(1)} collective-permute-done((bf16[192,1024]{1,0:T(8,128)(2,1)S(1)}, bf16[192,1024]{1,0:T(8,128)(2,1)S(1)}, u32[]{:S(2)}, u32[]{:S(2)}) %collective-permute-start.3) | collective-permute-done | bytes 393248 | tf_op jit(solution)/shard_map/ppermute | solution.py:11
  34.1 1.6 %collective-permute-start.4 = (bf16[96,1024]{1,0:T(8,128)(2,1)S(1)}, bf16[96,1024]{1,0:T(8,128)(2,1)S(1)}, u32[]{:S(2)}, u32[]{:S(2)}) collective-permute-start(bf16[96,1024]{1,0:T(8,128)(2,1)S(1)} %slice.70), channel_id=1, source_target_pairs={{0,1},{1,2},{2,3},{3,0},{4,5},{5,6},{6,7},{7,4},{8,9},{9,10},{10,1... | collective-permute-start | bytes 589832 | tf_op jit(solution)/shard_map/ppermute | solution.py:11
  35.7 0.2 fusion.55
  35.8 0.2 fusion.53
  36.0 0.5 fusion.12
  36.5 2.2 %fusion.18 = f32[192,768]{1,0:T(8,128)S(1)} fusion(bf16[1,4096,768]{2,1,0:T(8,128)(2,1)} %param.13, s32[]{:T(128)S(6)} %select_n.85, bf16[192,1024]{1,0:T(8,128)(2,1)S(1)} %collective-permute-done.5, f32[1024]{0:T(1024)S(1)} %get-tuple-element.28), kind=kOutput, calls=%fused_computation.18 | convolution fusion | flops 302579712 | bytes 2560004 | tf_op jit(solution)/shard_map/dot_general | solution.py:98
  38.7 0.2 copy-done.2
  38.9 0.5 fusion.39
  39.4 0.5 fusion.45
  39.9 1.7 %collective-permute-done.4 = bf16[96,1024]{1,0:T(8,128)(2,1)S(1)} collective-permute-done((bf16[96,1024]{1,0:T(8,128)(2,1)S(1)}, bf16[96,1024]{1,0:T(8,128)(2,1)S(1)}, u32[]{:S(2)}, u32[]{:S(2)}) %collective-permute-start.4) | collective-permute-done | bytes 196640 | tf_op jit(solution)/shard_map/ppermute | solution.py:11
  41.6 0.2 fusion.58
  41.8 0.5 fusion.8
  42.3 0.5 fusion.10
  42.8 0.3 multiply_convert_fusion.1
  43.1 0.3 slice-done.1
  43.4 0.5 fusion.48
  43.9 0.5 fusion
  44.4 0.7 collective-permute-start.7
  45.1 3.1 %collective-permute-start.9 = (bf16[96,1024]{1,0:T(8,128)(2,1)S(1)}, bf16[96,1024]{1,0:T(8,128)(2,1)S(1)}, u32[]{:S(2)}, u32[]{:S(2)}) collective-permute-start(bf16[96,1024]{1,0:T(8,128)(2,1)S(1)} %get-tuple-element.20), channel_id=1, source_target_pairs={{0,3},{1,0},{2,1},{3,2},{4,7},{5,4},{6,5},{7,6},{8,11},{9,8},{10,9... | collective-permute-start | bytes 589832 | tf_op jit(solution)/shard_map/ppermute | solution.py:11
  48.3 0.5 fusion.4
  48.8 5.3 %collective-permute-done.9 = bf16[96,1024]{1,0:T(8,128)(2,1)S(1)} collective-permute-done((bf16[96,1024]{1,0:T(8,128)(2,1)S(1)}, bf16[96,1024]{1,0:T(8,128)(2,1)S(1)}, u32[]{:S(2)}, u32[]{:S(2)}) %collective-permute-start.9) | collective-permute-done | bytes 196640 | tf_op jit(solution)/shard_map/ppermute | solution.py:11
  54.2 2.3 %collective-permute-start.10 = (bf16[192,1024]{1,0:T(8,128)(2,1)S(1)}, bf16[192,1024]{1,0:T(8,128)(2,1)S(1)}, u32[]{:S(2)}, u32[]{:S(2)}) collective-permute-start(bf16[192,1024]{1,0:T(8,128)(2,1)S(1)} %pad_maximum_fusion.3), channel_id=1, source_target_pairs={{0,3},{1,0},{2,1},{3,2},{4,7},{5,4},{6,5},{7,6},{8,11},{9,8},{10,9... | collective-permute-start | bytes 1179656 | tf_op jit(solution)/shard_map/ppermute | solution.py:11
  56.6 0.5 fusion.6
  57.1 15.7 %collective-permute-done.10 = bf16[192,1024]{1,0:T(8,128)(2,1)S(1)} collective-permute-done((bf16[192,1024]{1,0:T(8,128)(2,1)S(1)}, bf16[192,1024]{1,0:T(8,128)(2,1)S(1)}, u32[]{:S(2)}, u32[]{:S(2)}) %collective-permute-start.10) | collective-permute-done | bytes 393248 | tf_op jit(solution)/shard_map/ppermute | solution.py:11
  72.8 0.2 add_convert_fusion
  73.2 1.7 %collective-permute-start.11 = (bf16[48,1024]{1,0:T(8,128)(2,1)S(1)}, bf16[48,1024]{1,0:T(8,128)(2,1)S(1)}, u32[]{:S(2)}, u32[]{:S(2)}) collective-permute-start(bf16[48,1024]{1,0:T(8,128)(2,1)S(1)} %get-tuple-element.18), channel_id=1, source_target_pairs={{0,12},{4,0},{8,4},{12,8},{1,13},{5,1},{9,5},{13,9},{2,14},{6,2},{... | collective-permute-start | bytes 294920 | tf_op jit(solution)/shard_map/ppermute | solution.py:11
  75.0 2.5 %collective-permute-done.13 = bf16[48,1024]{1,0:T(8,128)(2,1)S(1)} collective-permute-done((bf16[48,1024]{1,0:T(8,128)(2,1)S(1)}, bf16[48,1024]{1,0:T(8,128)(2,1)S(1)}, u32[]{:S(2)}, u32[]{:S(2)}) %collective-permute-start.13) | collective-permute-done | bytes 98336 | tf_op jit(solution)/shard_map/ppermute | solution.py:11
  77.6 1.3 %collective-permute-done.12 = bf16[48,1024]{1,0:T(8,128)(2,1)S(1)} collective-permute-done((bf16[48,1024]{1,0:T(8,128)(2,1)S(1)}, bf16[48,1024]{1,0:T(8,128)(2,1)S(1)}, u32[]{:S(2)}, u32[]{:S(2)}) %collective-permute-start.12) | collective-permute-done | bytes 98336 | tf_op jit(solution)/shard_map/ppermute | solution.py:11
  78.9 0.4 fusion.70
  79.3 0.5 multiply_reduce_fusion
  79.8 1.7 %collective-permute-start.16 = (f32[384]{0:T(512)S(1)}, f32[384]{0:T(512)S(1)}, u32[]{:S(2)}, u32[]{:S(2)}) collective-permute-start(f32[384]{0:T(512)S(1)} %get-tuple-element.29), channel_id=1, source_target_pairs={{0,3},{1,0},{2,1},{3,2},{4,7},{5,4},{6,5},{7,6},{8,11},{9,8},{10,9... | collective-permute-start | bytes 4616 | tf_op jit(solution)/shard_map/ppermute | solution.py:11
  81.4 0.4 collective-permute-start.15
  81.9 1.2 %collective-permute-start.14 = (f32[384]{0:T(512)S(1)}, f32[384]{0:T(512)S(1)}, u32[]{:S(2)}, u32[]{:S(2)}) collective-permute-start(f32[384]{0:T(512)S(1)} %get-tuple-element.29), channel_id=1, source_target_pairs={{0,1},{1,2},{2,3},{3,0},{4,5},{5,6},{6,7},{7,4},{8,9},{9,10},{10,1... | collective-permute-start | bytes 4616 | tf_op jit(solution)/shard_map/ppermute | solution.py:11
  83.0 0.4 collective-permute-done.16
  83.4 2.5 %collective-permute-done.15 = f32[384]{0:T(512)S(1)} collective-permute-done((f32[384]{0:T(512)S(1)}, f32[384]{0:T(512)S(1)}, u32[]{:S(2)}, u32[]{:S(2)}) %collective-permute-start.15) | collective-permute-done | bytes 1568 | tf_op jit(solution)/shard_map/ppermute | solution.py:11
  85.9 1.3 %collective-permute-done.14 = f32[384]{0:T(512)S(1)} collective-permute-done((f32[384]{0:T(512)S(1)}, f32[384]{0:T(512)S(1)}, u32[]{:S(2)}, u32[]{:S(2)}) %collective-permute-start.14) | collective-permute-done | bytes 1568 | tf_op jit(solution)/shard_map/ppermute | solution.py:11
  87.3 1.2 %multiply_convert_fusion = bf16[384,1024]{1,0:T(8,128)(2,1)} fusion(f32[1024]{0:T(1024)S(1)} %copy-done.4, f32[384]{0:T(512)S(1)} %add_rsqrt_fusion, f32[384,1024]{1,0:T(8,128)S(1)} %get-tuple-element.30, f32[384,1024]{1,0:T(8,128)S(1)} %fusion.70, bf16[384,1024]{1,0:T(8,128)(2,1)S(1)} %copy-done), kind=kLoop, calls=%fused_computation.24 | loop fusion | flops 2359296 | bytes 4724224 | tf_op jit(solution)/shard_map/convert_element_type | solution.py:135
  (48 shorter events, 1.2 us)
Async XLA Ops:
  0.0 5.8 %copy-start.3 = (f32[4096]{0:T(1024)S(1)}, f32[4096]{0:T(1024)}, u32[]{:S(2)}) copy-start(f32[4096]{0:T(1024)} %param.9) | copy-start | bytes 49156
  2.6 5.6 %collective-permute-start.2 = (bf16[48,1024]{1,0:T(8,128)(2,1)S(1)}, bf16[48,1024]{1,0:T(8,128)(2,1)S(1)}, u32[]{:S(2)}, u32[]{:S(2)}) collective-permute-start(bf16[48,1024]{1,0:T(8,128)(2,1)S(1)} %get-tuple-element.22), channel_id=1, source_target_pairs={{0,12},{4,0},{8,4},{12,8},{1,13},{5,1},{9,5},{13,9},{2,14},{6,2},{... | collective-permute-start | bytes 294920 | tf_op jit(solution)/shard_map/ppermute | solution.py:11
  5.0 6.1 %collective-permute-start.1 = (bf16[48,1024]{1,0:T(8,128)(2,1)S(1)}, bf16[48,1024]{1,0:T(8,128)(2,1)S(1)}, u32[]{:S(2)}, u32[]{:S(2)}) collective-permute-start(bf16[48,1024]{1,0:T(8,128)(2,1)S(1)} %get-tuple-element.23), channel_id=1, source_target_pairs={{0,8},{4,12},{8,0},{12,4},{1,9},{5,13},{9,1},{13,5},{2,10},{6,14},... | collective-permute-start | bytes 294920 | tf_op jit(solution)/shard_map/ppermute | solution.py:11
  5.7 5.5 %collective-permute-start = (bf16[48,1024]{1,0:T(8,128)(2,1)S(1)}, bf16[48,1024]{1,0:T(8,128)(2,1)S(1)}, u32[]{:S(2)}, u32[]{:S(2)}) collective-permute-start(bf16[48,1024]{1,0:T(8,128)(2,1)S(1)} %get-tuple-element.24), channel_id=1, source_target_pairs={{0,4},{4,8},{8,12},{12,0},{1,5},{5,9},{9,13},{13,1},{2,6},{6,10},{... | collective-permute-start | bytes 294920 | tf_op jit(solution)/shard_map/ppermute | solution.py:11
  11.3 13.3 %collective-permute-start.5 = (bf16[192,1024]{1,0:T(8,128)(2,1)S(1)}, bf16[192,1024]{1,0:T(8,128)(2,1)S(1)}, u32[]{:S(2)}, u32[]{:S(2)}) collective-permute-start(bf16[192,1024]{1,0:T(8,128)(2,1)S(1)} %get-tuple-element.14), channel_id=1, source_target_pairs={{0,3},{1,0},{2,1},{3,2},{4,7},{5,4},{6,5},{7,6},{8,11},{9,8},{10,9... | collective-permute-start | bytes 1179656 | tf_op jit(solution)/shard_map/ppermute | solution.py:11
  15.2 18.9 %collective-permute-start.3 = (bf16[192,1024]{1,0:T(8,128)(2,1)S(1)}, bf16[192,1024]{1,0:T(8,128)(2,1)S(1)}, u32[]{:S(2)}, u32[]{:S(2)}) collective-permute-start(bf16[192,1024]{1,0:T(8,128)(2,1)S(1)} %get-tuple-element.14), channel_id=1, source_target_pairs={{0,1},{1,2},{2,3},{3,0},{4,5},{5,6},{6,7},{7,4},{8,9},{9,10},{10,1... | collective-permute-start | bytes 1179656 | tf_op jit(solution)/shard_map/ppermute | solution.py:11
  15.2 20.8 %copy-start.1 = (bf16[1,4096,768]{2,1,0:T(8,128)(2,1)S(1)}, bf16[1,4096,768]{2,1,0:T(8,128)(2,1)}, u32[]{:S(2)}) copy-start(bf16[1,4096,768]{2,1,0:T(8,128)(2,1)} %param.14) | copy-start | bytes 18874372
  24.7 15.2 %collective-permute-start.6 = (bf16[96,1024]{1,0:T(8,128)(2,1)S(1)}, bf16[96,1024]{1,0:T(8,128)(2,1)S(1)}, u32[]{:S(2)}, u32[]{:S(2)}) collective-permute-start(bf16[96,1024]{1,0:T(8,128)(2,1)S(1)} %slice.71), channel_id=1, source_target_pairs={{0,3},{1,0},{2,1},{3,2},{4,7},{5,4},{6,5},{7,6},{8,11},{9,8},{10,9... | collective-permute-start | bytes 589832 | tf_op jit(solution)/shard_map/ppermute | solution.py:11
  34.1 7.5 %collective-permute-start.4 = (bf16[96,1024]{1,0:T(8,128)(2,1)S(1)}, bf16[96,1024]{1,0:T(8,128)(2,1)S(1)}, u32[]{:S(2)}, u32[]{:S(2)}) collective-permute-start(bf16[96,1024]{1,0:T(8,128)(2,1)S(1)} %slice.70), channel_id=1, source_target_pairs={{0,1},{1,2},{2,3},{3,0},{4,5},{5,6},{6,7},{7,4},{8,9},{9,10},{10,1... | collective-permute-start | bytes 589832 | tf_op jit(solution)/shard_map/ppermute | solution.py:11
  35.7 3.3 %copy-start.2 = (bf16[1,4096,768]{2,1,0:T(8,128)(2,1)S(1)}, bf16[1,4096,768]{2,1,0:T(8,128)(2,1)}, u32[]{:S(2)}) copy-start(bf16[1,4096,768]{2,1,0:T(8,128)(2,1)} %param.13) | copy-start | bytes 18874372
  39.4 3.7 %slice-start = ((s8[6291456]{0:T(1024)(128)(4,1)}), s8[4194304]{0:T(1024)(128)(4,1)S(1)}, s32[]{:S(2)}) async-start(s8[6291456]{0:T(1024)(128)(4,1)} %bitcast.53), calls=%async_computation | async-start | bytes 8388608
  41.8 1.6 %slice-start.1 = ((s8[6291456]{0:T(1024)(128)(4,1)}), s8[2097152]{0:T(1024)(128)(4,1)S(1)}, s32[]{:S(2)}) async-start(s8[6291456]{0:T(1024)(128)(4,1)} %bitcast.53), calls=%async_computation.1 | async-start | bytes 4194304
  44.4 12.1 %collective-permute-start.7 = (bf16[96,1024]{1,0:T(8,128)(2,1)S(1)}, bf16[96,1024]{1,0:T(8,128)(2,1)S(1)}, u32[]{:S(2)}, u32[]{:S(2)}) collective-permute-start(bf16[96,1024]{1,0:T(8,128)(2,1)S(1)} %get-tuple-element.19), channel_id=1, source_target_pairs={{0,1},{1,2},{2,3},{3,0},{4,5},{5,6},{6,7},{7,4},{8,9},{9,10},{10,1... | collective-permute-start | bytes 589832 | tf_op jit(solution)/shard_map/ppermute | solution.py:11
  45.1 9.0 %collective-permute-start.9 = (bf16[96,1024]{1,0:T(8,128)(2,1)S(1)}, bf16[96,1024]{1,0:T(8,128)(2,1)S(1)}, u32[]{:S(2)}, u32[]{:S(2)}) collective-permute-start(bf16[96,1024]{1,0:T(8,128)(2,1)S(1)} %get-tuple-element.20), channel_id=1, source_target_pairs={{0,3},{1,0},{2,1},{3,2},{4,7},{5,4},{6,5},{7,6},{8,11},{9,8},{10,9... | collective-permute-start | bytes 589832 | tf_op jit(solution)/shard_map/ppermute | solution.py:11
  54.2 18.7 %collective-permute-start.10 = (bf16[192,1024]{1,0:T(8,128)(2,1)S(1)}, bf16[192,1024]{1,0:T(8,128)(2,1)S(1)}, u32[]{:S(2)}, u32[]{:S(2)}) collective-permute-start(bf16[192,1024]{1,0:T(8,128)(2,1)S(1)} %pad_maximum_fusion.3), channel_id=1, source_target_pairs={{0,3},{1,0},{2,1},{3,2},{4,7},{5,4},{6,5},{7,6},{8,11},{9,8},{10,9... | collective-permute-start | bytes 1179656 | tf_op jit(solution)/shard_map/ppermute | solution.py:11
  56.6 16.3 %collective-permute-start.8 = (bf16[192,1024]{1,0:T(8,128)(2,1)S(1)}, bf16[192,1024]{1,0:T(8,128)(2,1)S(1)}, u32[]{:S(2)}, u32[]{:S(2)}) collective-permute-start(bf16[192,1024]{1,0:T(8,128)(2,1)S(1)} %pad_maximum_fusion.2), channel_id=1, source_target_pairs={{0,1},{1,2},{2,3},{3,0},{4,5},{5,6},{6,7},{7,4},{8,9},{9,10},{10,1... | collective-permute-start | bytes 1179656 | tf_op jit(solution)/shard_map/ppermute | solution.py:11
  57.1 17.8 %copy-start.5 = (f32[1,4,48]{2,1,0:T(4,128)S(1)}, f32[1,4,48]{2,1,0:T(4,128)}, u32[]{:S(2)}) copy-start(f32[1,4,48]{2,1,0:T(4,128)} %param.12) | copy-start | bytes 2308
  73.0 6.2 %copy-start = (bf16[384,1024]{1,0:T(8,128)(2,1)S(1)}, bf16[384,1024]{1,0:T(8,128)(2,1)}, u32[]{:S(2)}) copy-start(bf16[384,1024]{1,0:T(8,128)(2,1)} %param.8) | copy-start | bytes 2359300
  73.1 4.5 %collective-permute-start.13 = (bf16[48,1024]{1,0:T(8,128)(2,1)S(1)}, bf16[48,1024]{1,0:T(8,128)(2,1)S(1)}, u32[]{:S(2)}, u32[]{:S(2)}) collective-permute-start(bf16[48,1024]{1,0:T(8,128)(2,1)S(1)} %get-tuple-element.16), channel_id=1, source_target_pairs={{0,4},{4,8},{8,12},{12,0},{1,5},{5,9},{9,13},{13,1},{2,6},{6,10},{... | collective-permute-start | bytes 294920 | tf_op jit(solution)/shard_map/ppermute | solution.py:11
  73.1 5.7 %collective-permute-start.12 = (bf16[48,1024]{1,0:T(8,128)(2,1)S(1)}, bf16[48,1024]{1,0:T(8,128)(2,1)S(1)}, u32[]{:S(2)}, u32[]{:S(2)}) collective-permute-start(bf16[48,1024]{1,0:T(8,128)(2,1)S(1)} %get-tuple-element.17), channel_id=1, source_target_pairs={{0,8},{4,12},{8,0},{12,4},{1,9},{5,13},{9,1},{13,5},{2,10},{6,14},... | collective-permute-start | bytes 294920 | tf_op jit(solution)/shard_map/ppermute | solution.py:11
  73.2 5.7 %collective-permute-start.11 = (bf16[48,1024]{1,0:T(8,128)(2,1)S(1)}, bf16[48,1024]{1,0:T(8,128)(2,1)S(1)}, u32[]{:S(2)}, u32[]{:S(2)}) collective-permute-start(bf16[48,1024]{1,0:T(8,128)(2,1)S(1)} %get-tuple-element.18), channel_id=1, source_target_pairs={{0,12},{4,0},{8,4},{12,8},{1,13},{5,1},{9,5},{13,9},{2,14},{6,2},{... | collective-permute-start | bytes 294920 | tf_op jit(solution)/shard_map/ppermute | solution.py:11
  79.2 8.0 %copy-start.4 = (f32[1024]{0:T(1024)S(1)}, f32[1024]{0:T(1024)}, u32[]{:S(2)}) copy-start(f32[1024]{0:T(1024)} %param.10) | copy-start | bytes 12292
  79.8 3.6 %collective-permute-start.16 = (f32[384]{0:T(512)S(1)}, f32[384]{0:T(512)S(1)}, u32[]{:S(2)}, u32[]{:S(2)}) collective-permute-start(f32[384]{0:T(512)S(1)} %get-tuple-element.29), channel_id=1, source_target_pairs={{0,3},{1,0},{2,1},{3,2},{4,7},{5,4},{6,5},{7,6},{8,11},{9,8},{10,9... | collective-permute-start | bytes 4616 | tf_op jit(solution)/shard_map/ppermute | solution.py:11
  81.4 4.5 %collective-permute-start.15 = (f32[384]{0:T(512)S(1)}, f32[384]{0:T(512)S(1)}, u32[]{:S(2)}, u32[]{:S(2)}) collective-permute-start(f32[384]{0:T(512)S(1)} %get-tuple-element.29), channel_id=1, source_target_pairs={{0,2},{1,3},{2,0},{3,1},{4,6},{5,7},{6,4},{7,5},{8,10},{9,11},{10,... | collective-permute-start | bytes 4616 | tf_op jit(solution)/shard_map/ppermute | solution.py:11
  81.9 5.4 %collective-permute-start.14 = (f32[384]{0:T(512)S(1)}, f32[384]{0:T(512)S(1)}, u32[]{:S(2)}, u32[]{:S(2)}) collective-permute-start(f32[384]{0:T(512)S(1)} %get-tuple-element.29), channel_id=1, source_target_pairs={{0,1},{1,2},{2,3},{3,0},{4,5},{5,6},{6,7},{7,4},{8,9},{9,10},{10,1... | collective-permute-start | bytes 4616 | tf_op jit(solution)/shard_map/ppermute | solution.py:11
